TPU v7x, 32 devices: a whole 2x2x4 slice. The times are simulated.
32 devices in a mesh: ep: 4 (over y, x), tp: 8 (over z, core).
Axes of the slice: x: 2, y: 2, z: 4, core: 2. Of those that a mesh axis runs over, the one named last changes fastest.
Arguments:
- residual: bfloat16 [128, 2048], P('ep'), may hold values from -6 to 6
- mixer_gain: float32 [2048], replicated, may hold values from 0.1 to 1.9
- gate_proj: bfloat16 [2048, 2048], P('ep', 'tp'), may hold values from -0.125 to 0.125
- input_proj: bfloat16 [2048, 2048], P('ep', 'tp'), may hold values from -0.125 to 0.125
- write_proj: bfloat16 [2048, 2048], P('ep', 'tp'), may hold values from -0.125 to 0.125
- read_proj: bfloat16 [2048, 2048], P('ep', 'tp'), may hold values from -0.125 to 0.125
- step_proj: bfloat16 [2048, 32], replicated, may hold values from -0.125 to 0.125
- conv_weight: float32 [4, 3, 2048], replicated, may hold values from -3 to 3
- step_bias: float32 [32], replicated, may hold values from -4 to 0
- log_rate: float32 [32], replicated, may hold values from 0 to 2.5
- skip_gain: float32 [32], replicated, may hold values from -4 to 4
- group_gain: float32 [2048], replicated, may hold values from 0.1 to 1.9
- ssm_state: float32 [128, 32, 64, 128], P('ep', 'tp'), may hold values from -2 to 2
- conv_state: bfloat16 [128, 3, 3, 2048], P('ep', None, None, 'tp'), may hold values from -6 to 6
- out_proj: bfloat16 [2048, 2048], P('tp'), may hold values from -0.125 to 0.125
- ffn_gain: float32 [2048], replicated, may hold values from 0.1 to 1.9
- routes: int32 [128, 2], P('ep'), may hold values from 0 to 7, all different within a row; in each aligned block of 32 rows (0 to 31, 32 to 63, ...) at most 16 rows name the same one
- route_weight: float32 [128, 2], P('ep'), may hold values from 0.2 to 1
- expert_gate: bfloat16 [8, 2048, 2048], P('ep', None, 'tp'), may hold values from -0.125 to 0.125
- expert_up: bfloat16 [8, 2048, 2048], P('ep', None, 'tp'), may hold values from -0.125 to 0.125
- expert_down: bfloat16 [8, 2048, 2048], P('ep', 'tp'), may hold values from -0.125 to 0.125
- dense_gate: bfloat16 [2048, 2048], P(None, 'tp'), may hold values from -0.125 to 0.125
- dense_up: bfloat16 [2048, 2048], P(None, 'tp'), may hold values from -0.125 to 0.125
- dense_down: bfloat16 [2048, 2048], P('tp'), may hold values from -0.125 to 0.125
- blend_weight: bfloat16 [2048], replicated, may hold values from -0.125 to 0.125
Outputs:
- layer_out: bfloat16 [128, 2048], P('ep', 'tp')
- new_state: float32 [128, 32, 64, 128], P('ep', 'tp')
- new_conv: bfloat16 [128, 3, 3, 2048], P('ep', None, None, 'tp')
Inputs may be any that keep to these rules, and one draw needn't show every extreme that they name: `routes`: each row names 2 different experts. Within the 32 rows of one index of ep no expert is named by more than 16 rows, and in some such block some expert is named by exactly 16 rows.
All inputs are finite; a program needn't handle non-finite values.
Results may differ from a plain program's by a relative error of at most 0.015.
Values may be sent and summed in bfloat16 or wider, within the bound.
No kernel may reach another device: no remote copies, remote signals or barrier semaphores. Data moves between devices by JAX's collectives and lax.ppermute only.
A program may use at most 128 MiB of HBM per device.

v0:
```python
import jax
import jax.numpy as jnp
from jax import lax
from jax.sharding import PartitionSpec as P

epsilon = 1e-06


def rms_rows(values, gain_vector):
    floats_in = values.astype(jnp.float32)
    return (
        floats_in
        * lax.rsqrt(jnp.mean(floats_in * floats_in, axis=-1, keepdims=True) + epsilon)
        * gain_vector
    )


def on_device(
    residual,
    mixer_gain,
    gate_proj,
    input_proj,
    write_proj,
    read_proj,
    step_proj,
    conv_weight,
    step_bias,
    log_rate,
    skip_gain,
    group_gain,
    ssm_state,
    conv_state,
    out_proj,
    ffn_gain,
    routes,
    route_weight,
    expert_gate,
    expert_up,
    expert_down,
    dense_gate,
    dense_up,
    dense_down,
    blend_weight,
):
    seq_rows = residual.shape[0]
    col_width = gate_proj.shape[1]
    heads_here = ssm_state.shape[1]
    head_dim = ssm_state.shape[2]
    state_dim = ssm_state.shape[3]
    groups_here = col_width // state_dim
    tp_rank = lax.axis_index("tp")
    head_start = tp_rank * heads_here
    chan_start = tp_rank * col_width
    normed = rms_rows(residual, mixer_gain).astype(jnp.bfloat16)
    joined = jnp.concatenate((gate_proj, input_proj, write_proj, read_proj), axis=1)
    pieces = lax.all_to_all(normed, "ep", split_axis=1, concat_axis=0, tiled=True)
    summed = lax.psum_scatter(
        jnp.dot(pieces, joined, preferred_element_type=jnp.float32),
        "ep",
        scatter_dimension=0,
        tiled=True,
    )
    projected = summed.astype(jnp.bfloat16)
    z_proj = projected[:, :col_width]
    x_proj = projected[:, col_width : 2 * col_width]
    b_proj = projected[:, 2 * col_width : 3 * col_width]
    c_proj = projected[:, 3 * col_width :]
    step_cols = lax.dynamic_slice_in_dim(step_proj, head_start, heads_here, 1)
    step_raw = jnp.dot(normed, step_cols, preferred_element_type=jnp.float32)
    newest = jnp.stack((x_proj, b_proj, c_proj), axis=1)[:, None]
    stacked = jnp.concatenate((conv_state, newest), axis=1)
    new_conv = stacked[:, 1:]
    conv_taps = lax.dynamic_slice_in_dim(conv_weight, chan_start, col_width, 2)
    activated = jax.nn.silu(jnp.einsum("skcw,kcw->scw", stacked.astype(jnp.float32), conv_taps))
    per_group = heads_here // groups_here
    x_act = activated[:, 0].reshape(seq_rows, heads_here, head_dim)
    b_act = jnp.repeat(activated[:, 1].reshape(seq_rows, groups_here, state_dim), per_group, axis=1)
    c_act = jnp.repeat(activated[:, 2].reshape(seq_rows, groups_here, state_dim), per_group, axis=1)
    step_size = jax.nn.softplus(
        step_raw + lax.dynamic_slice_in_dim(step_bias, head_start, heads_here, 0)
    )
    decay_rate = jnp.exp(lax.dynamic_slice_in_dim(log_rate, head_start, heads_here, 0))
    decay_factor = jnp.exp(-decay_rate * step_size)
    new_state = (
        decay_factor[:, :, None, None] * ssm_state
        + (step_size[:, :, None] * x_act)[..., None] * b_act[:, :, None, :]
    )
    skip_here = lax.dynamic_slice_in_dim(skip_gain, head_start, heads_here, 0)
    ssm_out = jnp.einsum("shpn,shn->shp", new_state, c_act) + skip_here[None, :, None] * x_act
    gated_out = ssm_out.reshape(seq_rows, col_width) * jax.nn.silu(z_proj.astype(jnp.float32))
    grouped = gated_out.reshape(seq_rows, groups_here, col_width // groups_here)
    grouped = grouped * lax.rsqrt(jnp.mean(grouped * grouped, axis=-1, keepdims=True) + epsilon)
    gain_here = lax.dynamic_slice_in_dim(group_gain, chan_start, col_width, 0)
    mixed_out = (grouped.reshape(seq_rows, col_width) * gain_here).astype(jnp.bfloat16)
    mixer_total = lax.psum(jnp.dot(mixed_out, out_proj, preferred_element_type=jnp.float32), "tp")
    resid_mid = (residual.astype(jnp.float32) + mixer_total).astype(jnp.bfloat16)
    normed_ffn = rms_rows(resid_mid, ffn_gain).astype(jnp.bfloat16)
    top_count = routes.shape[1]
    experts_here = expert_gate.shape[0]
    ep_count = lax.axis_size("ep")
    model_width = normed_ffn.shape[1]
    total_experts = experts_here * ep_count
    capacity = max(2, 2 * seq_rows * top_count // total_experts)
    flat_routes = routes.reshape(-1)
    onehot = (flat_routes[:, None] == jnp.arange(total_experts, dtype=jnp.int32)[None, :]).astype(
        jnp.int32
    )
    slot_rank = jnp.sum((jnp.cumsum(onehot, axis=0) - onehot) * onehot, axis=1)
    position = flat_routes * capacity + slot_rank
    placing = (
        jnp.arange(total_experts * capacity, dtype=jnp.int32)[:, None] == position[None, :]
    ).astype(jnp.bfloat16)
    outgoing = jnp.dot(
        placing, jnp.repeat(normed_ffn, top_count, axis=0), preferred_element_type=jnp.float32
    ).astype(jnp.bfloat16)
    outgoing = outgoing.reshape(total_experts, 1, capacity, model_width)
    received = lax.all_to_all(outgoing, "ep", split_axis=0, concat_axis=1, tiled=True)
    item_count = received.shape[2]
    expert_rows = received.reshape(experts_here, ep_count * item_count, received.shape[3])
    gate_val = jnp.einsum(
        "erd,edf->erf", expert_rows, expert_gate, preferred_element_type=jnp.float32
    )
    up_val = jnp.einsum("erd,edf->erf", expert_rows, expert_up, preferred_element_type=jnp.float32)
    hidden = (jax.nn.silu(gate_val) * up_val).astype(jnp.bfloat16)
    partial_out = jnp.einsum(
        "erf,efd->erd", hidden, expert_down, preferred_element_type=jnp.float32
    )
    partial_out = partial_out.reshape(experts_here, ep_count, item_count, partial_out.shape[2])
    reduced = lax.psum_scatter(
        partial_out.astype(jnp.bfloat16), "tp", scatter_dimension=3, tiled=True
    )
    returned = lax.all_to_all(reduced, "ep", split_axis=1, concat_axis=0, tiled=True)
    back_rows = returned.reshape(total_experts * capacity, returned.shape[3])
    picked = jnp.dot(placing.T, back_rows, preferred_element_type=jnp.float32)
    expert_mix = jnp.sum(
        picked.reshape(seq_rows, top_count, back_rows.shape[1]) * route_weight[..., None], axis=1
    )
    gate_val = jnp.dot(normed_ffn, dense_gate, preferred_element_type=jnp.float32)
    up_val = jnp.dot(normed_ffn, dense_up, preferred_element_type=jnp.float32)
    dense_hidden = (jax.nn.silu(gate_val) * up_val).astype(jnp.bfloat16)
    dense_out = lax.psum_scatter(
        jnp.dot(dense_hidden, dense_down, preferred_element_type=jnp.float32).astype(jnp.bfloat16),
        "tp",
        scatter_dimension=1,
        tiled=True,
    ).astype(jnp.float32)
    mix_weight = jax.nn.sigmoid(
        jnp.dot(normed_ffn, blend_weight, preferred_element_type=jnp.float32)
    )
    slice_width = dense_out.shape[1]
    own_resid = lax.dynamic_slice_in_dim(resid_mid, tp_rank * slice_width, slice_width, 1).astype(
        jnp.float32
    )
    layer_out = (own_resid + expert_mix + mix_weight[:, None] * dense_out).astype(jnp.bfloat16)
    return (layer_out, new_state, new_conv)


def solution(mesh):
    return jax.shard_map(
        on_device,
        mesh=mesh,
        in_specs=(
            P("ep", None),
            P(),
            P("ep", "tp"),
            P("ep", "tp"),
            P("ep", "tp"),
            P("ep", "tp"),
            P(),
            P(),
            P(),
            P(),
            P(),
            P(),
            P("ep", "tp", None, None),
            P("ep", None, None, "tp"),
            P("tp", None),
            P(),
            P("ep", None),
            P("ep", None),
            P("ep", None, "tp"),
            P("ep", None, "tp"),
            P("ep", "tp", None),
            P(None, "tp"),
            P(None, "tp"),
            P("tp", None),
            P(),
        ),
        out_specs=(P("ep", "tp"), P("ep", "tp", None, None), P("ep", None, None, "tp")),
        check_vma=False,
    )
```

profile of v0, /device:TPU:0, one launch (start us, length us, event | category | flops | bytes accessed | tf_op | source)
XLA Modules:
  0.0 202.6 jit_solution(5780126422556502276)
XLA Ops:
  7.2 1.2 fusion.18
  9.4 10.0 %all_to_all.49 = bf16[32,4,512]{2,0,1:T(8,128)(2,1)S(1)} all-to-all(bf16[32,4,512]{2,0,1:T(8,128)(2,1)S(1)} %bitcast.104), channel_id=1, replica_groups=mesh['ep'=4,'tp'=8] {'ep'}, dimensions={1} | all-to-all | bytes 262144 | tf_op jit(solution)/shard_map/all_to_all | solution.py:56
  19.5 2.4 %fusion.7 = f32[128,1024]{1,0:T(8,128)} fusion(bf16[128,512]{1,0:T(8,128)(2,1)S(1)} %bitcast.109, bf16[512,256]{1,0:T(8,128)(2,1)} %param.30, bf16[512,256]{1,0:T(8,128)(2,1)} %param.29, bf16[512,256]{1,0:T(8,128)(2,1)} %param.28, bf16[512,256]{1,0:T(8,128)(2,1)} %param.27), kind=kOutput, calls=%fused_computation.16 | convolution fusion | flops 138412032 | bytes 1703936 | tf_op jit(solution)/shard_map/dot_general | solution.py:58
  22.6 1.3 dynamic_slice.26
  26.9 19.9 %reduce-scatter.4.cloned.1.call-done = f32[32,1024]{1,0:T(8,128)} async-done(((f32[128,1024]{1,0:T(8,128)}), f32[32,1024]{1,0:T(8,128)}) %reduce-scatter.4.cloned.1.call-update) | async-done | bytes 131088 | tf_op jit(solution)/shard_map/reduce_scatter | solution.py:57
  48.8 3.8 %multiply_add_fusion = f32[32,4,64,128]{3,2,1,0:T(8,128)S(1)} fusion(f32[32,4,64,128]{3,2,1,0:T(8,128)} %param.37, f32[32,4,128]{2,1,0:T(4,128)S(1)} %bitcast.106, f32[32,4,64]{2,1,0:T(4,128)S(1)} %broadcast_multiply_fusion, f32[32,4]{1,0:T(8,128)S(1)} %copy.40), kind=kLoop, calls=%fused_computation | loop fusion | flops 3145728 | bytes 8487424 | tf_op jit(solution)/shard_map/add | solution.py:85
  52.7 1.2 fusion.62
  59.2 1.6 fusion.47
  61.6 54.9 %all-reduce.2.cloned.1.call-done = f32[32,2048]{1,0:T(8,128)} async-done(((f32[32,2048]{1,0:T(8,128)}), f32[32,2048]{1,0:T(8,128)}) %all-reduce.2.cloned.1.call-update) | async-done | bytes 262160 | tf_op jit(solution)/shard_map/psum | solution.py:95
  116.5 1.1 fusion.15
  119.0 10.7 %all_to_all.50 = bf16[8,1,16,2048]{3,2,1,0:T(8,128)(2,1)S(1)} all-to-all(bf16[8,1,16,2048]{3,2,1,0:T(8,128)(2,1)S(1)} %bitcast.100), channel_id=1, replica_groups=mesh['ep'=4,'tp'=8] {'ep'}, dimensions={0} | all-to-all | bytes 1048576 | tf_op jit(solution)/shard_map/all_to_all | solution.py:117
  129.7 1.1 fusion.63
  130.9 2.5 %convolution_convert_fusion = bf16[2,64,2048]{2,1,0:T(8,128)(2,1)S(1)} fusion(bf16[2,256,2048]{2,1,0:T(8,128)(2,1)S(1)} %copy-done, bf16[2,64,2048]{2,1,0:T(8,128)(2,1)S(1)} %bitcast.99, bf16[2,2048,256]{2,1,0:T(8,128)(2,1)} %param.44, f32[2,64,256]{2,1,0:T(8,128)} %fusion.63), kind=kOutput, calls=%fused_computation.1 | convolution fusion | flops 268894208 | bytes 5373952 | tf_op jit(solution)/shard_map/erf,efd->erd/dot_general | solution.py:125
  134.3 1.4 reshape.125
  135.6 1.3 iota_compare_fusion.3
  137.0 1.3 eq.47
  138.3 1.5 fusion.23
  139.8 1.5 fusion.64
  141.3 2.6 %convolution_convert_fusion.2 = bf16[32,2048]{1,0:T(8,128)(2,1)} fusion(bf16[256,2048]{1,0:T(8,128)(2,1)S(1)} %copy-done.4, bf16[32,2048]{1,0:T(8,128)(2,1)S(1)} %fusion.17, bf16[2048,256]{1,0:T(8,128)(2,1)} %param.47, f32[32,256]{1,0:T(8,128)S(1)} %fusion.64), kind=kOutput, calls=%fused_computation.3 | convolution fusion | flops 67223552 | bytes 2392064 | tf_op jit(solution)/shard_map/dot_general | solution.py:142
  144.0 20.0 %reduce-scatter.6.cloned.1.call-done = bf16[2,4,16,256]{3,2,0,1:T(8,128)(2,1)} async-done(((bf16[2,4,16,2048]{3,2,0,1:T(8,128)(2,1)}), bf16[2,4,16,256]{3,2,0,1:T(8,128)(2,1)}) %reduce-scatter.6.cloned.1.call-update) | async-done | bytes 65552 | tf_op jit(solution)/shard_map/reduce_scatter | solution.py:129
  163.9 3.5 %all-to-all-start.2 = ((bf16[2,4,16,256]{3,2,0,1:T(8,128)(2,1)}), bf16[2,4,16,256]{3,2,0,1:T(8,128)(2,1)S(1)}, u32[]{:S(2)}, u32[]{:S(2)}) async-start(bf16[2,4,16,256]{3,2,0,1:T(8,128)(2,1)} %reduce-scatter.6.cloned.1.call-done), calls=%async_computation.4 | async-start | bytes 131072 | tf_op jit(solution)/shard_map/all_to_all | solution.py:132
  167.6 4.7 %all-to-all-done.2 = bf16[2,4,16,256]{3,2,0,1:T(8,128)(2,1)S(1)} async-done(((bf16[2,4,16,256]{3,2,0,1:T(8,128)(2,1)}), bf16[2,4,16,256]{3,2,0,1:T(8,128)(2,1)S(1)}, u32[]{:S(2)}, u32[]{:S(2)}) %all-to-all-start.2) | async-done | bytes 65568 | tf_op jit(solution)/shard_map/all_to_all | solution.py:132
  172.4 22.2 %reduce-scatter.8.cloned.1.call-done = bf16[32,256]{1,0:T(8,128)(2,1)} async-done(((bf16[32,2048]{1,0:T(8,128)(2,1)}), bf16[32,256]{1,0:T(8,128)(2,1)}) %reduce-scatter.8.cloned.1.call-update) | async-done | bytes 16400 | tf_op jit(solution)/shard_map/reduce_scatter | solution.py:141
  194.6 1.4 add_convert_fusion
  (89 shorter events, 15.3 us)
Async XLA Ops:
  7.2 123.7 %copy-start = (bf16[2,256,2048]{2,1,0:T(8,128)(2,1)S(1)}, bf16[2,256,2048]{2,1,0:T(8,128)(2,1)}, u32[]{:S(2)}) copy-start(bf16[2,256,2048]{2,1,0:T(8,128)(2,1)} %param.45) | copy-start | bytes 6291460
  7.2 39.7 %reduce-scatter.4.cloned.1.call-start = ((), (), s32[]{:S(2)}) async-start(), calls=%async_computation.6 | async-start | bytes 655360 | tf_op jit(solution)/shard_map/reduce_scatter | solution.py:57
  19.5 2.5 %copy-start.15 = (f32[32]{0:T(128)S(1)}, f32[32]{0:T(128)}, u32[]{:S(2)}) copy-start(f32[32]{0:T(128)} %param.33) | copy-start | bytes 388
  19.5 2.6 %copy-start.16 = (f32[32]{0:T(128)S(1)}, f32[32]{0:T(128)}, u32[]{:S(2)}) copy-start(f32[32]{0:T(128)} %param.35) | copy-start | bytes 388
  19.5 5.2 %copy-start.12 = (s32[32,2]{0,1:T(2,128)S(1)}, s32[32,2]{0,1:T(2,128)}, u32[]{:S(2)}) copy-start(s32[32,2]{0,1:T(2,128)} %param.41) | copy-start | bytes 772
  19.5 5.6 %copy-start.17 = (f32[32]{0:T(128)S(1)}, f32[32]{0:T(128)}, u32[]{:S(2)}) copy-start(f32[32]{0:T(128)} %param.34) | copy-start | bytes 388
  19.5 29.0 %copy-start.6 = (bf16[32,3,3,256]{3,0,2,1:T(8,128)(2,1)S(1)}, bf16[32,3,3,256]{3,0,2,1:T(8,128)(2,1)}, u32[]{:S(2)}) copy-start(bf16[32,3,3,256]{3,0,2,1:T(8,128)(2,1)} %param.38) | copy-start | bytes 442372
  21.9 94.6 %all-reduce.2.cloned.1.call-start = ((), (), s32[]{:S(2)}) async-start(), calls=%async_computation.7 | async-start | bytes 524288 | tf_op jit(solution)/shard_map/psum | solution.py:95
  24.9 22.0 %copy-start.10 = (s32[64]{0:T(128)}, s32[64]{0:T(128)S(1)}, u32[]{:S(2)}) copy-start(s32[64]{0:T(128)S(1)} %reshape.115) | copy-start | bytes 772
  47.8 0.6 copy-start.7
  52.6 2.0 copy-start.1
  52.6 2.0 copy-start.13
  52.7 6.6 %copy-start.5 = (bf16[256,2048]{1,0:T(8,128)(2,1)S(1)}, bf16[256,2048]{1,0:T(8,128)(2,1)}, u32[]{:S(2)}) copy-start(bf16[256,2048]{1,0:T(8,128)(2,1)} %param.39) | copy-start | bytes 3145732
  54.6 61.9 %copy-start.3 = (bf16[32,2048]{1,0:T(8,128)(2,1)S(1)}, bf16[32,2048]{1,0:T(8,128)(2,1)}, u32[]{:S(2)}) copy-start(bf16[32,2048]{1,0:T(8,128)(2,1)} %param.25) | copy-start | bytes 393220
  60.9 103.0 %reduce-scatter.6.cloned.1.call-start = ((), (), s32[]{:S(2)}) async-start(), calls=%async_computation.8 | async-start | bytes 589824 | tf_op jit(solution)/shard_map/reduce_scatter | solution.py:129
  61.6 68.2 %copy-start.11 = (s32[64]{0:T(128)}, s32[64]{0:T(128)S(1)}, u32[]{:S(2)}) copy-start(s32[64]{0:T(128)S(1)} %multiply_add_fusion.2) | copy-start | bytes 772
  118.7 11.1 %copy-start.2 = (bf16[2,2048,256]{2,1,0:T(8,128)(2,1)S(1)}, bf16[2,2048,256]{2,1,0:T(8,128)(2,1)}, u32[]{:S(2)}) copy-start(bf16[2,2048,256]{2,1,0:T(8,128)(2,1)} %param.43) | copy-start | bytes 6291460
  134.2 7.1 %copy-start.4 = (bf16[256,2048]{1,0:T(8,128)(2,1)S(1)}, bf16[256,2048]{1,0:T(8,128)(2,1)}, u32[]{:S(2)}) copy-start(bf16[256,2048]{1,0:T(8,128)(2,1)} %param.48) | copy-start | bytes 3145732
  134.2 60.4 %reduce-scatter.8.cloned.1.call-start = ((), (), s32[]{:S(2)}) async-start(), calls=%async_computation.9 | async-start | bytes 147456 | tf_op jit(solution)/shard_map/reduce_scatter | solution.py:141
  139.8 27.7 %copy-start.9 = (bf16[2048,1]{0,1:T(2,128)(2,1)S(1)}, bf16[2048,1]{0,1:T(2,128)(2,1)}, u32[]{:S(2)}) copy-start(bf16[2048,1]{0,1:T(2,128)(2,1)} %reshape.125) | copy-start | bytes 12292
  139.8 32.5 %copy-start.8 = (pred[32,2,128]{2,1,0:T(4,128)(4,1)S(1)}, pred[32,2,128]{2,1,0:T(4,128)(4,1)}, u32[]{:S(2)}) copy-start(pred[32,2,128]{2,1,0:T(4,128)(4,1)} %eq.47) | copy-start | bytes 24580
  139.8 32.5 %copy-start.14 = (f32[32,2]{0,1:T(2,128)S(1)}, f32[32,2]{0,1:T(2,128)}, u32[]{:S(2)}) copy-start(f32[32,2]{0,1:T(2,128)} %param.42) | copy-start | bytes 772
  163.9 8.4 %all-to-all-start.2 = ((bf16[2,4,16,256]{3,2,0,1:T(8,128)(2,1)}), bf16[2,4,16,256]{3,2,0,1:T(8,128)(2,1)S(1)}, u32[]{:S(2)}, u32[]{:S(2)}) async-start(bf16[2,4,16,256]{3,2,0,1:T(8,128)(2,1)} %reduce-scatter.6.cloned.1.call-done), calls=%async_computation.4 | async-start | bytes 131072 | tf_op jit(solution)/shard_map/all_to_all | solution.py:132
Sparse Core Ops, SparseCore 0:
  22.0 24.8 reduce-scatter.3
  61.0 55.4 all-reduce.1
  134.3 29.5 reduce-scatter.5
  166.0 28.5 reduce-scatter.7
where the time goes:
time: 204 us; the launch traced here: 203 us
  waiting for transfers between devices  122 us (60%)
  blocking collectives  20.7 us (10%)
  other arithmetic  17.5 us (9%)
  matrix products  14.4 us (7%)
  between operations  14.1 us (7%)
  local copies, waits for them, and re-layouts  10.4 us (5%)
  starting transfers between devices  3.7 us (2%)
    psum x1, waiting for transfers between devices, on_device(): lax.psum(jnp.dot(mixed_out, out_proj, preferred_element_type=jnp.float32)...  54.9 us
    reduce_scatter x1, waiting for transfers between devices, on_device(): lax.psum_scatter(jnp.dot(dense_hidden, dense_down, preferred_element_type...  22.2 us
    reduce_scatter x1, waiting for transfers between devices, on_device(): lax.psum_scatter(partial_out.astype(jnp.bfloat16), 'tp', scatter_dimensio...  20 us
    reduce_scatter x1, waiting for transfers between devices, on_device(): lax.psum_scatter(jnp.dot(pieces, joined, preferred_element_type=jnp.float...  19.9 us
    all_to_all x1, blocking collectives, on_device(): lax.all_to_all(outgoing, 'ep', split_axis=0, concat_axis=1, tiled=True)  10.7 us
    all_to_all x1, blocking collectives, on_device(): lax.all_to_all(normed, 'ep', split_axis=1, concat_axis=0, tiled=True)  10 us
    all_to_all x1, waiting for transfers between devices, on_device(): lax.all_to_all(reduced, 'ep', split_axis=1, concat_axis=0, tiled=True)  4.7 us
  transfers between devices with their start and end apart: 5, of which 5 were waited for; matrix products, arithmetic and copies ran while one was open for 8% of the time, Pallas kernels for 0%

commit v1 on v0

v1 whole, which is shorter than its diff:
```python
import jax
import jax.numpy as jnp
from jax import lax
from jax.experimental import pallas as pl
from jax.experimental.pallas import tpu as pltpu
from jax.sharding import PartitionSpec as P

epsilon = 1e-06
CORES = 2
LANES = 128
F32 = jnp.float32
BF16 = jnp.bfloat16
EXACT = lax.Precision.HIGHEST


def partner(count, index, step):
    return index ^ step if count & (count - 1) == 0 else (index + step) % count


def send_ep(block, count, step, back=False):
    pairs = [(i, partner(count, i, step)) for i in range(count)]
    return lax.ppermute(block, "ep", [(b, a) for a, b in pairs] if back else pairs)


def send_z(block, count, step):
    pairs = [
        (z * CORES + c, partner(count, z, step) * CORES + c)
        for z in range(count)
        for c in range(CORES)
    ]
    return lax.ppermute(block, "tp", pairs)


def send_core(block, count):
    return lax.ppermute(block, "tp", [(i, i ^ 1) for i in range(count)])


def local_kernel(body, name, outs, operands, flops=0, scratch=()):
    whole = pl.BlockSpec(memory_space=pltpu.VMEM)
    return pl.pallas_call(
        body,
        name=name,
        out_shape=outs,
        in_specs=[whole] * len(operands),
        out_specs=jax.tree.map(lambda _: whole, outs),
        scratch_shapes=scratch,
        cost_estimate=pl.CostEstimate(flops=flops, bytes_accessed=0, transcendentals=0),
        compiler_params=pltpu.CompilerParams(vmem_limit_bytes=40 << 20),
    )(*operands)


def row_scale(values):
    return lax.rsqrt(jnp.mean(values * values, axis=-1, keepdims=True) + epsilon)


def halves(array, core, width):
    count = array.shape[1] // width
    even = jnp.concatenate([array[:, i * width : (i + 1) * width] for i in range(0, count, 2)], 1)
    odd = jnp.concatenate([array[:, i * width : (i + 1) * width] for i in range(1, count, 2)], 1)
    first = core == 0
    return jnp.where(first, even, odd), jnp.where(first, odd, even)


def interleave(mine, other, core, width):
    first = core == 0
    even, odd = jnp.where(first, mine, other), jnp.where(first, other, mine)
    parts = []
    for i in range(mine.shape[1] // width):
        parts += [even[:, i * width : (i + 1) * width], odd[:, i * width : (i + 1) * width]]
    return jnp.concatenate(parts, 1)


def pack_tokens(ep_count, expert_total, residual, mixer_gain, routes, route_weight):
    rows, model = residual.shape
    depth = model // ep_count
    side = -(-2 * expert_total // LANES) * LANES

    def body(res_ref, gain_ref, routes_ref, weight_ref, *outs):
        rank = lax.axis_index("ep")
        lane = lax.broadcasted_iota(jnp.int32, (rows, side), 1)
        named = jnp.where(lane < expert_total, lane, lane - expert_total)
        dense = jnp.zeros((rows, side), F32)
        for k in range(routes.shape[1]):
            dense = dense + jnp.where(
                routes_ref[:, k : k + 1] == named, weight_ref[:, k : k + 1], 0.0
            )
        high = dense.astype(BF16).astype(F32)
        dense = jnp.where(lane < expert_total, high, dense - high).astype(BF16)
        for step, out in enumerate(outs):
            start = pl.multiple_of(partner(ep_count, rank, step) * depth, LANES)
            cols = res_ref[:, pl.ds(start, depth)].astype(F32) * gain_ref[:, pl.ds(start, depth)]
            out[:, :depth] = cols.astype(BF16)
            out[:, depth:] = dense

    outs = [jax.ShapeDtypeStruct((rows, depth + side), BF16)] * ep_count
    return local_kernel(body, "pack_tokens", outs, (residual, mixer_gain, routes, route_weight))


def project(blocks, weights):
    rows = blocks[0].shape[0]
    depth, width = weights[0].shape
    count, kinds = len(blocks), len(weights)

    def body(*refs):
        ins, mats, outs = refs[:count], refs[count : count + kinds], refs[count + kinds :]
        stacked = jnp.concatenate([r[:, :depth] for r in ins], 0)
        for j, mat in enumerate(mats):
            result = jnp.dot(stacked, mat[...], preferred_element_type=F32)
            for i, out in enumerate(outs):
                piece = result[i * rows : (i + 1) * rows]
                out[:, j * width : (j + 1) * width] = piece.astype(out.dtype)

    outs = [jax.ShapeDtypeStruct((rows, kinds * width), BF16 if i else F32) for i in range(count)]
    flops = 2 * rows * count * depth * kinds * width
    return local_kernel(body, "project", outs, (*blocks, *weights), flops)


def head_terms(residual, mixer_gain, step_proj, step_bias, log_rate, skip_gain, heads, width):
    rows, model = residual.shape
    total = step_proj.shape[1]
    state = LANES

    def body(res_ref, gain_ref, proj_ref, bias_ref, rate_ref, skip_ref, scale, step, decay, skip, half):
        rank = lax.axis_index("tp")
        head_start = rank * heads
        values = res_ref[...].astype(F32)
        scaling = row_scale(values)
        normed = (values * scaling * gain_ref[...]).astype(BF16)
        raw = jnp.dot(normed, proj_ref[...], preferred_element_type=F32) + bias_ref[...]
        size = jnp.maximum(raw, 0.0) + jnp.log1p(jnp.exp(-jnp.abs(raw)))
        fade = jnp.exp(-jnp.exp(rate_ref[...]) * size)

        def spread(table, lanes):
            head = lax.broadcasted_iota(jnp.int32, (total, heads * lanes), 0) - head_start
            lane = lax.broadcasted_iota(jnp.int32, (total, heads * lanes), 1)
            hot = ((lane >= head * lanes) & (lane < (head + 1) * lanes)).astype(F32)
            return jnp.dot(table, hot, preferred_element_type=F32, precision=EXACT)

        scale[...] = jnp.broadcast_to(scaling, (rows, LANES))
        step[...] = spread(size, width // heads)
        decay[...] = spread(fade, state)
        skip[...] = spread(jnp.broadcast_to(skip_ref[...], (8, total)), width // heads)
        half[...] = halves(values, rank % CORES, width)[0].astype(BF16)

    outs = [
        jax.ShapeDtypeStruct((rows, LANES), F32),
        jax.ShapeDtypeStruct((rows, width), F32),
        jax.ShapeDtypeStruct((rows, heads * state), F32),
        jax.ShapeDtypeStruct((8, width), F32),
        jax.ShapeDtypeStruct((rows, model // CORES), BF16),
    ]
    operands = (residual, mixer_gain, step_proj, step_bias, log_rate, skip_gain)
    return local_kernel(body, "head_terms", outs, operands, 2 * rows * model * total)


def silu(values):
    return values * jax.nn.sigmoid(values)


def mix(partials, scale, step, decay, skip, conv_old, conv_last, ssm_state, group_gain, out_proj):
    rows, heads, head_dim, state = ssm_state.shape
    width = heads * head_dim
    model = out_proj.shape[1]
    groups = width // state
    count = len(partials)

    def body(*refs):
        parts = refs[:count]
        (scale_ref, step_ref, decay_ref, skip_ref, old_ref, last_ref, state_ref, gain_ref, out_ref) = refs[
            count : count + 9
        ]
        proj_out, fed_out, write_out, mine_out, other_out, read_buf, sum_buf = refs[count + 9 :]
        rank = lax.axis_index("tp")
        summed = parts[0][...].astype(F32)
        for part in parts[1:]:
            summed = summed + part[...].astype(F32)
        projected = (summed * scale_ref[:, :1]).astype(BF16)
        proj_out[...] = projected
        fresh = projected.astype(F32)
        act = [
            silu(old_ref[j] + fresh[:, (j + 1) * width : (j + 2) * width] * last_ref[j : j + 1, :])
            for j in range(3)
        ]
        x_act, b_act, c_act = act
        fed = step_ref[...] * x_act
        fed_out[...] = fed
        write_out[...] = b_act
        c_low = c_act.astype(BF16)
        read_buf[...] = c_low.astype(F32)
        lane = lax.broadcasted_iota(jnp.int32, (1, width), 1)
        for s in range(rows):
            block = state_ref[s].reshape(width, state).astype(BF16)
            reads = [read_buf[s : s + 1, g * state : (g + 1) * state] for g in range(groups)]
            reads = jnp.concatenate(reads + [jnp.zeros((8 - groups, state), F32)], 0).astype(BF16)
            found = lax.dot_general(
                reads, block, (((1,), (1,)), ((), ())), preferred_element_type=F32
            )
            row = found[0:1]
            for g in range(1, groups):
                row = jnp.where(lane >= g * state, found[g : g + 1], row)
            sum_buf[s : s + 1, :] = row
        old_part = sum_buf[...]
        decay_ch = jnp.concatenate(
            [decay_ref[:, h * state : h * state + head_dim] for h in range(heads)], 1
        )
        both = []
        for g in range(groups):
            cols = slice(g * state, (g + 1) * state)
            inner = jnp.sum(b_act[:, cols] * c_act[:, cols], axis=-1, keepdims=True)
            both.append(fed[:, cols] * inner)
        ssm_out = decay_ch * old_part + jnp.concatenate(both, 1) + skip_ref[0:1] * x_act
        gated = ssm_out * silu(fresh[:, :width])
        start = pl.multiple_of(rank * width, LANES)
        gain = gain_ref[:, pl.ds(start, width)]
        mixed = []
        for g in range(groups):
            cols = slice(g * state, (g + 1) * state)
            mixed.append(gated[:, cols] * row_scale(gated[:, cols]) * gain[:, cols])
        mixed = jnp.concatenate(mixed, 1).astype(BF16)
        result = jnp.dot(mixed, out_ref[...], preferred_element_type=F32)
        mine, other = halves(result, rank % CORES, width)
        mine_out[...] = mine
        other_out[...] = other.astype(BF16)

    outs = [
        jax.ShapeDtypeStruct((rows, partials[0].shape[1]), BF16),
        jax.ShapeDtypeStruct((rows, width), F32),
        jax.ShapeDtypeStruct((rows, width), F32),
        jax.ShapeDtypeStruct((rows, model // CORES), F32),
        jax.ShapeDtypeStruct((rows, model // CORES), BF16),
    ]
    operands = (
        *partials, scale, step, decay, skip, conv_old, conv_last, ssm_state, group_gain, out_proj,
    )
    scratch = [pltpu.VMEM((rows, width), F32), pltpu.VMEM((rows, width), F32)]
    return local_kernel(body, "mix", outs, operands, 2 * rows * width * model, scratch)


def advance_state(ssm_state, decay, fed, written):
    rows, heads, head_dim, state = ssm_state.shape
    width = heads * head_dim
    groups = width // state
    per_group = heads // groups
    chunk = 8

    def body(state_ref, decay_ref, fed_ref, write_ref, out_ref):
        fed_cols = fed_ref[...].T
        for s in range(chunk):
            for h in range(heads):
                g = h // per_group
                fade = decay_ref[s : s + 1, h * state : (h + 1) * state]
                write = write_ref[s : s + 1, g * state : (g + 1) * state]
                column = fed_cols[h * head_dim : (h + 1) * head_dim, s : s + 1]
                out_ref[s, h] = fade * state_ref[s, h] + column * write

    block = pl.BlockSpec((chunk, heads, head_dim, state), lambda i: (i, 0, 0, 0))
    return pl.pallas_call(
        body,
        name="advance_state",
        grid=(rows // chunk,),
        out_shape=jax.ShapeDtypeStruct(ssm_state.shape, F32),
        in_specs=[
            block,
            pl.BlockSpec((chunk, heads * state), lambda i: (i, 0)),
            pl.BlockSpec((chunk, width), lambda i: (i, 0)),
            pl.BlockSpec((chunk, width), lambda i: (i, 0)),
        ],
        out_specs=block,
        cost_estimate=pl.CostEstimate(
            flops=8 << 20, bytes_accessed=2 * ssm_state.size * 4, transcendentals=0
        ),
    )(ssm_state, decay, fed, written)


def dense_branch(mine, other, ffn_gain, gate, up, down, blend):
    rows, half = mine.shape
    model = half * CORES
    width = model // lax.axis_size("tp")

    def body(mine_ref, other_ref, gain_ref, gate_ref, up_ref, down_ref, blend_ref, mine_out, other_out):
        core = lax.axis_index("tp") % CORES
        values = interleave(mine_ref[...].astype(F32), other_ref[...].astype(F32), core, width)
        normed = (values * row_scale(values) * gain_ref[...]).astype(BF16)
        gated = jnp.dot(normed, gate_ref[...], preferred_element_type=F32)
        raised = jnp.dot(normed, up_ref[...], preferred_element_type=F32)
        hidden = (silu(gated) * raised).astype(BF16)
        weight = jax.nn.sigmoid(
            jnp.sum(normed.astype(F32) * blend_ref[...].astype(F32), axis=-1, keepdims=True)
        )
        result = jnp.dot(hidden, down_ref[...], preferred_element_type=F32) * weight
        kept, sent = halves(result, core, width)
        mine_out[...] = kept
        other_out[...] = sent

    outs = [jax.ShapeDtypeStruct((rows, half), F32)] * 2
    operands = (mine, other, ffn_gain, gate, up, down, blend)
    return local_kernel(body, "dense_branch", outs, operands, 6 * rows * model * gate.shape[1])


def run_experts(tokens, ffn_gain, gate, up, down, dense_mine, dense_other, packed, depth):
    own, rest, own_other, rest_other = tokens
    rows, half = own.shape
    every = rows + rest.shape[0]
    model = half * CORES
    width = model // lax.axis_size("tp")
    experts = gate.shape[0]
    total = experts * lax.axis_size("ep")
    count = len(packed)

    def body(own_ref, rest_ref, own2_ref, rest2_ref, gain_ref, gate_ref, up_ref, down_ref, dm, do, *more):
        packed_refs, (mine_out, other_out) = more[:count], more[count:]
        core = lax.axis_index("tp") % CORES
        first = lax.axis_index("ep") * experts
        mine = jnp.concatenate([own_ref[...].astype(F32), rest_ref[...].astype(F32)], 0)
        other = jnp.concatenate([own2_ref[...].astype(F32), rest2_ref[...].astype(F32)], 0)
        values = interleave(mine, other, core, width)
        normed = (values * row_scale(values) * gain_ref[...]).astype(BF16)
        weights = jnp.concatenate([r[:, depth:].astype(F32) for r in packed_refs], 0)
        lane = lax.broadcasted_iota(jnp.int32, weights.shape, 1)
        result = None
        for j in range(experts):
            gated = jnp.dot(normed, gate_ref[j], preferred_element_type=F32)
            raised = jnp.dot(normed, up_ref[j], preferred_element_type=F32)
            picked = (lane == first + j) | (lane == first + j + total)
            share = jnp.sum(jnp.where(picked, weights, 0.0), axis=-1, keepdims=True)
            hidden = (silu(gated) * raised * share).astype(BF16)
            part = jnp.dot(hidden, down_ref[j], preferred_element_type=F32)
            result = part if result is None else result + part
        kept, sent = halves(result, core, width)
        mine_out[:rows] = kept[:rows] + dm[...]
        mine_out[rows:] = kept[rows:]
        other_out[:rows] = (sent[:rows] + do[...]).astype(BF16)
        other_out[rows:] = sent[rows:].astype(BF16)

    outs = [jax.ShapeDtypeStruct((every, half), F32), jax.ShapeDtypeStruct((every, half), BF16)]
    operands = (*tokens, ffn_gain, gate, up, down, dense_mine, dense_other, *packed)
    flops = 6 * every * model * gate.shape[2] * experts
    return local_kernel(body, "run_experts", outs, operands, flops)


def on_device(
    residual,
    mixer_gain,
    gate_proj,
    input_proj,
    write_proj,
    read_proj,
    step_proj,
    conv_weight,
    step_bias,
    log_rate,
    skip_gain,
    group_gain,
    ssm_state,
    conv_state,
    out_proj,
    ffn_gain,
    routes,
    route_weight,
    expert_gate,
    expert_up,
    expert_down,
    dense_gate,
    dense_up,
    dense_down,
    blend_weight,
):
    rows = residual.shape[0]
    depth, width = gate_proj.shape
    heads = ssm_state.shape[1]
    ep_count, tp_count = lax.axis_size("ep"), lax.axis_size("tp")
    z_count = tp_count // CORES
    tp_rank = lax.axis_index("tp")
    z_rank = tp_rank // CORES
    ep_steps, z_steps = range(1, ep_count), range(1, z_count)
    expert_total = expert_gate.shape[0] * ep_count
    as_row = lambda vector: vector.reshape(1, -1)

    packed = pack_tokens(ep_count, expert_total, residual, as_row(mixer_gain), routes, route_weight)
    blocks = [packed[0]] + [send_ep(packed[k], ep_count, k) for k in ep_steps]
    partials = project(blocks, (gate_proj, input_proj, write_proj, read_proj))
    parts = [partials[0]] + [send_ep(partials[k], ep_count, k, back=True) for k in ep_steps]

    scale, step, decay, skip, resid_half = head_terms(
        residual, as_row(mixer_gain), step_proj, as_row(step_bias), as_row(log_rate),
        as_row(skip_gain), heads, width,
    )
    taps = lax.dynamic_slice_in_dim(conv_weight, tp_rank * width, width, 2)
    conv_old = jnp.sum(
        conv_state.astype(F32) * taps[None, :-1], axis=1
    ).transpose(1, 0, 2)

    projected, fed, written, mine, other = mix(
        parts, scale, step, decay, skip, conv_old, taps[-1], ssm_state, as_row(group_gain), out_proj
    )
    newest = projected[:, width:].reshape(rows, 1, 3, width)
    new_conv = jnp.concatenate((conv_state[:, 1:], newest), axis=1)

    mine = mine + send_core(other, tp_count).astype(F32)
    shared = mine.astype(BF16)
    for k in z_steps:
        mine = mine + send_z(shared, z_count, k).astype(F32)
    resid_mid = (resid_half.astype(F32) + mine).astype(BF16)
    new_state = advance_state(ssm_state, decay, fed, written)

    others = [send_ep(resid_mid, ep_count, k) for k in ep_steps]
    rest = jnp.concatenate(others, 0)
    own_other = send_core(resid_mid, tp_count)
    dense_mine, dense_other = dense_branch(
        resid_mid, own_other, as_row(ffn_gain), dense_gate, dense_up, dense_down, as_row(blend_weight)
    )
    rest_other = send_core(rest, tp_count)
    mine, other = run_experts(
        (resid_mid, rest, own_other, rest_other), as_row(ffn_gain), expert_gate, expert_up,
        expert_down, dense_mine, dense_other, blocks, depth,
    )
    mine = mine + send_core(other, tp_count).astype(F32)
    total = mine[:rows]
    low = mine.astype(BF16)
    for k in ep_steps:
        total = total + send_ep(low[k * rows : (k + 1) * rows], ep_count, k, back=True).astype(F32)
    piece = lambda array, z: lax.dynamic_slice_in_dim(array, z * width, width, 1)
    low = total.astype(BF16)
    result = piece(total, z_rank) + piece(resid_mid, z_rank).astype(F32)
    for k in z_steps:
        result = result + send_z(piece(low, partner(z_count, z_rank, k)), z_count, k).astype(F32)
    return result.astype(BF16), new_state, new_conv


def solution(mesh):
    return jax.shard_map(
        on_device,
        mesh=mesh,
        in_specs=(
            P("ep", None),
            P(),
            P("ep", "tp"),
            P("ep", "tp"),
            P("ep", "tp"),
            P("ep", "tp"),
            P(),
            P(),
            P(),
            P(),
            P(),
            P(),
            P("ep", "tp", None, None),
            P("ep", None, None, "tp"),
            P("tp", None),
            P(),
            P("ep", None),
            P("ep", None),
            P("ep", None, "tp"),
            P("ep", None, "tp"),
            P("ep", "tp", None),
            P(None, "tp"),
            P(None, "tp"),
            P("tp", None),
            P(),
        ),
        out_specs=(P("ep", "tp"), P("ep", "tp", None, None), P("ep", None, None, "tp")),
        check_vma=False,
    )
```

time: 204 us -> 72.2 us (0.35)
  waiting for transfers between devices: 122 us -> 19.8 us
  blocking collectives: 20.7 us -> 0 us
  starting transfers between devices: 3.7 us -> 24.2 us
  other arithmetic: 17.5 us -> 2.43 us
  matrix products: 14.4 us -> 0 us
  between operations: 14.1 us -> 0.98 us
  Pallas kernels: 0 us -> 10 us
  local copies, waits for them, and re-layouts: 10.4 us -> 14.2 us
    reduce_scatter x3 -> x0, waiting for transfers between devices: 62.1 us -> none  [the longest x1 22.2 us: on_device(): lax.psum_scatter(jnp.dot(dense_hidden, dense_down, preferred_element_type...]
    psum x1 -> x0, waiting for transfers between devices: 54.9 us -> none  [on_device(): lax.psum(jnp.dot(mixed_out, out_proj, preferred_element_type=jnp.float32)...]
    ppermute x0 -> x22, starting transfers between devices: none -> 24.2 us  [the longest x12 15.2 us: send_ep(): lax.ppermute(block, 'ep', [(b, a) for a, b in pairs] if back else pairs)]
    all_to_all x2 -> x0, blocking collectives: 20.7 us -> none  [the longest x1 10.7 us: on_device(): lax.all_to_all(outgoing, 'ep', split_axis=0, concat_axis=1, tiled=True)]
    ppermute x0 -> x22, waiting for transfers between devices: none -> 19.8 us  [the longest x12 11.2 us: send_ep(): lax.ppermute(block, 'ep', [(b, a) for a, b in pairs] if back else pairs)]
    dot_general x11 -> x0, matrix products: 14.4 us -> none  [the longest x1 2.61 us: on_device(): jnp.dot(dense_hidden, dense_down, preferred_element_type=jnp.float32)]
    unnamed x40 -> x59, local copies, waits for them, and re-layouts: 3.64 us -> 14 us
    pallas_call x0 -> x7, Pallas kernels: none -> 10 us  [the longest x1 5.8 us: advance_state(): pl.pallas_call(body, name='advance_state', grid=(rows // chunk,), out_sha...]
  transfers between devices with their start and end apart: 5 -> 22, of which waited for: 5 -> 12; matrix products, arithmetic and copies ran while one was open for 8% -> 4% of each run, Pallas kernels for 0% -> 10%
where the time goes in v1:
time: 72.2 us; the launch traced here: 71.6 us
  starting transfers between devices  24.2 us (34%)
  waiting for transfers between devices  19.8 us (27%)
  local copies, waits for them, and re-layouts  14.2 us (20%)
  Pallas kernels  10 us (14%)
  other arithmetic  2.43 us (3%)
  between operations  0.98 us (1%)
    ppermute x12, starting transfers between devices, send_ep(): lax.ppermute(block, 'ep', [(b, a) for a, b in pairs] if back else pairs)  15.2 us
    unnamed x59, local copies, waits for them, and re-layouts  14 us
    ppermute x12, waiting for transfers between devices, send_ep(): lax.ppermute(block, 'ep', [(b, a) for a, b in pairs] if back else pairs)  11.2 us
    ppermute x6, starting transfers between devices, send_z(): return lax.ppermute(block, 'tp', pairs)  8.01 us
    pallas_call x1, Pallas kernels, advance_state(): pl.pallas_call(body, name='advance_state', grid=(rows // chunk,), out_sha...  5.8 us
    ppermute x6, waiting for transfers between devices, send_z(): return lax.ppermute(block, 'tp', pairs)  5.11 us
    pallas_call x6, Pallas kernels, local_kernel(): pl.pallas_call(body, name=name, out_shape=outs, in_specs=[whole] * len(op...  4.22 us
    ppermute x4, waiting for transfers between devices, send_core(): return lax.ppermute(block, 'tp', [(i, i ^ 1) for i in range(count)])  3.56 us
  transfers between devices with their start and end apart: 22, of which 12 were waited for; matrix products, arithmetic and copies ran while one was open for 4% of the time, Pallas kernels for 10%

profile of v1, /device:TPU:0, one launch (start us, length us, event | category | flops | bytes accessed | tf_op | source)
XLA Modules:
  0.0 71.6 jit_solution(8528419690622208183)
XLA Ops:
  4.0 3.0 %collective-permute-start = (bf16[32,640]{1,0:T(8,128)(2,1)S(1)}, bf16[32,640]{1,0:T(8,128)(2,1)S(1)}, u32[]{:S(2)}, u32[]{:S(2)}) collective-permute-start(bf16[32,640]{1,0:T(8,128)(2,1)S(1)} %get-tuple-element.27), channel_id=1, source_target_pairs={{0,8},{8,0},{16,24},{24,16},{1,9},{9,1},{17,25},{25,17},{2,10},{10... | collective-permute-start | bytes 122888 | tf_op jit(solution)/shard_map/ppermute | solution.py:22
  7.0 1.5 %collective-permute-start.1 = (bf16[32,640]{1,0:T(8,128)(2,1)S(1)}, bf16[32,640]{1,0:T(8,128)(2,1)S(1)}, u32[]{:S(2)}, u32[]{:S(2)}) collective-permute-start(bf16[32,640]{1,0:T(8,128)(2,1)S(1)} %get-tuple-element.28), channel_id=1, source_target_pairs={{0,16},{8,24},{16,0},{24,8},{1,17},{9,25},{17,1},{25,9},{2,18},{10... | collective-permute-start | bytes 122888 | tf_op jit(solution)/shard_map/ppermute | solution.py:22
  8.6 1.2 %copy.33.proj_ref = bf16[2048,32]{1,0:T(8,128)(2,1)S(1)} copy(bf16[2048,32]{0,1:T(8,128)(2,1)} %param.31) | data formatting | bytes 262144 | tf_op args[6]
  18.1 2.0 %collective-permute-start.3 = (bf16[32,1024]{1,0:T(8,128)(2,1)S(1)}, bf16[32,1024]{1,0:T(8,128)(2,1)S(1)}, u32[]{:S(2)}, u32[]{:S(2)}) collective-permute-start(bf16[32,1024]{1,0:T(8,128)(2,1)S(1)} %get-tuple-element.31), channel_id=1, source_target_pairs={{8,0},{0,8},{24,16},{16,24},{9,1},{1,9},{25,17},{17,25},{10,2},{2,... | collective-permute-start | bytes 196616 | tf_op jit(solution)/shard_map/ppermute | solution.py:22
  20.1 1.5 %collective-permute-start.4 = (bf16[32,1024]{1,0:T(8,128)(2,1)S(1)}, bf16[32,1024]{1,0:T(8,128)(2,1)S(1)}, u32[]{:S(2)}, u32[]{:S(2)}) collective-permute-start(bf16[32,1024]{1,0:T(8,128)(2,1)S(1)} %get-tuple-element.32), channel_id=1, source_target_pairs={{16,0},{24,8},{0,16},{8,24},{17,1},{25,9},{1,17},{9,25},{18,2},{26... | collective-permute-start | bytes 196616 | tf_op jit(solution)/shard_map/ppermute | solution.py:22
  22.7 2.4 %collective-permute-done.4.refs_2_ = bf16[32,1024]{1,0:T(8,128)(2,1)S(1)} collective-permute-done((bf16[32,1024]{1,0:T(8,128)(2,1)S(1)}, bf16[32,1024]{1,0:T(8,128)(2,1)S(1)}, u32[]{:S(2)}, u32[]{:S(2)}) %collective-permute-start.4) | collective-permute-done | bytes 65568 | tf_op jit(solution)/shard_map/ppermute | solution.py:22
  25.1 1.8 %collective-permute-done.5.refs_3_ = bf16[32,1024]{1,0:T(8,128)(2,1)S(1)} collective-permute-done((bf16[32,1024]{1,0:T(8,128)(2,1)S(1)}, bf16[32,1024]{1,0:T(8,128)(2,1)S(1)}, u32[]{:S(2)}, u32[]{:S(2)}) %collective-permute-start.5) | collective-permute-done | bytes 65568 | tf_op jit(solution)/shard_map/ppermute | solution.py:22
  26.8 2.2 %copy-done.1 = f32[32,4,64,128]{3,2,1,0:T(8,128)S(1)} copy-done((f32[32,4,64,128]{3,2,1,0:T(8,128)S(1)}, f32[32,4,64,128]{3,2,1,0:T(8,128)}, u32[]{:S(2)}) %copy-start.1) | copy-done | bytes 4194328
  29.1 1.1 %mix.1 = (bf16[32,1024]{1,0:T(8,128)(2,1)S(1)}, f32[32,256]{1,0:T(8,128)S(1)}, f32[32,256]{1,0:T(8,128)S(1)}, f32[32,1024]{1,0:T(8,128)S(1)}, bf16[32,1024]{1,0:T(8,128)(2,1)S(1)}) custom-call(f32[32,1024]{1,0:T(8,128)S(1)} %get-tuple-element.30.refs_0_, bf16[32,1024]{1,0:T(8,128)(2,1)S(1)} %collective-permute-done.3.refs_1_, ...), custom_call_target="tpu_custom_call" | custom-call | flops 33554432 | tf_op jit(solution)/shard_map/mix/pallas_call | solution.py:40
  30.2 1.2 %collective-permute-done.6 = bf16[32,1024]{1,0:T(8,128)(2,1)S(1)} collective-permute-done((bf16[32,1024]{1,0:T(8,128)(2,1)S(1)}, bf16[32,1024]{1,0:T(8,128)(2,1)S(1)}, u32[]{:S(2)}, u32[]{:S(2)}) %collective-permute-start.6) | collective-permute-done | bytes 65568 | tf_op jit(solution)/shard_map/ppermute | solution.py:35
  31.5 3.7 %collective-permute-start.9 = (bf16[32,1024]{1,0:T(8,128)(2,1)S(1)}, bf16[32,1024]{1,0:T(8,128)(2,1)S(1)}, u32[]{:S(2)}, u32[]{:S(2)}) collective-permute-start(bf16[32,1024]{1,0:T(8,128)(2,1)S(1)} %fusion.2), channel_id=1, source_target_pairs={{0,6},{1,7},{2,4},{3,5},{4,2},{5,3},{6,0},{7,1},{8,14},{9,15},{10,... | collective-permute-start | bytes 196616 | tf_op jit(solution)/shard_map/ppermute | solution.py:31
  36.0 1.8 %collective-permute-done.9 = bf16[32,1024]{1,0:T(8,128)(2,1)S(1)} collective-permute-done((bf16[32,1024]{1,0:T(8,128)(2,1)S(1)}, bf16[32,1024]{1,0:T(8,128)(2,1)S(1)}, u32[]{:S(2)}, u32[]{:S(2)}) %collective-permute-start.9) | collective-permute-done | bytes 65568 | tf_op jit(solution)/shard_map/ppermute | solution.py:31
  37.8 3.3 %collective-permute-done.8 = bf16[32,1024]{1,0:T(8,128)(2,1)S(1)} collective-permute-done((bf16[32,1024]{1,0:T(8,128)(2,1)S(1)}, bf16[32,1024]{1,0:T(8,128)(2,1)S(1)}, u32[]{:S(2)}, u32[]{:S(2)}) %collective-permute-start.8) | collective-permute-done | bytes 65568 | tf_op jit(solution)/shard_map/ppermute | solution.py:31
  41.7 1.4 %collective-permute-start.12 = (bf16[32,1024]{1,0:T(8,128)(2,1)S(1)}, bf16[32,1024]{1,0:T(8,128)(2,1)S(1)}, u32[]{:S(2)}, u32[]{:S(2)}) collective-permute-start(bf16[32,1024]{1,0:T(8,128)(2,1)S(1)} %add_convert_fusion.mine_ref.own_ref), channel_id=1, source_target_pairs={{0,24},{8,16},{16,8},{24,0},{1,25},{9,17},{17,9},{25,1},{2,26},{10... | collective-permute-start | bytes 196616 | tf_op jit(solution)/shard_map/ppermute | solution.py:22
  43.2 1.5 %collective-permute-start.11 = (bf16[32,1024]{1,0:T(8,128)(2,1)S(1)}, bf16[32,1024]{1,0:T(8,128)(2,1)S(1)}, u32[]{:S(2)}, u32[]{:S(2)}) collective-permute-start(bf16[32,1024]{1,0:T(8,128)(2,1)S(1)} %add_convert_fusion.mine_ref.own_ref), channel_id=1, source_target_pairs={{0,16},{8,24},{16,0},{24,8},{1,17},{9,25},{17,1},{25,9},{2,18},{10... | collective-permute-start | bytes 196616 | tf_op jit(solution)/shard_map/ppermute | solution.py:22
  45.6 2.0 %collective-permute-done.11 = bf16[32,1024]{1,0:T(8,128)(2,1)S(1)} collective-permute-done((bf16[32,1024]{1,0:T(8,128)(2,1)S(1)}, bf16[32,1024]{1,0:T(8,128)(2,1)S(1)}, u32[]{:S(2)}, u32[]{:S(2)}) %collective-permute-start.11) | collective-permute-done | bytes 65568 | tf_op jit(solution)/shard_map/ppermute | solution.py:22
  50.1 1.4 %run_experts.1 = (f32[128,1024]{1,0:T(8,128)S(1)}, bf16[128,1024]{1,0:T(8,128)(2,1)S(1)}) custom-call(bf16[32,1024]{1,0:T(8,128)(2,1)S(1)} %add_convert_fusion.mine_ref.own_ref, bf16[96,1024]{1,0:T(8,128)(2,1)S(1)} %constant_dynamic-update-slice_fusion.rest_ref, bf16[32,1024]{1,0:T(8,128)(2,1)S(1)} %collective-permute-done.13.other_ref.own2_ref, ...), custom_call_target="tpu_custom_call" | custom-call | flops 805306368 | tf_op jit(solution)/shard_map/run_experts/pallas_call | solution.py:40
  51.8 1.3 %collective-permute-done.15 = bf16[128,1024]{1,0:T(8,128)(2,1)S(1)} collective-permute-done((bf16[128,1024]{1,0:T(8,128)(2,1)S(1)}, bf16[128,1024]{1,0:T(8,128)(2,1)S(1)}, u32[]{:S(2)}, u32[]{:S(2)}) %collective-permute-start.15) | collective-permute-done | bytes 262176 | tf_op jit(solution)/shard_map/ppermute | solution.py:35
  53.2 1.1 %collective-permute-start.16 = (bf16[32,1024]{1,0:T(8,128)(2,1)S(1)}, bf16[32,1024]{1,0:T(8,128)(2,1)S(1)}, u32[]{:S(2)}, u32[]{:S(2)}) collective-permute-start(bf16[32,1024]{1,0:T(8,128)(2,1)S(1)} %get-tuple-element.51), channel_id=1, source_target_pairs={{8,0},{0,8},{24,16},{16,24},{9,1},{1,9},{25,17},{17,25},{10,2},{2,... | collective-permute-start | bytes 196616 | tf_op jit(solution)/shard_map/ppermute | solution.py:22
  54.4 1.7 %collective-permute-start.18 = (bf16[32,1024]{1,0:T(8,128)(2,1)S(1)}, bf16[32,1024]{1,0:T(8,128)(2,1)S(1)}, u32[]{:S(2)}, u32[]{:S(2)}) collective-permute-start(bf16[32,1024]{1,0:T(8,128)(2,1)S(1)} %get-tuple-element.52), channel_id=1, source_target_pairs={{24,0},{16,8},{8,16},{0,24},{25,1},{17,9},{9,17},{1,25},{26,2},{18... | collective-permute-start | bytes 196616 | tf_op jit(solution)/shard_map/ppermute | solution.py:22
  57.8 2.0 %collective-permute-done.18 = bf16[32,1024]{1,0:T(8,128)(2,1)S(1)} collective-permute-done((bf16[32,1024]{1,0:T(8,128)(2,1)S(1)}, bf16[32,1024]{1,0:T(8,128)(2,1)S(1)}, u32[]{:S(2)}, u32[]{:S(2)}) %collective-permute-start.18) | collective-permute-done | bytes 65568 | tf_op jit(solution)/shard_map/ppermute | solution.py:22
  61.0 1.2 %collective-permute-start.19 = (bf16[32,256]{1,0:T(8,128)(2,1)S(1)}, bf16[32,256]{1,0:T(8,128)(2,1)S(1)}, u32[]{:S(2)}, u32[]{:S(2)}) collective-permute-start(bf16[32,256]{1,0:T(8,128)(2,1)S(1)} %get-tuple-element.54), channel_id=1, source_target_pairs={{0,2},{1,3},{2,0},{3,1},{4,6},{5,7},{6,4},{7,5},{8,10},{9,11},{10,... | collective-permute-start | bytes 49160 | tf_op jit(solution)/shard_map/ppermute | solution.py:31
  62.1 1.7 %collective-permute-start.21 = (bf16[32,256]{1,0:T(8,128)(2,1)S(1)}, bf16[32,256]{1,0:T(8,128)(2,1)S(1)}, u32[]{:S(2)}, u32[]{:S(2)}) collective-permute-start(bf16[32,256]{1,0:T(8,128)(2,1)S(1)} %get-tuple-element.55), channel_id=1, source_target_pairs={{0,6},{1,7},{2,4},{3,5},{4,2},{5,3},{6,0},{7,1},{8,14},{9,15},{10,... | collective-permute-start | bytes 49160 | tf_op jit(solution)/shard_map/ppermute | solution.py:31
  65.2 5.8 %advance_state.1 = f32[32,4,64,128]{3,2,1,0:T(8,128)} custom-call(f32[32,4,64,128]{3,2,1,0:T(8,128)} %state_ref.1, f32[32,512]{1,0:T(8,128)} %copy-done.11, f32[32,256]{1,0:T(8,128)} %copy-done.16, f32[32,256]{1,0:T(8,128)} %copy-done.17), custom_call_target="tpu_custom_call" | custom-call | flops 8388608 | bytes 8388608 | tf_op jit(solution)/shard_map/advance_state/pallas_call | solution.py:257
  (104 shorter events, 22.8 us)
Async XLA Ops:
  0.6 26.2 %copy-start.5 = (bf16[256,2048]{1,0:T(8,128)(2,1)S(1)}, bf16[256,2048]{1,0:T(8,128)(2,1)}, u32[]{:S(2)}) copy-start(bf16[256,2048]{1,0:T(8,128)(2,1)} %refs_12_.1) | copy-start | bytes 3145732
  4.0 10.0 %collective-permute-start = (bf16[32,640]{1,0:T(8,128)(2,1)S(1)}, bf16[32,640]{1,0:T(8,128)(2,1)S(1)}, u32[]{:S(2)}, u32[]{:S(2)}) collective-permute-start(bf16[32,640]{1,0:T(8,128)(2,1)S(1)} %get-tuple-element.27), channel_id=1, source_target_pairs={{0,8},{8,0},{16,24},{24,16},{1,9},{9,1},{17,25},{25,17},{2,10},{10... | collective-permute-start | bytes 122888 | tf_op jit(solution)/shard_map/ppermute | solution.py:22
  7.0 7.0 %collective-permute-start.1 = (bf16[32,640]{1,0:T(8,128)(2,1)S(1)}, bf16[32,640]{1,0:T(8,128)(2,1)S(1)}, u32[]{:S(2)}, u32[]{:S(2)}) collective-permute-start(bf16[32,640]{1,0:T(8,128)(2,1)S(1)} %get-tuple-element.28), channel_id=1, source_target_pairs={{0,16},{8,24},{16,0},{24,8},{1,17},{9,25},{17,1},{25,9},{2,18},{10... | collective-permute-start | bytes 122888 | tf_op jit(solution)/shard_map/ppermute | solution.py:22
  8.5 5.5 %collective-permute-start.2 = (bf16[32,640]{1,0:T(8,128)(2,1)S(1)}, bf16[32,640]{1,0:T(8,128)(2,1)S(1)}, u32[]{:S(2)}, u32[]{:S(2)}) collective-permute-start(bf16[32,640]{1,0:T(8,128)(2,1)S(1)} %get-tuple-element.29), channel_id=1, source_target_pairs={{0,24},{8,16},{16,8},{24,0},{1,25},{9,17},{17,9},{25,1},{2,26},{10... | collective-permute-start | bytes 122888 | tf_op jit(solution)/shard_map/ppermute | solution.py:22
  18.1 4.5 %collective-permute-start.3 = (bf16[32,1024]{1,0:T(8,128)(2,1)S(1)}, bf16[32,1024]{1,0:T(8,128)(2,1)S(1)}, u32[]{:S(2)}, u32[]{:S(2)}) collective-permute-start(bf16[32,1024]{1,0:T(8,128)(2,1)S(1)} %get-tuple-element.31), channel_id=1, source_target_pairs={{8,0},{0,8},{24,16},{16,24},{9,1},{1,9},{25,17},{17,25},{10,2},{2,... | collective-permute-start | bytes 196616 | tf_op jit(solution)/shard_map/ppermute | solution.py:22
  20.1 4.9 %collective-permute-start.4 = (bf16[32,1024]{1,0:T(8,128)(2,1)S(1)}, bf16[32,1024]{1,0:T(8,128)(2,1)S(1)}, u32[]{:S(2)}, u32[]{:S(2)}) collective-permute-start(bf16[32,1024]{1,0:T(8,128)(2,1)S(1)} %get-tuple-element.32), channel_id=1, source_target_pairs={{16,0},{24,8},{0,16},{8,24},{17,1},{25,9},{1,17},{9,25},{18,2},{26... | collective-permute-start | bytes 196616 | tf_op jit(solution)/shard_map/ppermute | solution.py:22
  21.7 5.2 %collective-permute-start.5 = (bf16[32,1024]{1,0:T(8,128)(2,1)S(1)}, bf16[32,1024]{1,0:T(8,128)(2,1)S(1)}, u32[]{:S(2)}, u32[]{:S(2)}) collective-permute-start(bf16[32,1024]{1,0:T(8,128)(2,1)S(1)} %get-tuple-element.33), channel_id=1, source_target_pairs={{24,0},{16,8},{8,16},{0,24},{25,1},{17,9},{9,17},{1,25},{26,2},{18... | collective-permute-start | bytes 196616 | tf_op jit(solution)/shard_map/ppermute | solution.py:22
  29.1 21.0 %copy-start.4 = (bf16[2,256,2048]{2,1,0:T(8,128)(2,1)S(1)}, bf16[2,256,2048]{2,1,0:T(8,128)(2,1)}, u32[]{:S(2)}) copy-start(bf16[2,256,2048]{2,1,0:T(8,128)(2,1)} %down_ref.3) | copy-start | bytes 6291460
  30.2 1.3 %collective-permute-start.6 = (bf16[32,1024]{1,0:T(8,128)(2,1)S(1)}, bf16[32,1024]{1,0:T(8,128)(2,1)S(1)}, u32[]{:S(2)}, u32[]{:S(2)}) collective-permute-start(bf16[32,1024]{1,0:T(8,128)(2,1)S(1)} %get-tuple-element.39), channel_id=1, source_target_pairs={{0,1},{1,0},{2,3},{3,2},{4,5},{5,4},{6,7},{7,6},{8,9},{9,8},{10,11... | collective-permute-start | bytes 196616 | tf_op jit(solution)/shard_map/ppermute | solution.py:35
  31.5 6.3 %collective-permute-start.9 = (bf16[32,1024]{1,0:T(8,128)(2,1)S(1)}, bf16[32,1024]{1,0:T(8,128)(2,1)S(1)}, u32[]{:S(2)}, u32[]{:S(2)}) collective-permute-start(bf16[32,1024]{1,0:T(8,128)(2,1)S(1)} %fusion.2), channel_id=1, source_target_pairs={{0,6},{1,7},{2,4},{3,5},{4,2},{5,3},{6,0},{7,1},{8,14},{9,15},{10,... | collective-permute-start | bytes 196616 | tf_op jit(solution)/shard_map/ppermute | solution.py:31
  35.2 5.9 %collective-permute-start.8 = (bf16[32,1024]{1,0:T(8,128)(2,1)S(1)}, bf16[32,1024]{1,0:T(8,128)(2,1)S(1)}, u32[]{:S(2)}, u32[]{:S(2)}) collective-permute-start(bf16[32,1024]{1,0:T(8,128)(2,1)S(1)} %fusion.2), channel_id=1, source_target_pairs={{0,4},{1,5},{2,6},{3,7},{4,0},{5,1},{6,2},{7,3},{8,12},{9,13},{10,... | collective-permute-start | bytes 196616 | tf_op jit(solution)/shard_map/ppermute | solution.py:31
  35.2 5.9 %collective-permute-start.7 = (bf16[32,1024]{1,0:T(8,128)(2,1)S(1)}, bf16[32,1024]{1,0:T(8,128)(2,1)S(1)}, u32[]{:S(2)}, u32[]{:S(2)}) collective-permute-start(bf16[32,1024]{1,0:T(8,128)(2,1)S(1)} %fusion.2), channel_id=1, source_target_pairs={{0,2},{1,3},{2,0},{3,1},{4,6},{5,7},{6,4},{7,5},{8,10},{9,11},{10,... | collective-permute-start | bytes 196616 | tf_op jit(solution)/shard_map/ppermute | solution.py:31
  41.1 4.5 %collective-permute-start.10 = (bf16[32,1024]{1,0:T(8,128)(2,1)S(1)}, bf16[32,1024]{1,0:T(8,128)(2,1)S(1)}, u32[]{:S(2)}, u32[]{:S(2)}) collective-permute-start(bf16[32,1024]{1,0:T(8,128)(2,1)S(1)} %add_convert_fusion.mine_ref.own_ref), channel_id=1, source_target_pairs={{0,8},{8,0},{16,24},{24,16},{1,9},{9,1},{17,25},{25,17},{2,10},{10... | collective-permute-start | bytes 196616 | tf_op jit(solution)/shard_map/ppermute | solution.py:22
  41.7 5.9 %collective-permute-start.12 = (bf16[32,1024]{1,0:T(8,128)(2,1)S(1)}, bf16[32,1024]{1,0:T(8,128)(2,1)S(1)}, u32[]{:S(2)}, u32[]{:S(2)}) collective-permute-start(bf16[32,1024]{1,0:T(8,128)(2,1)S(1)} %add_convert_fusion.mine_ref.own_ref), channel_id=1, source_target_pairs={{0,24},{8,16},{16,8},{24,0},{1,25},{9,17},{17,9},{25,1},{2,26},{10... | collective-permute-start | bytes 196616 | tf_op jit(solution)/shard_map/ppermute | solution.py:22
  43.2 4.4 %collective-permute-start.11 = (bf16[32,1024]{1,0:T(8,128)(2,1)S(1)}, bf16[32,1024]{1,0:T(8,128)(2,1)S(1)}, u32[]{:S(2)}, u32[]{:S(2)}) collective-permute-start(bf16[32,1024]{1,0:T(8,128)(2,1)S(1)} %add_convert_fusion.mine_ref.own_ref), channel_id=1, source_target_pairs={{0,16},{8,24},{16,0},{24,8},{1,17},{9,25},{17,1},{25,9},{2,18},{10... | collective-permute-start | bytes 196616 | tf_op jit(solution)/shard_map/ppermute | solution.py:22
  47.6 2.5 %collective-permute-start.14 = (bf16[96,1024]{1,0:T(8,128)(2,1)S(1)}, bf16[96,1024]{1,0:T(8,128)(2,1)S(1)}, u32[]{:S(2)}, u32[]{:S(2)}) collective-permute-start(bf16[96,1024]{1,0:T(8,128)(2,1)S(1)} %constant_dynamic-update-slice_fusion.rest_ref), channel_id=1, source_target_pairs={{0,1},{1,0},{2,3},{3,2},{4,5},{5,4},{6,7},{7,6},{8,9},{9,8},{10,11... | collective-permute-start | bytes 589832 | tf_op jit(solution)/shard_map/ppermute | solution.py:35
  47.7 1.5 %collective-permute-start.13 = (bf16[32,1024]{1,0:T(8,128)(2,1)S(1)}, bf16[32,1024]{1,0:T(8,128)(2,1)S(1)}, u32[]{:S(2)}, u32[]{:S(2)}) collective-permute-start(bf16[32,1024]{1,0:T(8,128)(2,1)S(1)} %add_convert_fusion.mine_ref.own_ref), channel_id=1, source_target_pairs={{0,1},{1,0},{2,3},{3,2},{4,5},{5,4},{6,7},{7,6},{8,9},{9,8},{10,11... | collective-permute-start | bytes 196616 | tf_op jit(solution)/shard_map/ppermute | solution.py:35
  51.5 1.6 %collective-permute-start.15 = (bf16[128,1024]{1,0:T(8,128)(2,1)S(1)}, bf16[128,1024]{1,0:T(8,128)(2,1)S(1)}, u32[]{:S(2)}, u32[]{:S(2)}) collective-permute-start(bf16[128,1024]{1,0:T(8,128)(2,1)S(1)} %get-tuple-element.43), channel_id=1, source_target_pairs={{0,1},{1,0},{2,3},{3,2},{4,5},{5,4},{6,7},{7,6},{8,9},{9,8},{10,11... | collective-permute-start | bytes 786440 | tf_op jit(solution)/shard_map/ppermute | solution.py:35
  53.2 4.6 %collective-permute-start.16 = (bf16[32,1024]{1,0:T(8,128)(2,1)S(1)}, bf16[32,1024]{1,0:T(8,128)(2,1)S(1)}, u32[]{:S(2)}, u32[]{:S(2)}) collective-permute-start(bf16[32,1024]{1,0:T(8,128)(2,1)S(1)} %get-tuple-element.51), channel_id=1, source_target_pairs={{8,0},{0,8},{24,16},{16,24},{9,1},{1,9},{25,17},{17,25},{10,2},{2,... | collective-permute-start | bytes 196616 | tf_op jit(solution)/shard_map/ppermute | solution.py:22
  54.4 5.5 %collective-permute-start.18 = (bf16[32,1024]{1,0:T(8,128)(2,1)S(1)}, bf16[32,1024]{1,0:T(8,128)(2,1)S(1)}, u32[]{:S(2)}, u32[]{:S(2)}) collective-permute-start(bf16[32,1024]{1,0:T(8,128)(2,1)S(1)} %get-tuple-element.52), channel_id=1, source_target_pairs={{24,0},{16,8},{8,16},{0,24},{25,1},{17,9},{9,17},{1,25},{26,2},{18... | collective-permute-start | bytes 196616 | tf_op jit(solution)/shard_map/ppermute | solution.py:22
  56.1 4.8 %collective-permute-start.17 = (bf16[32,1024]{1,0:T(8,128)(2,1)S(1)}, bf16[32,1024]{1,0:T(8,128)(2,1)S(1)}, u32[]{:S(2)}, u32[]{:S(2)}) collective-permute-start(bf16[32,1024]{1,0:T(8,128)(2,1)S(1)} %get-tuple-element.53), channel_id=1, source_target_pairs={{16,0},{24,8},{0,16},{8,24},{17,1},{25,9},{1,17},{9,25},{18,2},{26... | collective-permute-start | bytes 196616 | tf_op jit(solution)/shard_map/ppermute | solution.py:22
  61.0 10.0 %collective-permute-start.19 = (bf16[32,256]{1,0:T(8,128)(2,1)S(1)}, bf16[32,256]{1,0:T(8,128)(2,1)S(1)}, u32[]{:S(2)}, u32[]{:S(2)}) collective-permute-start(bf16[32,256]{1,0:T(8,128)(2,1)S(1)} %get-tuple-element.54), channel_id=1, source_target_pairs={{0,2},{1,3},{2,0},{3,1},{4,6},{5,7},{6,4},{7,5},{8,10},{9,11},{10,... | collective-permute-start | bytes 49160 | tf_op jit(solution)/shard_map/ppermute | solution.py:31
  62.1 8.9 %collective-permute-start.21 = (bf16[32,256]{1,0:T(8,128)(2,1)S(1)}, bf16[32,256]{1,0:T(8,128)(2,1)S(1)}, u32[]{:S(2)}, u32[]{:S(2)}) collective-permute-start(bf16[32,256]{1,0:T(8,128)(2,1)S(1)} %get-tuple-element.55), channel_id=1, source_target_pairs={{0,6},{1,7},{2,4},{3,5},{4,2},{5,3},{6,0},{7,1},{8,14},{9,15},{10,... | collective-permute-start | bytes 49160 | tf_op jit(solution)/shard_map/ppermute | solution.py:31
  63.8 7.2 %collective-permute-start.20 = (bf16[32,256]{1,0:T(8,128)(2,1)S(1)}, bf16[32,256]{1,0:T(8,128)(2,1)S(1)}, u32[]{:S(2)}, u32[]{:S(2)}) collective-permute-start(bf16[32,256]{1,0:T(8,128)(2,1)S(1)} %get-tuple-element.56), channel_id=1, source_target_pairs={{0,4},{1,5},{2,6},{3,7},{4,0},{5,1},{6,2},{7,3},{8,12},{9,13},{10,... | collective-permute-start | bytes 49160 | tf_op jit(solution)/shard_map/ppermute | solution.py:31
  (25 other events, 219.5 us)

commit v2 on v1

--- a/solution.py
+++ b/solution.py
@@ -4,6 +4,7 @@
 from jax.experimental import pallas as pl
 from jax.experimental.pallas import tpu as pltpu
 from jax.sharding import PartitionSpec as P
+
 
 epsilon = 1e-06
 CORES = 2
@@ -35,18 +36,30 @@
     return lax.ppermute(block, "tp", [(i, i ^ 1) for i in range(count)])
 
 
-def local_kernel(body, name, outs, operands, flops=0, scratch=()):
-    whole = pl.BlockSpec(memory_space=pltpu.VMEM)
-    return pl.pallas_call(
+def local_kernel(body, outs, operands, flops=0, scratch=(), remote=(), far_outs=()):
+    near, far = pl.BlockSpec(memory_space=pltpu.VMEM), pl.BlockSpec(memory_space=pltpu.HBM)
+    call = pl.pallas_call(
         body,
-        name=name,
         out_shape=outs,
-        in_specs=[whole] * len(operands),
-        out_specs=jax.tree.map(lambda _: whole, outs),
+        in_specs=[far if i in remote else near for i in range(len(operands))],
+        out_specs=[far if i in far_outs else near for i in range(len(outs))],
         scratch_shapes=scratch,
         cost_estimate=pl.CostEstimate(flops=flops, bytes_accessed=0, transcendentals=0),
         compiler_params=pltpu.CompilerParams(vmem_limit_bytes=40 << 20),
-    )(*operands)
+    )
+    return call(
+        *(
+            pltpu.with_memory_space_constraint(x, pltpu.HBM) if i in remote else x
+            for i, x in enumerate(operands)
+        )
+    )
+
+
+def fetch(pairs, sems):
+    copies = [pltpu.make_async_copy(a, b, sems.at[i]) for i, (a, b) in enumerate(pairs)]
+    for copy in copies:
+        copy.start()
+    return copies
 
 
 def row_scale(values):
@@ -72,20 +85,33 @@
 
 def pack_tokens(ep_count, expert_total, residual, mixer_gain, routes, route_weight):
     rows, model = residual.shape
+    choices = routes.shape[0]
     depth = model // ep_count
     side = -(-2 * expert_total // LANES) * LANES
 
-    def body(res_ref, gain_ref, routes_ref, weight_ref, *outs):
+    def body(res_hbm, gain_hbm, routes_hbm, weight_hbm, *refs):
+        outs, (res_ref, gain_ref, routes_ref, weight_ref, sems) = refs[:ep_count], refs[ep_count:]
+        copies = fetch(
+            (
+                (routes_hbm, routes_ref),
+                (weight_hbm, weight_ref),
+                (gain_hbm, gain_ref),
+                (res_hbm, res_ref),
+            ),
+            sems,
+        )
+        for copy in copies:
+            copy.wait()
         rank = lax.axis_index("ep")
-        lane = lax.broadcasted_iota(jnp.int32, (rows, side), 1)
-        named = jnp.where(lane < expert_total, lane, lane - expert_total)
-        dense = jnp.zeros((rows, side), F32)
-        for k in range(routes.shape[1]):
+        slot = lax.broadcasted_iota(jnp.int32, (side, rows), 0)
+        named = jnp.where(slot < expert_total, slot, slot - expert_total)
+        dense = jnp.zeros((side, rows), F32)
+        for k in range(choices):
             dense = dense + jnp.where(
-                routes_ref[:, k : k + 1] == named, weight_ref[:, k : k + 1], 0.0
+                routes_ref[k : k + 1, :] == named, weight_ref[k : k + 1, :], 0.0
             )
         high = dense.astype(BF16).astype(F32)
-        dense = jnp.where(lane < expert_total, high, dense - high).astype(BF16)
+        dense = jnp.where(slot < expert_total, high, dense - high).T.astype(BF16)
         for step, out in enumerate(outs):
             start = pl.multiple_of(partner(ep_count, rank, step) * depth, LANES)
             cols = res_ref[:, pl.ds(start, depth)].astype(F32) * gain_ref[:, pl.ds(start, depth)]
@@ -93,7 +119,9 @@
             out[:, depth:] = dense
 
     outs = [jax.ShapeDtypeStruct((rows, depth + side), BF16)] * ep_count
-    return local_kernel(body, "pack_tokens", outs, (residual, mixer_gain, routes, route_weight))
+    operands = (residual, mixer_gain, routes, route_weight)
+    scratch = [pltpu.VMEM(x.shape, x.dtype) for x in operands] + [pltpu.SemaphoreType.DMA((4,))]
+    return local_kernel(body, outs, operands, 0, scratch, range(4))
 
 
 def project(blocks, weights):
@@ -112,21 +140,48 @@
 
     outs = [jax.ShapeDtypeStruct((rows, kinds * width), BF16 if i else F32) for i in range(count)]
     flops = 2 * rows * count * depth * kinds * width
-    return local_kernel(body, "project", outs, (*blocks, *weights), flops)
-
-
-def head_terms(residual, mixer_gain, step_proj, step_bias, log_rate, skip_gain, heads, width):
+    return local_kernel(body, outs, (*blocks, *weights), flops)
+
+
+def head_terms(residual, mixer_gain, step_proj, step_bias, log_rate, skip_gain, conv_state, conv_weight,
+               group_gain, weights, heads, width):
     rows, model = residual.shape
-    total = step_proj.shape[1]
+    total = step_proj.shape[0]
     state = LANES
-
-    def body(res_ref, gain_ref, proj_ref, bias_ref, rate_ref, skip_ref, scale, step, decay, skip, half):
+    kinds, taps = conv_weight.shape[:2]
+    count = len(weights)
+    fetched = (residual, mixer_gain, step_proj, step_bias, log_rate, skip_gain, conv_state)
+
+    def body(*refs):
+        sources, refs = refs[: len(fetched)], refs[len(fetched) :]
+        tap_hbm, group_hbm, refs = refs[0], refs[1], refs[2:]
+        weight_hbm, refs = refs[:count], refs[count:]
+        (scale, step, decay, skip, half, old, last, gain_out), refs = refs[:8], refs[8:]
+        weight_outs, refs = refs[:count], refs[count:]
+        held, (tap_ref, sems) = refs[: len(fetched)], refs[len(fetched) :]
+        res_ref, gain_ref, proj_ref, bias_ref, rate_ref, skip_ref, conv_ref = held
         rank = lax.axis_index("tp")
+        mine = pl.ds(pl.multiple_of(rank * width, LANES), width)
+        copies = fetch(
+            (
+                *zip(sources, held),
+                (tap_hbm.at[:, :, mine], tap_ref),
+                (group_hbm.at[:, mine], gain_out),
+                *zip(weight_hbm, weight_outs),
+            ),
+            sems,
+        )
+        local = len(fetched) + 2
+        for copy in copies[:local]:
+            copy.wait()
         head_start = rank * heads
         values = res_ref[...].astype(F32)
         scaling = row_scale(values)
         normed = (values * scaling * gain_ref[...]).astype(BF16)
-        raw = jnp.dot(normed, proj_ref[...], preferred_element_type=F32) + bias_ref[...]
+        raw = lax.dot_general(
+            normed, proj_ref[...], (((1,), (1,)), ((), ())), preferred_element_type=F32
+        )
+        raw = raw + bias_ref[...]
         size = jnp.maximum(raw, 0.0) + jnp.log1p(jnp.exp(-jnp.abs(raw)))
         fade = jnp.exp(-jnp.exp(rate_ref[...]) * size)
 
@@ -141,6 +196,14 @@
         decay[...] = spread(fade, state)
         skip[...] = spread(jnp.broadcast_to(skip_ref[...], (8, total)), width // heads)
         half[...] = halves(values, rank % CORES, width)[0].astype(BF16)
+        for j in range(kinds):
+            part = conv_ref[0, j].astype(F32) * tap_ref[j, 0:1]
+            for k in range(1, taps - 1):
+                part = part + conv_ref[k, j].astype(F32) * tap_ref[j, k : k + 1]
+            old[j] = part
+            last[j : j + 1, :] = tap_ref[j, taps - 1 : taps]
+        for copy in copies[local:]:
+            copy.wait()
 
     outs = [
         jax.ShapeDtypeStruct((rows, LANES), F32),
@@ -148,9 +211,31 @@
         jax.ShapeDtypeStruct((rows, heads * state), F32),
         jax.ShapeDtypeStruct((8, width), F32),
         jax.ShapeDtypeStruct((rows, model // CORES), BF16),
+        jax.ShapeDtypeStruct((kinds, rows, width), F32),
+        jax.ShapeDtypeStruct((8, width), F32),
+        jax.ShapeDtypeStruct((1, width), F32),
+        *(jax.ShapeDtypeStruct(w.shape, w.dtype) for w in weights),
     ]
-    operands = (residual, mixer_gain, step_proj, step_bias, log_rate, skip_gain)
-    return local_kernel(body, "head_terms", outs, operands, 2 * rows * model * total)
+    operands = (*fetched, conv_weight, group_gain, *weights)
+    scratch = [
+        *(pltpu.VMEM(x.shape, x.dtype) for x in fetched),
+        pltpu.VMEM((kinds, taps, width), F32),
+        pltpu.SemaphoreType.DMA((len(operands),)),
+    ]
+    flops = 2 * rows * model * total
+    return local_kernel(body, outs, operands, flops, scratch, range(len(operands)))
+
+
+def load(arrays):
+    count = len(arrays)
+
+    def body(*refs):
+        for copy in fetch(list(zip(refs[:count], refs[count : 2 * count])), refs[-1]):
+            copy.wait()
+
+    outs = [jax.ShapeDtypeStruct(x.shape, x.dtype) for x in arrays]
+    scratch = [pltpu.SemaphoreType.DMA((count,))]
+    return local_kernel(body, outs, arrays, 0, scratch, range(count))
 
 
 def silu(values):
@@ -210,8 +295,7 @@
             both.append(fed[:, cols] * inner)
         ssm_out = decay_ch * old_part + jnp.concatenate(both, 1) + skip_ref[0:1] * x_act
         gated = ssm_out * silu(fresh[:, :width])
-        start = pl.multiple_of(rank * width, LANES)
-        gain = gain_ref[:, pl.ds(start, width)]
+        gain = gain_ref[...]
         mixed = []
         for g in range(groups):
             cols = slice(g * state, (g + 1) * state)
@@ -233,43 +317,55 @@
         *partials, scale, step, decay, skip, conv_old, conv_last, ssm_state, group_gain, out_proj,
     )
     scratch = [pltpu.VMEM((rows, width), F32), pltpu.VMEM((rows, width), F32)]
-    return local_kernel(body, "mix", outs, operands, 2 * rows * width * model, scratch)
-
-
-def advance_state(ssm_state, decay, fed, written):
+    return local_kernel(body, outs, operands, 2 * rows * width * model, scratch)
+
+
+def advance_state(ssm_state, decay, fed, written, projected, conv_state):
     rows, heads, head_dim, state = ssm_state.shape
     width = heads * head_dim
     groups = width // state
     per_group = heads // groups
+    taps, kinds = conv_state.shape[:2]
     chunk = 8
 
-    def body(state_ref, decay_ref, fed_ref, write_ref, out_ref):
+    def body(state_ref, decay_ref, fed_ref, write_ref, proj_ref, conv_hbm, out_hbm, conv_out, *scratch):
+        buf, fresh, sems = scratch
+        shift = pltpu.make_async_copy(
+            conv_hbm.at[1:], conv_out.at[: taps - 1], sems.at[rows // chunk]
+        )
+        shift.start()
+        for j in range(kinds):
+            fresh[j] = proj_ref[:, (j + 1) * width : (j + 2) * width]
+        newest = pltpu.make_async_copy(fresh, conv_out.at[taps - 1], sems.at[rows // chunk + 1])
+        newest.start()
         fed_cols = fed_ref[...].T
-        for s in range(chunk):
+        copies = [shift, newest]
+        for s in range(rows):
             for h in range(heads):
                 g = h // per_group
                 fade = decay_ref[s : s + 1, h * state : (h + 1) * state]
                 write = write_ref[s : s + 1, g * state : (g + 1) * state]
                 column = fed_cols[h * head_dim : (h + 1) * head_dim, s : s + 1]
-                out_ref[s, h] = fade * state_ref[s, h] + column * write
-
-    block = pl.BlockSpec((chunk, heads, head_dim, state), lambda i: (i, 0, 0, 0))
-    return pl.pallas_call(
-        body,
-        name="advance_state",
-        grid=(rows // chunk,),
-        out_shape=jax.ShapeDtypeStruct(ssm_state.shape, F32),
-        in_specs=[
-            block,
-            pl.BlockSpec((chunk, heads * state), lambda i: (i, 0)),
-            pl.BlockSpec((chunk, width), lambda i: (i, 0)),
-            pl.BlockSpec((chunk, width), lambda i: (i, 0)),
-        ],
-        out_specs=block,
-        cost_estimate=pl.CostEstimate(
-            flops=8 << 20, bytes_accessed=2 * ssm_state.size * 4, transcendentals=0
-        ),
-    )(ssm_state, decay, fed, written)
+                buf[s, h] = fade * state_ref[s, h] + column * write
+            if s % chunk == chunk - 1:
+                span = pl.ds(s - chunk + 1, chunk)
+                done = pltpu.make_async_copy(buf.at[span], out_hbm.at[span], sems.at[s // chunk])
+                done.start()
+                copies.append(done)
+        for copy in copies:
+            copy.wait()
+
+    outs = [
+        jax.ShapeDtypeStruct(ssm_state.shape, F32),
+        jax.ShapeDtypeStruct(conv_state.shape, conv_state.dtype),
+    ]
+    scratch = [
+        pltpu.VMEM(ssm_state.shape, F32),
+        pltpu.VMEM((kinds, rows, width), conv_state.dtype),
+        pltpu.SemaphoreType.DMA((rows // chunk + 2,)),
+    ]
+    operands = (ssm_state, decay, fed, written, projected, conv_state)
+    return local_kernel(body, outs, operands, 8 << 20, scratch, (5,), (0, 1))
 
 
 def dense_branch(mine, other, ffn_gain, gate, up, down, blend):
@@ -294,11 +390,11 @@
 
     outs = [jax.ShapeDtypeStruct((rows, half), F32)] * 2
     operands = (mine, other, ffn_gain, gate, up, down, blend)
-    return local_kernel(body, "dense_branch", outs, operands, 6 * rows * model * gate.shape[1])
+    return local_kernel(body, outs, operands, 6 * rows * model * gate.shape[1])
 
 
 def run_experts(tokens, ffn_gain, gate, up, down, dense_mine, dense_other, packed, depth):
-    own, rest, own_other, rest_other = tokens
+    own, rest, _, _ = tokens
     rows, half = own.shape
     every = rows + rest.shape[0]
     model = half * CORES
@@ -335,10 +431,10 @@
     outs = [jax.ShapeDtypeStruct((every, half), F32), jax.ShapeDtypeStruct((every, half), BF16)]
     operands = (*tokens, ffn_gain, gate, up, down, dense_mine, dense_other, *packed)
     flops = 6 * every * model * gate.shape[2] * experts
-    return local_kernel(body, "run_experts", outs, operands, flops)
-
-
-def on_device(
+    return local_kernel(body, outs, operands, flops)
+
+
+def layer(
     residual,
     mixer_gain,
     gate_proj,
@@ -376,39 +472,38 @@
     expert_total = expert_gate.shape[0] * ep_count
     as_row = lambda vector: vector.reshape(1, -1)
 
-    packed = pack_tokens(ep_count, expert_total, residual, as_row(mixer_gain), routes, route_weight)
+    packed = pack_tokens(
+        ep_count, expert_total, residual, as_row(mixer_gain), routes.T, route_weight.T
+    )
     blocks = [packed[0]] + [send_ep(packed[k], ep_count, k) for k in ep_steps]
-    partials = project(blocks, (gate_proj, input_proj, write_proj, read_proj))
+    conv_rows = conv_state.transpose(1, 2, 0, 3)
+    scale, step, decay, skip, resid_half, conv_old, conv_last, gain, *weights = head_terms(
+        residual, as_row(mixer_gain), step_proj.T, as_row(step_bias), as_row(log_rate),
+        as_row(skip_gain), conv_rows, conv_weight.transpose(1, 0, 2), as_row(group_gain),
+        (gate_proj, input_proj, write_proj, read_proj), heads, width,
+    )
+    partials = project(blocks, weights)
     parts = [partials[0]] + [send_ep(partials[k], ep_count, k, back=True) for k in ep_steps]
-
-    scale, step, decay, skip, resid_half = head_terms(
-        residual, as_row(mixer_gain), step_proj, as_row(step_bias), as_row(log_rate),
-        as_row(skip_gain), heads, width,
-    )
-    taps = lax.dynamic_slice_in_dim(conv_weight, tp_rank * width, width, 2)
-    conv_old = jnp.sum(
-        conv_state.astype(F32) * taps[None, :-1], axis=1
-    ).transpose(1, 0, 2)
-
+    state, out_weight = load((ssm_state, out_proj))
     projected, fed, written, mine, other = mix(
-        parts, scale, step, decay, skip, conv_old, taps[-1], ssm_state, as_row(group_gain), out_proj
-    )
-    newest = projected[:, width:].reshape(rows, 1, 3, width)
-    new_conv = jnp.concatenate((conv_state[:, 1:], newest), axis=1)
+        parts, scale, step, decay, skip, conv_old, conv_last, state, gain, out_weight
+    )
 
     mine = mine + send_core(other, tp_count).astype(F32)
     shared = mine.astype(BF16)
-    for k in z_steps:
-        mine = mine + send_z(shared, z_count, k).astype(F32)
+    gathered = [send_z(shared, z_count, k) for k in z_steps]
+    new_state, new_conv = advance_state(state, decay, fed, written, projected, conv_rows)
+    new_conv = new_conv.transpose(2, 0, 1, 3)
+    for part in gathered:
+        mine = mine + part.astype(F32)
     resid_mid = (resid_half.astype(F32) + mine).astype(BF16)
-    new_state = advance_state(ssm_state, decay, fed, written)
 
     others = [send_ep(resid_mid, ep_count, k) for k in ep_steps]
-    rest = jnp.concatenate(others, 0)
     own_other = send_core(resid_mid, tp_count)
     dense_mine, dense_other = dense_branch(
         resid_mid, own_other, as_row(ffn_gain), dense_gate, dense_up, dense_down, as_row(blend_weight)
     )
+    rest = jnp.concatenate(others, 0)
     rest_other = send_core(rest, tp_count)
     mine, other = run_experts(
         (resid_mid, rest, own_other, rest_other), as_row(ffn_gain), expert_gate, expert_up,
@@ -429,7 +524,7 @@
 
 def solution(mesh):
     return jax.shard_map(
-        on_device,
+        layer,
         mesh=mesh,
         in_specs=(
             P("ep", None),

time: 72.2 us -> 61.5 us (0.85)
  local copies, waits for them, and re-layouts: 14.2 us -> 2.3 us
  Pallas kernels: 10 us -> 13.1 us
  other arithmetic: 2.43 us -> 0.81 us
  starting transfers between devices: 24.2 us -> 25 us
    unnamed x59 -> x22, local copies, waits for them, and re-layouts: 14 us -> 2.25 us
    pallas_call x7 -> x8, Pallas kernels: 10 us -> 13.1 us  [local_kernel(): call(*(pltpu.with_memory_space_constraint(x, pltpu.HBM) if i in remote el...]
    reduce_sum x1 -> x0, other arithmetic: 0.95 us -> none  [on_device(): jnp.sum(conv_state.astype(F32) * taps[None, :-1], axis=1).transpose(1, 0, 2)]
    ppermute x6, starting transfers between devices: 8.01 us -> 8.91 us  [send_z(): return lax.ppermute(block, 'tp', pairs)]
  transfers between devices with their start and end apart: 22 -> 22, of which waited for: 12 -> 12; matrix products, arithmetic and copies ran while one was open for 4% -> 0% of each run, Pallas kernels for 10% -> 15%
where the time goes in v2:
time: 61.5 us; the launch traced here: 61.4 us
  starting transfers between devices  25 us (41%)
  waiting for transfers between devices  19.2 us (31%)
  Pallas kernels  13.1 us (21%)
  local copies, waits for them, and re-layouts  2.3 us (4%)
  between operations  0.93 us (2%)
  other arithmetic  0.81 us (1%)
    ppermute x12, starting transfers between devices, send_ep(): lax.ppermute(block, 'ep', [(b, a) for a, b in pairs] if back else pairs)  15.2 us
    pallas_call x8, Pallas kernels, local_kernel(): call(*(pltpu.with_memory_space_constraint(x, pltpu.HBM) if i in remote el...  13.1 us
    ppermute x12, waiting for transfers between devices, send_ep(): lax.ppermute(block, 'ep', [(b, a) for a, b in pairs] if back else pairs)  10.5 us
    ppermute x6, starting transfers between devices, send_z(): return lax.ppermute(block, 'tp', pairs)  8.91 us
    ppermute x6, waiting for transfers between devices, send_z(): return lax.ppermute(block, 'tp', pairs)  5.18 us
    ppermute x4, waiting for transfers between devices, send_core(): return lax.ppermute(block, 'tp', [(i, i ^ 1) for i in range(count)])  3.56 us
    unnamed x22, local copies, waits for them, and re-layouts  2.25 us
  transfers between devices with their start and end apart: 22, of which 12 were waited for; matrix products, arithmetic and copies ran while one was open for 0% of the time, Pallas kernels for 15%

profile of v2, /device:TPU:0, one launch (start us, length us, event | category | flops | bytes accessed | tf_op | source)
XLA Modules:
  0.0 61.4 jit_solution(11411407559808332283)
XLA Ops:
  0.6 1.1 %shard_map.257 = (bf16[32,640]{1,0:T(8,128)(2,1)S(1)}, bf16[32,640]{1,0:T(8,128)(2,1)S(1)}, bf16[32,640]{1,0:T(8,128)(2,1)S(1)}, bf16[32,640]{1,0:T(8,128)(2,1)S(1)}) custom-call(bf16[32,2048]{1,0:T(8,128)(2,1)} %res_hbm.1, f32[1,2048]{1,0:T(1,128)} %bitcast.18, s32[2,32]{1,0:T(2,128)} %bitcast.21, f32[2,32]{1,0:T(2,128)} %bitcast.22), custom_call_target="tpu_custom_call" | custom-call | tf_op jit(solution)/shard_map/pallas_call | solution.py:50
  1.7 3.0 %collective-permute-start = (bf16[32,640]{1,0:T(8,128)(2,1)S(1)}, bf16[32,640]{1,0:T(8,128)(2,1)S(1)}, u32[]{:S(2)}, u32[]{:S(2)}) collective-permute-start(bf16[32,640]{1,0:T(8,128)(2,1)S(1)} %get-tuple-element.38), channel_id=1, source_target_pairs={{0,8},{8,0},{16,24},{24,16},{1,9},{9,1},{17,25},{25,17},{2,10},{10... | collective-permute-start | bytes 122888 | tf_op jit(solution)/shard_map/ppermute | solution.py:23
  4.8 1.5 %collective-permute-start.1 = (bf16[32,640]{1,0:T(8,128)(2,1)S(1)}, bf16[32,640]{1,0:T(8,128)(2,1)S(1)}, u32[]{:S(2)}, u32[]{:S(2)}) collective-permute-start(bf16[32,640]{1,0:T(8,128)(2,1)S(1)} %get-tuple-element.39), channel_id=1, source_target_pairs={{0,16},{8,24},{16,0},{24,8},{1,17},{9,25},{17,1},{25,9},{2,18},{10... | collective-permute-start | bytes 122888 | tf_op jit(solution)/shard_map/ppermute | solution.py:23
  6.3 1.8 %shard_map.256 = (f32[32,128]{1,0:T(8,128)S(1)}, f32[32,256]{1,0:T(8,128)S(1)}, f32[32,512]{1,0:T(8,128)S(1)}, f32[8,256]{1,0:T(8,128)S(1)}, bf16[32,1024]{1,0:T...) custom-call(bf16[32,2048]{1,0:T(8,128)(2,1)} %res_hbm.1, ...), custom_call_target="tpu_custom_call" | custom-call | flops 4194304 | tf_op jit(solution)/shard_map/pallas_call | solution.py:50
  8.8 2.4 %collective-permute-done.2.refs_3_.more_3_ = bf16[32,640]{1,0:T(8,128)(2,1)S(1)} collective-permute-done((bf16[32,640]{1,0:T(8,128)(2,1)S(1)}, bf16[32,640]{1,0:T(8,128)(2,1)S(1)}, u32[]{:S(2)}, u32[]{:S(2)}) %collective-permute-start.2) | collective-permute-done | bytes 40992 | tf_op jit(solution)/shard_map/ppermute | solution.py:23
  12.2 2.9 %collective-permute-start.5 = (bf16[32,1024]{1,0:T(8,128)(2,1)S(1)}, bf16[32,1024]{1,0:T(8,128)(2,1)S(1)}, u32[]{:S(2)}, u32[]{:S(2)}) collective-permute-start(bf16[32,1024]{1,0:T(8,128)(2,1)S(1)} %get-tuple-element.48), channel_id=1, source_target_pairs={{24,0},{16,8},{8,16},{0,24},{25,1},{17,9},{9,17},{1,25},{26,2},{18... | collective-permute-start | bytes 196616 | tf_op jit(solution)/shard_map/ppermute | solution.py:23
  15.1 2.5 %shard_map.259 = (f32[32,4,64,128]{3,2,1,0:T(8,128)S(1)}, bf16[256,2048]{1,0:T(8,128)(2,1)S(1)}) custom-call(f32[32,4,64,128]{3,2,1,0:T(8,128)} %refs_0_.3, bf16[256,2048]{1,0:T(8,128)(2,1)} %refs_1_.1), custom_call_target="tpu_custom_call" | custom-call | tf_op jit(solution)/shard_map/pallas_call | solution.py:50
  18.8 1.2 %collective-permute-done.6 = bf16[32,1024]{1,0:T(8,128)(2,1)S(1)} collective-permute-done((bf16[32,1024]{1,0:T(8,128)(2,1)S(1)}, bf16[32,1024]{1,0:T(8,128)(2,1)S(1)}, u32[]{:S(2)}, u32[]{:S(2)}) %collective-permute-start.6) | collective-permute-done | bytes 65568 | tf_op jit(solution)/shard_map/ppermute | solution.py:36
  20.1 3.7 %collective-permute-start.9 = (bf16[32,1024]{1,0:T(8,128)(2,1)S(1)}, bf16[32,1024]{1,0:T(8,128)(2,1)S(1)}, u32[]{:S(2)}, u32[]{:S(2)}) collective-permute-start(bf16[32,1024]{1,0:T(8,128)(2,1)S(1)} %fusion.2), channel_id=1, source_target_pairs={{0,6},{1,7},{2,4},{3,5},{4,2},{5,3},{6,0},{7,1},{8,14},{9,15},{10,... | collective-permute-start | bytes 196616 | tf_op jit(solution)/shard_map/ppermute | solution.py:32
  24.5 1.9 %collective-permute-done.9 = bf16[32,1024]{1,0:T(8,128)(2,1)S(1)} collective-permute-done((bf16[32,1024]{1,0:T(8,128)(2,1)S(1)}, bf16[32,1024]{1,0:T(8,128)(2,1)S(1)}, u32[]{:S(2)}, u32[]{:S(2)}) %collective-permute-start.9) | collective-permute-done | bytes 65568 | tf_op jit(solution)/shard_map/ppermute | solution.py:32
  26.4 3.3 %collective-permute-done.8 = bf16[32,1024]{1,0:T(8,128)(2,1)S(1)} collective-permute-done((bf16[32,1024]{1,0:T(8,128)(2,1)S(1)}, bf16[32,1024]{1,0:T(8,128)(2,1)S(1)}, u32[]{:S(2)}, u32[]{:S(2)}) %collective-permute-start.8) | collective-permute-done | bytes 65568 | tf_op jit(solution)/shard_map/ppermute | solution.py:32
  29.8 1.6 %collective-permute-start.10 = (bf16[32,1024]{1,0:T(8,128)(2,1)S(1)}, bf16[32,1024]{1,0:T(8,128)(2,1)S(1)}, u32[]{:S(2)}, u32[]{:S(2)}) collective-permute-start(bf16[32,1024]{1,0:T(8,128)(2,1)S(1)} %add_convert_fusion.mine_ref.own_ref), channel_id=1, source_target_pairs={{0,8},{8,0},{16,24},{24,16},{1,9},{9,1},{17,25},{25,17},{2,10},{10... | collective-permute-start | bytes 196616 | tf_op jit(solution)/shard_map/ppermute | solution.py:23
  31.3 1.5 %collective-permute-start.11 = (bf16[32,1024]{1,0:T(8,128)(2,1)S(1)}, bf16[32,1024]{1,0:T(8,128)(2,1)S(1)}, u32[]{:S(2)}, u32[]{:S(2)}) collective-permute-start(bf16[32,1024]{1,0:T(8,128)(2,1)S(1)} %add_convert_fusion.mine_ref.own_ref), channel_id=1, source_target_pairs={{0,16},{8,24},{16,0},{24,8},{1,17},{9,25},{17,1},{25,9},{2,18},{10... | collective-permute-start | bytes 196616 | tf_op jit(solution)/shard_map/ppermute | solution.py:23
  34.1 2.2 %collective-permute-done.11 = bf16[32,1024]{1,0:T(8,128)(2,1)S(1)} collective-permute-done((bf16[32,1024]{1,0:T(8,128)(2,1)S(1)}, bf16[32,1024]{1,0:T(8,128)(2,1)S(1)}, u32[]{:S(2)}, u32[]{:S(2)}) %collective-permute-start.11) | collective-permute-done | bytes 65568 | tf_op jit(solution)/shard_map/ppermute | solution.py:23
  36.3 1.7 %collective-permute-done.12 = bf16[32,1024]{1,0:T(8,128)(2,1)S(1)} collective-permute-done((bf16[32,1024]{1,0:T(8,128)(2,1)S(1)}, bf16[32,1024]{1,0:T(8,128)(2,1)S(1)}, u32[]{:S(2)}, u32[]{:S(2)}) %collective-permute-start.12) | collective-permute-done | bytes 65568 | tf_op jit(solution)/shard_map/ppermute | solution.py:23
  40.4 1.3 %shard_map.262 = (f32[128,1024]{1,0:T(8,128)S(1)}, bf16[128,1024]{1,0:T(8,128)(2,1)S(1)}) custom-call(bf16[32,1024]{1,0:T(8,128)(2,1)S(1)} %add_convert_fusion.mine_ref.own_ref, bf16[96,1024]{1,0:T(8,128)(2,1)S(1)} %constant_dynamic-update-slice_fusion.rest_ref, bf16[32,1024]{1,0:T(8,128)(2,1)S(1)} %collective-permute-done.13.other_ref.own2_ref, ...), custom_call_target="tpu_custom_call" | custom-call | flops 805306368 | tf_op jit(solution)/shard_map/pallas_call | solution.py:50
  42.1 1.3 %collective-permute-done.15 = bf16[128,1024]{1,0:T(8,128)(2,1)S(1)} collective-permute-done((bf16[128,1024]{1,0:T(8,128)(2,1)S(1)}, bf16[128,1024]{1,0:T(8,128)(2,1)S(1)}, u32[]{:S(2)}, u32[]{:S(2)}) %collective-permute-start.15) | collective-permute-done | bytes 262176 | tf_op jit(solution)/shard_map/ppermute | solution.py:36
  44.1 1.5 %collective-permute-start.17 = (bf16[32,1024]{1,0:T(8,128)(2,1)S(1)}, bf16[32,1024]{1,0:T(8,128)(2,1)S(1)}, u32[]{:S(2)}, u32[]{:S(2)}) collective-permute-start(bf16[32,1024]{1,0:T(8,128)(2,1)S(1)} %get-tuple-element.75), channel_id=1, source_target_pairs={{16,0},{24,8},{0,16},{8,24},{17,1},{25,9},{1,17},{9,25},{18,2},{26... | collective-permute-start | bytes 196616 | tf_op jit(solution)/shard_map/ppermute | solution.py:23
  45.6 1.5 %collective-permute-start.16 = (bf16[32,1024]{1,0:T(8,128)(2,1)S(1)}, bf16[32,1024]{1,0:T(8,128)(2,1)S(1)}, u32[]{:S(2)}, u32[]{:S(2)}) collective-permute-start(bf16[32,1024]{1,0:T(8,128)(2,1)S(1)} %get-tuple-element.73), channel_id=1, source_target_pairs={{8,0},{0,8},{24,16},{16,24},{9,1},{1,9},{25,17},{17,25},{10,2},{2,... | collective-permute-start | bytes 196616 | tf_op jit(solution)/shard_map/ppermute | solution.py:23
  47.1 2.3 %collective-permute-done.18 = bf16[32,1024]{1,0:T(8,128)(2,1)S(1)} collective-permute-done((bf16[32,1024]{1,0:T(8,128)(2,1)S(1)}, bf16[32,1024]{1,0:T(8,128)(2,1)S(1)}, u32[]{:S(2)}, u32[]{:S(2)}) %collective-permute-start.18) | collective-permute-done | bytes 65568 | tf_op jit(solution)/shard_map/ppermute | solution.py:23
  49.9 2.5 %collective-permute-start.21 = (bf16[32,256]{1,0:T(8,128)(2,1)S(1)}, bf16[32,256]{1,0:T(8,128)(2,1)S(1)}, u32[]{:S(2)}, u32[]{:S(2)}) collective-permute-start(bf16[32,256]{1,0:T(8,128)(2,1)S(1)} %get-tuple-element.77), channel_id=1, source_target_pairs={{0,6},{1,7},{2,4},{3,5},{4,2},{5,3},{6,0},{7,1},{8,14},{9,15},{10,... | collective-permute-start | bytes 49160 | tf_op jit(solution)/shard_map/ppermute | solution.py:32
  52.5 1.8 %collective-permute-start.19 = (bf16[32,256]{1,0:T(8,128)(2,1)S(1)}, bf16[32,256]{1,0:T(8,128)(2,1)S(1)}, u32[]{:S(2)}, u32[]{:S(2)}) collective-permute-start(bf16[32,256]{1,0:T(8,128)(2,1)S(1)} %get-tuple-element.76), channel_id=1, source_target_pairs={{0,2},{1,3},{2,0},{3,1},{4,6},{5,7},{6,4},{7,5},{8,10},{9,11},{10,... | collective-permute-start | bytes 49160 | tf_op jit(solution)/shard_map/ppermute | solution.py:32
  54.4 2.2 %copy-done.1 = f32[32,4,64,128]{3,2,1,0:T(8,128)S(1)} copy-done((f32[32,4,64,128]{3,2,1,0:T(8,128)S(1)}, f32[32,4,64,128]{3,2,1,0:T(8,128)}, u32[]{:S(2)}) %copy-start.1) | copy-done | bytes 4194328
  56.5 4.1 %shard_map.263 = (f32[32,4,64,128]{3,2,1,0:T(8,128)}, bf16[3,3,32,256]{3,2,1,0:T(8,128)(2,1)}) custom-call(f32[32,4,64,128]{3,2,1,0:T(8,128)S(1)} %copy-done.1, f32[32,512]{1,0:T(8,128)S(1)} %get-tuple-element.51.refs_6_.decay_ref, f32[32,256]{1,0:T(8,128)S(1)} %get-tuple-element.64.fed_ref, f32[32,256]{1,0:T(8,128)S(1)} %get-tuple-element.65.write_ref, ...), custom_call_target="tpu_custom_call" | custom-call | flops 8388608 | tf_op jit(solution)/shard_map/pallas_call | solution.py:50
  (59 shorter events, 9.3 us)
Async XLA Ops:
  1.7 6.4 %collective-permute-start = (bf16[32,640]{1,0:T(8,128)(2,1)S(1)}, bf16[32,640]{1,0:T(8,128)(2,1)S(1)}, u32[]{:S(2)}, u32[]{:S(2)}) collective-permute-start(bf16[32,640]{1,0:T(8,128)(2,1)S(1)} %get-tuple-element.38), channel_id=1, source_target_pairs={{0,8},{8,0},{16,24},{24,16},{1,9},{9,1},{17,25},{25,17},{2,10},{10... | collective-permute-start | bytes 122888 | tf_op jit(solution)/shard_map/ppermute | solution.py:23
  4.8 4.0 %collective-permute-start.1 = (bf16[32,640]{1,0:T(8,128)(2,1)S(1)}, bf16[32,640]{1,0:T(8,128)(2,1)S(1)}, u32[]{:S(2)}, u32[]{:S(2)}) collective-permute-start(bf16[32,640]{1,0:T(8,128)(2,1)S(1)} %get-tuple-element.39), channel_id=1, source_target_pairs={{0,16},{8,24},{16,0},{24,8},{1,17},{9,25},{17,1},{25,9},{2,18},{10... | collective-permute-start | bytes 122888 | tf_op jit(solution)/shard_map/ppermute | solution.py:23
  6.3 4.9 %collective-permute-start.2 = (bf16[32,640]{1,0:T(8,128)(2,1)S(1)}, bf16[32,640]{1,0:T(8,128)(2,1)S(1)}, u32[]{:S(2)}, u32[]{:S(2)}) collective-permute-start(bf16[32,640]{1,0:T(8,128)(2,1)S(1)} %get-tuple-element.40), channel_id=1, source_target_pairs={{0,24},{8,16},{16,8},{24,0},{1,25},{9,17},{17,9},{25,1},{2,26},{10... | collective-permute-start | bytes 122888 | tf_op jit(solution)/shard_map/ppermute | solution.py:23
  11.5 6.1 %collective-permute-start.3 = (bf16[32,1024]{1,0:T(8,128)(2,1)S(1)}, bf16[32,1024]{1,0:T(8,128)(2,1)S(1)}, u32[]{:S(2)}, u32[]{:S(2)}) collective-permute-start(bf16[32,1024]{1,0:T(8,128)(2,1)S(1)} %get-tuple-element.46), channel_id=1, source_target_pairs={{8,0},{0,8},{24,16},{16,24},{9,1},{1,9},{25,17},{17,25},{10,2},{2,... | collective-permute-start | bytes 196616 | tf_op jit(solution)/shard_map/ppermute | solution.py:23
  12.1 5.5 %collective-permute-start.4 = (bf16[32,1024]{1,0:T(8,128)(2,1)S(1)}, bf16[32,1024]{1,0:T(8,128)(2,1)S(1)}, u32[]{:S(2)}, u32[]{:S(2)}) collective-permute-start(bf16[32,1024]{1,0:T(8,128)(2,1)S(1)} %get-tuple-element.47), channel_id=1, source_target_pairs={{16,0},{24,8},{0,16},{8,24},{17,1},{25,9},{1,17},{9,25},{18,2},{26... | collective-permute-start | bytes 196616 | tf_op jit(solution)/shard_map/ppermute | solution.py:23
  12.2 5.5 %collective-permute-start.5 = (bf16[32,1024]{1,0:T(8,128)(2,1)S(1)}, bf16[32,1024]{1,0:T(8,128)(2,1)S(1)}, u32[]{:S(2)}, u32[]{:S(2)}) collective-permute-start(bf16[32,1024]{1,0:T(8,128)(2,1)S(1)} %get-tuple-element.48), channel_id=1, source_target_pairs={{24,0},{16,8},{8,16},{0,24},{25,1},{17,9},{9,17},{1,25},{26,2},{18... | collective-permute-start | bytes 196616 | tf_op jit(solution)/shard_map/ppermute | solution.py:23
  17.6 22.8 %copy-start = (f32[32,4,64,128]{3,2,1,0:T(8,128)}, f32[32,4,64,128]{3,2,1,0:T(8,128)S(1)}, u32[]{:S(2)}) copy-start(f32[32,4,64,128]{3,2,1,0:T(8,128)S(1)} %get-tuple-element.55.refs_10_.state_ref) | copy-start | bytes 12582916
  17.7 22.8 %copy-start.2 = (bf16[2,2048,256]{2,1,0:T(8,128)(2,1)S(1)}, bf16[2,2048,256]{2,1,0:T(8,128)(2,1)}, u32[]{:S(2)}) copy-start(bf16[2,2048,256]{2,1,0:T(8,128)(2,1)} %gate_ref.3) | copy-start | bytes 6291460
  18.8 1.3 %collective-permute-start.6 = (bf16[32,1024]{1,0:T(8,128)(2,1)S(1)}, bf16[32,1024]{1,0:T(8,128)(2,1)S(1)}, u32[]{:S(2)}, u32[]{:S(2)}) collective-permute-start(bf16[32,1024]{1,0:T(8,128)(2,1)S(1)} %get-tuple-element.59), channel_id=1, source_target_pairs={{0,1},{1,0},{2,3},{3,2},{4,5},{5,4},{6,7},{7,6},{8,9},{9,8},{10,11... | collective-permute-start | bytes 196616 | tf_op jit(solution)/shard_map/ppermute | solution.py:36
  20.1 6.4 %collective-permute-start.9 = (bf16[32,1024]{1,0:T(8,128)(2,1)S(1)}, bf16[32,1024]{1,0:T(8,128)(2,1)S(1)}, u32[]{:S(2)}, u32[]{:S(2)}) collective-permute-start(bf16[32,1024]{1,0:T(8,128)(2,1)S(1)} %fusion.2), channel_id=1, source_target_pairs={{0,6},{1,7},{2,4},{3,5},{4,2},{5,3},{6,0},{7,1},{8,14},{9,15},{10,... | collective-permute-start | bytes 196616 | tf_op jit(solution)/shard_map/ppermute | solution.py:32
  23.8 5.9 %collective-permute-start.8 = (bf16[32,1024]{1,0:T(8,128)(2,1)S(1)}, bf16[32,1024]{1,0:T(8,128)(2,1)S(1)}, u32[]{:S(2)}, u32[]{:S(2)}) collective-permute-start(bf16[32,1024]{1,0:T(8,128)(2,1)S(1)} %fusion.2), channel_id=1, source_target_pairs={{0,4},{1,5},{2,6},{3,7},{4,0},{5,1},{6,2},{7,3},{8,12},{9,13},{10,... | collective-permute-start | bytes 196616 | tf_op jit(solution)/shard_map/ppermute | solution.py:32
  23.8 5.9 %collective-permute-start.7 = (bf16[32,1024]{1,0:T(8,128)(2,1)S(1)}, bf16[32,1024]{1,0:T(8,128)(2,1)S(1)}, u32[]{:S(2)}, u32[]{:S(2)}) collective-permute-start(bf16[32,1024]{1,0:T(8,128)(2,1)S(1)} %fusion.2), channel_id=1, source_target_pairs={{0,2},{1,3},{2,0},{3,1},{4,6},{5,7},{6,4},{7,5},{8,10},{9,11},{10,... | collective-permute-start | bytes 196616 | tf_op jit(solution)/shard_map/ppermute | solution.py:32
  29.8 4.3 %collective-permute-start.10 = (bf16[32,1024]{1,0:T(8,128)(2,1)S(1)}, bf16[32,1024]{1,0:T(8,128)(2,1)S(1)}, u32[]{:S(2)}, u32[]{:S(2)}) collective-permute-start(bf16[32,1024]{1,0:T(8,128)(2,1)S(1)} %add_convert_fusion.mine_ref.own_ref), channel_id=1, source_target_pairs={{0,8},{8,0},{16,24},{24,16},{1,9},{9,1},{17,25},{25,17},{2,10},{10... | collective-permute-start | bytes 196616 | tf_op jit(solution)/shard_map/ppermute | solution.py:23
  31.3 5.0 %collective-permute-start.11 = (bf16[32,1024]{1,0:T(8,128)(2,1)S(1)}, bf16[32,1024]{1,0:T(8,128)(2,1)S(1)}, u32[]{:S(2)}, u32[]{:S(2)}) collective-permute-start(bf16[32,1024]{1,0:T(8,128)(2,1)S(1)} %add_convert_fusion.mine_ref.own_ref), channel_id=1, source_target_pairs={{0,16},{8,24},{16,0},{24,8},{1,17},{9,25},{17,1},{25,9},{2,18},{10... | collective-permute-start | bytes 196616 | tf_op jit(solution)/shard_map/ppermute | solution.py:23
  32.8 5.2 %collective-permute-start.12 = (bf16[32,1024]{1,0:T(8,128)(2,1)S(1)}, bf16[32,1024]{1,0:T(8,128)(2,1)S(1)}, u32[]{:S(2)}, u32[]{:S(2)}) collective-permute-start(bf16[32,1024]{1,0:T(8,128)(2,1)S(1)} %add_convert_fusion.mine_ref.own_ref), channel_id=1, source_target_pairs={{0,24},{8,16},{16,8},{24,0},{1,25},{9,17},{17,9},{25,1},{2,26},{10... | collective-permute-start | bytes 196616 | tf_op jit(solution)/shard_map/ppermute | solution.py:23
  38.0 2.4 %collective-permute-start.14 = (bf16[96,1024]{1,0:T(8,128)(2,1)S(1)}, bf16[96,1024]{1,0:T(8,128)(2,1)S(1)}, u32[]{:S(2)}, u32[]{:S(2)}) collective-permute-start(bf16[96,1024]{1,0:T(8,128)(2,1)S(1)} %constant_dynamic-update-slice_fusion.rest_ref), channel_id=1, source_target_pairs={{0,1},{1,0},{2,3},{3,2},{4,5},{5,4},{6,7},{7,6},{8,9},{9,8},{10,11... | collective-permute-start | bytes 589832 | tf_op jit(solution)/shard_map/ppermute | solution.py:36
  38.0 1.5 %collective-permute-start.13 = (bf16[32,1024]{1,0:T(8,128)(2,1)S(1)}, bf16[32,1024]{1,0:T(8,128)(2,1)S(1)}, u32[]{:S(2)}, u32[]{:S(2)}) collective-permute-start(bf16[32,1024]{1,0:T(8,128)(2,1)S(1)} %add_convert_fusion.mine_ref.own_ref), channel_id=1, source_target_pairs={{0,1},{1,0},{2,3},{3,2},{4,5},{5,4},{6,7},{7,6},{8,9},{9,8},{10,11... | collective-permute-start | bytes 196616 | tf_op jit(solution)/shard_map/ppermute | solution.py:36
  41.8 1.6 %collective-permute-start.15 = (bf16[128,1024]{1,0:T(8,128)(2,1)S(1)}, bf16[128,1024]{1,0:T(8,128)(2,1)S(1)}, u32[]{:S(2)}, u32[]{:S(2)}) collective-permute-start(bf16[128,1024]{1,0:T(8,128)(2,1)S(1)} %get-tuple-element.63), channel_id=1, source_target_pairs={{0,1},{1,0},{2,3},{3,2},{4,5},{5,4},{6,7},{7,6},{8,9},{9,8},{10,11... | collective-permute-start | bytes 786440 | tf_op jit(solution)/shard_map/ppermute | solution.py:36
  43.5 5.9 %collective-permute-start.18 = (bf16[32,1024]{1,0:T(8,128)(2,1)S(1)}, bf16[32,1024]{1,0:T(8,128)(2,1)S(1)}, u32[]{:S(2)}, u32[]{:S(2)}) collective-permute-start(bf16[32,1024]{1,0:T(8,128)(2,1)S(1)} %get-tuple-element.74), channel_id=1, source_target_pairs={{24,0},{16,8},{8,16},{0,24},{25,1},{17,9},{9,17},{1,25},{26,2},{18... | collective-permute-start | bytes 196616 | tf_op jit(solution)/shard_map/ppermute | solution.py:23
  44.1 5.4 %collective-permute-start.17 = (bf16[32,1024]{1,0:T(8,128)(2,1)S(1)}, bf16[32,1024]{1,0:T(8,128)(2,1)S(1)}, u32[]{:S(2)}, u32[]{:S(2)}) collective-permute-start(bf16[32,1024]{1,0:T(8,128)(2,1)S(1)} %get-tuple-element.75), channel_id=1, source_target_pairs={{16,0},{24,8},{0,16},{8,24},{17,1},{25,9},{1,17},{9,25},{18,2},{26... | collective-permute-start | bytes 196616 | tf_op jit(solution)/shard_map/ppermute | solution.py:23
  45.6 4.3 %collective-permute-start.16 = (bf16[32,1024]{1,0:T(8,128)(2,1)S(1)}, bf16[32,1024]{1,0:T(8,128)(2,1)S(1)}, u32[]{:S(2)}, u32[]{:S(2)}) collective-permute-start(bf16[32,1024]{1,0:T(8,128)(2,1)S(1)} %get-tuple-element.73), channel_id=1, source_target_pairs={{8,0},{0,8},{24,16},{16,24},{9,1},{1,9},{25,17},{17,25},{10,2},{2,... | collective-permute-start | bytes 196616 | tf_op jit(solution)/shard_map/ppermute | solution.py:23
  49.9 10.8 %collective-permute-start.21 = (bf16[32,256]{1,0:T(8,128)(2,1)S(1)}, bf16[32,256]{1,0:T(8,128)(2,1)S(1)}, u32[]{:S(2)}, u32[]{:S(2)}) collective-permute-start(bf16[32,256]{1,0:T(8,128)(2,1)S(1)} %get-tuple-element.77), channel_id=1, source_target_pairs={{0,6},{1,7},{2,4},{3,5},{4,2},{5,3},{6,0},{7,1},{8,14},{9,15},{10,... | collective-permute-start | bytes 49160 | tf_op jit(solution)/shard_map/ppermute | solution.py:32
  52.4 8.3 %collective-permute-start.20 = (bf16[32,256]{1,0:T(8,128)(2,1)S(1)}, bf16[32,256]{1,0:T(8,128)(2,1)S(1)}, u32[]{:S(2)}, u32[]{:S(2)}) collective-permute-start(bf16[32,256]{1,0:T(8,128)(2,1)S(1)} %get-tuple-element.78), channel_id=1, source_target_pairs={{0,4},{1,5},{2,6},{3,7},{4,0},{5,1},{6,2},{7,3},{8,12},{9,13},{10,... | collective-permute-start | bytes 49160 | tf_op jit(solution)/shard_map/ppermute | solution.py:32
  52.5 8.2 %collective-permute-start.19 = (bf16[32,256]{1,0:T(8,128)(2,1)S(1)}, bf16[32,256]{1,0:T(8,128)(2,1)S(1)}, u32[]{:S(2)}, u32[]{:S(2)}) collective-permute-start(bf16[32,256]{1,0:T(8,128)(2,1)S(1)} %get-tuple-element.76), channel_id=1, source_target_pairs={{0,2},{1,3},{2,0},{3,1},{4,6},{5,7},{6,4},{7,5},{8,10},{9,11},{10,... | collective-permute-start | bytes 49160 | tf_op jit(solution)/shard_map/ppermute | solution.py:32
  (8 other events, 156.4 us)

commit v3 on v2

--- a/solution.py
+++ b/solution.py
@@ -18,18 +18,28 @@
     return index ^ step if count & (count - 1) == 0 else (index + step) % count
 
 
-def send_ep(block, count, step, back=False):
-    pairs = [(i, partner(count, i, step)) for i in range(count)]
-    return lax.ppermute(block, "ep", [(b, a) for a, b in pairs] if back else pairs)
-
-
-def send_z(block, count, step):
+def hop(block, pairs):
+    return lax.ppermute(block, ("ep", "tp"), pairs)
+
+
+def send_ep(block, ep_count, tp_count, step, cross=False, back=False):
     pairs = [
-        (z * CORES + c, partner(count, z, step) * CORES + c)
-        for z in range(count)
+        (i * tp_count + t, partner(ep_count, i, step) * tp_count + (t ^ cross))
+        for i in range(ep_count)
+        for t in range(tp_count)
+    ]
+    return hop(block, [(b, a) for a, b in pairs] if back else pairs)
+
+
+def send_z(block, ep_count, tp_count, step, cross=False):
+    z_count = tp_count // CORES
+    pairs = [
+        (i * tp_count + z * CORES + c, i * tp_count + partner(z_count, z, step) * CORES + (c ^ cross))
+        for i in range(ep_count)
+        for z in range(z_count)
         for c in range(CORES)
     ]
-    return lax.ppermute(block, "tp", pairs)
+    return hop(block, pairs)
 
 
 def send_core(block, count):
@@ -83,55 +93,16 @@
     return jnp.concatenate(parts, 1)
 
 
-def pack_tokens(ep_count, expert_total, residual, mixer_gain, routes, route_weight):
-    rows, model = residual.shape
-    choices = routes.shape[0]
-    depth = model // ep_count
-    side = -(-2 * expert_total // LANES) * LANES
-
-    def body(res_hbm, gain_hbm, routes_hbm, weight_hbm, *refs):
-        outs, (res_ref, gain_ref, routes_ref, weight_ref, sems) = refs[:ep_count], refs[ep_count:]
-        copies = fetch(
-            (
-                (routes_hbm, routes_ref),
-                (weight_hbm, weight_ref),
-                (gain_hbm, gain_ref),
-                (res_hbm, res_ref),
-            ),
-            sems,
-        )
-        for copy in copies:
-            copy.wait()
-        rank = lax.axis_index("ep")
-        slot = lax.broadcasted_iota(jnp.int32, (side, rows), 0)
-        named = jnp.where(slot < expert_total, slot, slot - expert_total)
-        dense = jnp.zeros((side, rows), F32)
-        for k in range(choices):
-            dense = dense + jnp.where(
-                routes_ref[k : k + 1, :] == named, weight_ref[k : k + 1, :], 0.0
-            )
-        high = dense.astype(BF16).astype(F32)
-        dense = jnp.where(slot < expert_total, high, dense - high).T.astype(BF16)
-        for step, out in enumerate(outs):
-            start = pl.multiple_of(partner(ep_count, rank, step) * depth, LANES)
-            cols = res_ref[:, pl.ds(start, depth)].astype(F32) * gain_ref[:, pl.ds(start, depth)]
-            out[:, :depth] = cols.astype(BF16)
-            out[:, depth:] = dense
-
-    outs = [jax.ShapeDtypeStruct((rows, depth + side), BF16)] * ep_count
-    operands = (residual, mixer_gain, routes, route_weight)
-    scratch = [pltpu.VMEM(x.shape, x.dtype) for x in operands] + [pltpu.SemaphoreType.DMA((4,))]
-    return local_kernel(body, outs, operands, 0, scratch, range(4))
-
-
-def project(blocks, weights):
+def project(blocks, gain, weights):
     rows = blocks[0].shape[0]
     depth, width = weights[0].shape
     count, kinds = len(blocks), len(weights)
 
     def body(*refs):
-        ins, mats, outs = refs[:count], refs[count : count + kinds], refs[count + kinds :]
-        stacked = jnp.concatenate([r[:, :depth] for r in ins], 0)
+        ins, gain_ref, refs = refs[:count], refs[count], refs[count + 1 :]
+        mats, outs = refs[:kinds], refs[kinds:]
+        scaled = [(r[...].astype(F32) * gain_ref[...]).astype(BF16) for r in ins]
+        stacked = jnp.concatenate(scaled, 0)
         for j, mat in enumerate(mats):
             result = jnp.dot(stacked, mat[...], preferred_element_type=F32)
             for i, out in enumerate(outs):
@@ -140,26 +111,33 @@
 
     outs = [jax.ShapeDtypeStruct((rows, kinds * width), BF16 if i else F32) for i in range(count)]
     flops = 2 * rows * count * depth * kinds * width
-    return local_kernel(body, outs, (*blocks, *weights), flops)
-
-
-def head_terms(residual, mixer_gain, step_proj, step_bias, log_rate, skip_gain, conv_state, conv_weight,
-               group_gain, weights, heads, width):
+    return local_kernel(body, outs, (*blocks, gain, *weights), flops)
+
+
+def head_terms(
+    residual, mixer_gain, step_proj, step_bias, log_rate, skip_gain, conv_state, routes, route_weight,
+    conv_weight, group_gain, weights, heads, width, expert_total,
+):
     rows, model = residual.shape
     total = step_proj.shape[0]
     state = LANES
     kinds, taps = conv_weight.shape[:2]
     count = len(weights)
-    fetched = (residual, mixer_gain, step_proj, step_bias, log_rate, skip_gain, conv_state)
+    depth = weights[0].shape[0]
+    side = -(-2 * expert_total // LANES) * LANES
+    fetched = (
+        residual, mixer_gain, step_proj, step_bias, log_rate, skip_gain, conv_state, routes, route_weight,
+    )
 
     def body(*refs):
         sources, refs = refs[: len(fetched)], refs[len(fetched) :]
         tap_hbm, group_hbm, refs = refs[0], refs[1], refs[2:]
         weight_hbm, refs = refs[:count], refs[count:]
         (scale, step, decay, skip, half, old, last, gain_out), refs = refs[:8], refs[8:]
+        (own_out, depth_gain, table_out), refs = refs[:3], refs[3:]
         weight_outs, refs = refs[:count], refs[count:]
         held, (tap_ref, sems) = refs[: len(fetched)], refs[len(fetched) :]
-        res_ref, gain_ref, proj_ref, bias_ref, rate_ref, skip_ref, conv_ref = held
+        res_ref, gain_ref, proj_ref, bias_ref, rate_ref, skip_ref, conv_ref, routes_ref, share_ref = held
         rank = lax.axis_index("tp")
         mine = pl.ds(pl.multiple_of(rank * width, LANES), width)
         copies = fetch(
@@ -202,6 +180,18 @@
                 part = part + conv_ref[k, j].astype(F32) * tap_ref[j, k : k + 1]
             old[j] = part
             last[j : j + 1, :] = tap_ref[j, taps - 1 : taps]
+        owned = pl.ds(pl.multiple_of(lax.axis_index("ep") * depth, LANES), depth)
+        own_out[...] = res_ref[:, owned]
+        depth_gain[...] = gain_ref[:, owned]
+        slot = lax.broadcasted_iota(jnp.int32, (side, rows), 0)
+        named = jnp.where(slot < expert_total, slot, slot - expert_total)
+        table = jnp.zeros((side, rows), F32)
+        for k in range(routes.shape[0]):
+            table = table + jnp.where(
+                routes_ref[k : k + 1, :] == named, share_ref[k : k + 1, :], 0.0
+            )
+        high = table.astype(BF16).astype(F32)
+        table_out[...] = jnp.where(slot < expert_total, high, table - high).T.astype(BF16)
         for copy in copies[local:]:
             copy.wait()
 
@@ -214,6 +204,9 @@
         jax.ShapeDtypeStruct((kinds, rows, width), F32),
         jax.ShapeDtypeStruct((8, width), F32),
         jax.ShapeDtypeStruct((1, width), F32),
+        jax.ShapeDtypeStruct((rows, depth), BF16),
+        jax.ShapeDtypeStruct((1, depth), F32),
+        jax.ShapeDtypeStruct((rows, side), BF16),
         *(jax.ShapeDtypeStruct(w.shape, w.dtype) for w in weights),
     ]
     operands = (*fetched, conv_weight, group_gain, *weights)
@@ -368,14 +361,30 @@
     return local_kernel(body, outs, operands, 8 << 20, scratch, (5,), (0, 1))
 
 
+def column_blocks(width, z_count, kept):
+    rank = lax.axis_index("tp")
+    z, core = rank // CORES, rank % CORES
+    starts = []
+    for step in range(z_count):
+        same = (step == 0) == kept
+        parity = core if same else 1 - core
+        starts.append(pl.multiple_of((partner(z_count, z, step) * CORES + parity) * width, LANES))
+    return starts
+
+
 def dense_branch(mine, other, ffn_gain, gate, up, down, blend):
-    rows, half = mine.shape
-    model = half * CORES
-    width = model // lax.axis_size("tp")
+    rows = mine.shape[0]
+    model = gate.shape[0]
+    half = model // CORES
+    tp_count = lax.axis_size("tp")
+    width = model // tp_count
+    z_count = tp_count // CORES
 
     def body(mine_ref, other_ref, gain_ref, gate_ref, up_ref, down_ref, blend_ref, mine_out, other_out):
         core = lax.axis_index("tp") % CORES
-        values = interleave(mine_ref[...].astype(F32), other_ref[...].astype(F32), core, width)
+        values = interleave(
+            mine_ref[:, :half].astype(F32), other_ref[:, :half].astype(F32), core, width
+        )
         normed = (values * row_scale(values) * gain_ref[...]).astype(BF16)
         gated = jnp.dot(normed, gate_ref[...], preferred_element_type=F32)
         raised = jnp.dot(normed, up_ref[...], preferred_element_type=F32)
@@ -383,55 +392,85 @@
         weight = jax.nn.sigmoid(
             jnp.sum(normed.astype(F32) * blend_ref[...].astype(F32), axis=-1, keepdims=True)
         )
-        result = jnp.dot(hidden, down_ref[...], preferred_element_type=F32) * weight
-        kept, sent = halves(result, core, width)
-        mine_out[...] = kept
-        other_out[...] = sent
+        for kept, out in ((True, mine_out), (False, other_out)):
+            for i, start in enumerate(column_blocks(width, z_count, kept)):
+                part = jnp.dot(hidden, down_ref[:, pl.ds(start, width)], preferred_element_type=F32)
+                out[:, i * width : (i + 1) * width] = part * weight
 
     outs = [jax.ShapeDtypeStruct((rows, half), F32)] * 2
     operands = (mine, other, ffn_gain, gate, up, down, blend)
     return local_kernel(body, outs, operands, 6 * rows * model * gate.shape[1])
 
 
-def run_experts(tokens, ffn_gain, gate, up, down, dense_mine, dense_other, packed, depth):
-    own, rest, _, _ = tokens
-    rows, half = own.shape
-    every = rows + rest.shape[0]
-    model = half * CORES
-    width = model // lax.axis_size("tp")
-    experts = gate.shape[0]
+def down_blocks(hidden, down_ref, width, z_count, kept):
+    ffe = down_ref.shape[1]
+    for i, start in enumerate(column_blocks(width, z_count, kept)):
+        result = None
+        for j in range(down_ref.shape[0]):
+            part = jnp.dot(
+                hidden[:, j * ffe : (j + 1) * ffe],
+                down_ref[j, :, pl.ds(start, width)],
+                preferred_element_type=F32,
+            )
+            result = part if result is None else result + part
+        yield slice(i * width, (i + 1) * width), result
+
+
+def expert_sent(first, second, ffn_gain, gate, up, down, dense_other):
+    count = len(first)
+    rows = first[0].shape[0]
+    experts, model, ffe = gate.shape
+    half = model // CORES
+    tp_count = lax.axis_size("tp")
+    width = model // tp_count
+    z_count = tp_count // CORES
     total = experts * lax.axis_size("ep")
-    count = len(packed)
-
-    def body(own_ref, rest_ref, own2_ref, rest2_ref, gain_ref, gate_ref, up_ref, down_ref, dm, do, *more):
-        packed_refs, (mine_out, other_out) = more[:count], more[count:]
+
+    def body(*refs):
+        mine_refs, other_refs, refs = refs[:count], refs[count : 2 * count], refs[2 * count :]
+        gain_ref, gate_ref, up_ref, down_ref, dense_ref, hidden_out, other_out = refs
         core = lax.axis_index("tp") % CORES
-        first = lax.axis_index("ep") * experts
-        mine = jnp.concatenate([own_ref[...].astype(F32), rest_ref[...].astype(F32)], 0)
-        other = jnp.concatenate([own2_ref[...].astype(F32), rest2_ref[...].astype(F32)], 0)
+        start = lax.axis_index("ep") * experts
+        mine = jnp.concatenate([r[:, :half].astype(F32) for r in mine_refs], 0)
+        other = jnp.concatenate([r[:, :half].astype(F32) for r in other_refs], 0)
         values = interleave(mine, other, core, width)
         normed = (values * row_scale(values) * gain_ref[...]).astype(BF16)
-        weights = jnp.concatenate([r[:, depth:].astype(F32) for r in packed_refs], 0)
-        lane = lax.broadcasted_iota(jnp.int32, weights.shape, 1)
-        result = None
+        table = jnp.concatenate([r[:, half:].astype(F32) for r in mine_refs], 0)
+        lane = lax.broadcasted_iota(jnp.int32, table.shape, 1)
         for j in range(experts):
             gated = jnp.dot(normed, gate_ref[j], preferred_element_type=F32)
             raised = jnp.dot(normed, up_ref[j], preferred_element_type=F32)
-            picked = (lane == first + j) | (lane == first + j + total)
-            share = jnp.sum(jnp.where(picked, weights, 0.0), axis=-1, keepdims=True)
-            hidden = (silu(gated) * raised * share).astype(BF16)
-            part = jnp.dot(hidden, down_ref[j], preferred_element_type=F32)
-            result = part if result is None else result + part
-        kept, sent = halves(result, core, width)
-        mine_out[:rows] = kept[:rows] + dm[...]
-        mine_out[rows:] = kept[rows:]
-        other_out[:rows] = (sent[:rows] + do[...]).astype(BF16)
-        other_out[rows:] = sent[rows:].astype(BF16)
-
-    outs = [jax.ShapeDtypeStruct((every, half), F32), jax.ShapeDtypeStruct((every, half), BF16)]
-    operands = (*tokens, ffn_gain, gate, up, down, dense_mine, dense_other, *packed)
-    flops = 6 * every * model * gate.shape[2] * experts
-    return local_kernel(body, outs, operands, flops)
+            picked = (lane == start + j) | (lane == start + j + total)
+            share = jnp.sum(jnp.where(picked, table, 0.0), axis=-1, keepdims=True)
+            hidden_out[:, j * ffe : (j + 1) * ffe] = (silu(gated) * raised * share).astype(BF16)
+        for cols, part in down_blocks(hidden_out, down_ref, width, z_count, False):
+            other_out[:rows, cols] = (part[:rows] + dense_ref[:, cols]).astype(BF16)
+            other_out[rows:, cols] = part[rows:].astype(BF16)
+
+    every = rows * count
+    outs = [
+        jax.ShapeDtypeStruct((every, experts * ffe), BF16),
+        jax.ShapeDtypeStruct((every, half), BF16),
+    ]
+    operands = (*first, *second, ffn_gain, gate, up, down, dense_other)
+    return local_kernel(body, outs, operands, 5 * every * model * ffe * experts)
+
+
+def expert_kept(hidden, down, dense_mine):
+    every = hidden.shape[0]
+    rows, half = dense_mine.shape
+    tp_count = lax.axis_size("tp")
+    width = half * CORES // tp_count
+    z_count = tp_count // CORES
+
+    def body(hidden_ref, down_ref, dense_ref, out):
+        for cols, part in down_blocks(hidden_ref, down_ref, width, z_count, True):
+            out[:rows, cols] = part[:rows] + dense_ref[:, cols]
+            out[rows:, cols] = part[rows:]
+
+    outs = [jax.ShapeDtypeStruct((every, half), F32)]
+    flops = 2 * every * half * hidden.shape[1]
+    return local_kernel(body, outs, (hidden, down, dense_mine), flops)[0]
 
 
 def layer(
@@ -468,22 +507,27 @@
     z_count = tp_count // CORES
     tp_rank = lax.axis_index("tp")
     z_rank = tp_rank // CORES
+    ep_rank = lax.axis_index("ep")
     ep_steps, z_steps = range(1, ep_count), range(1, z_count)
+    sizes = ep_count, tp_count
     expert_total = expert_gate.shape[0] * ep_count
     as_row = lambda vector: vector.reshape(1, -1)
 
-    packed = pack_tokens(
-        ep_count, expert_total, residual, as_row(mixer_gain), routes.T, route_weight.T
-    )
-    blocks = [packed[0]] + [send_ep(packed[k], ep_count, k) for k in ep_steps]
+    slices = [
+        lax.dynamic_slice_in_dim(residual, partner(ep_count, ep_rank, k) * depth, depth, 1)
+        for k in ep_steps
+    ]
+    blocks = [send_ep(s, *sizes, k, cross=True) for k, s in zip(ep_steps, slices)]
     conv_rows = conv_state.transpose(1, 2, 0, 3)
-    scale, step, decay, skip, resid_half, conv_old, conv_last, gain, *weights = head_terms(
+    (
+        scale, step, decay, skip, resid_half, conv_old, conv_last, gain, own, depth_gain, table, *weights
+    ) = head_terms(
         residual, as_row(mixer_gain), step_proj.T, as_row(step_bias), as_row(log_rate),
-        as_row(skip_gain), conv_rows, conv_weight.transpose(1, 0, 2), as_row(group_gain),
-        (gate_proj, input_proj, write_proj, read_proj), heads, width,
-    )
-    partials = project(blocks, weights)
-    parts = [partials[0]] + [send_ep(partials[k], ep_count, k, back=True) for k in ep_steps]
+        as_row(skip_gain), conv_rows, routes.T, route_weight.T, conv_weight.transpose(1, 0, 2),
+        as_row(group_gain), (gate_proj, input_proj, write_proj, read_proj), heads, width, expert_total,
+    )
+    partials = project((own, *blocks), depth_gain, weights)
+    parts = [partials[0]] + [send_ep(partials[k], *sizes, k, back=True) for k in ep_steps]
     state, out_weight = load((ssm_state, out_proj))
     projected, fed, written, mine, other = mix(
         parts, scale, step, decay, skip, conv_old, conv_last, state, gain, out_weight
@@ -491,34 +535,37 @@
 
     mine = mine + send_core(other, tp_count).astype(F32)
     shared = mine.astype(BF16)
-    gathered = [send_z(shared, z_count, k) for k in z_steps]
+    gathered = [send_z(shared, *sizes, k) for k in z_steps]
     new_state, new_conv = advance_state(state, decay, fed, written, projected, conv_rows)
     new_conv = new_conv.transpose(2, 0, 1, 3)
     for part in gathered:
         mine = mine + part.astype(F32)
     resid_mid = (resid_half.astype(F32) + mine).astype(BF16)
-
-    others = [send_ep(resid_mid, ep_count, k) for k in ep_steps]
-    own_other = send_core(resid_mid, tp_count)
+    packed = jnp.concatenate((resid_mid, table), 1)
+
+    seconds = [send_ep(packed, *sizes, k, cross=True) for k in ep_steps]
+    own_other = send_core(packed, tp_count)
     dense_mine, dense_other = dense_branch(
-        resid_mid, own_other, as_row(ffn_gain), dense_gate, dense_up, dense_down, as_row(blend_weight)
-    )
-    rest = jnp.concatenate(others, 0)
-    rest_other = send_core(rest, tp_count)
-    mine, other = run_experts(
-        (resid_mid, rest, own_other, rest_other), as_row(ffn_gain), expert_gate, expert_up,
-        expert_down, dense_mine, dense_other, blocks, depth,
-    )
-    mine = mine + send_core(other, tp_count).astype(F32)
+        packed, own_other, as_row(ffn_gain), dense_gate, dense_up, dense_down, as_row(blend_weight)
+    )
+    firsts = [send_core(second, tp_count) for second in seconds]
+    hidden, other = expert_sent(
+        (packed, *firsts), (own_other, *seconds), as_row(ffn_gain), expert_gate, expert_up, expert_down,
+        dense_other,
+    )
+    summed = send_core(other, tp_count)
+    mine = expert_kept(hidden, expert_down, dense_mine) + summed.astype(F32)
     total = mine[:rows]
     low = mine.astype(BF16)
     for k in ep_steps:
-        total = total + send_ep(low[k * rows : (k + 1) * rows], ep_count, k, back=True).astype(F32)
-    piece = lambda array, z: lax.dynamic_slice_in_dim(array, z * width, width, 1)
+        piece = low[k * rows : (k + 1) * rows]
+        total = total + send_ep(piece, *sizes, k, back=True).astype(F32)
     low = total.astype(BF16)
-    result = piece(total, z_rank) + piece(resid_mid, z_rank).astype(F32)
+    result = lax.dynamic_slice_in_dim(resid_mid, z_rank * width, width, 1).astype(F32)
+    result = result + total[:, :width]
     for k in z_steps:
-        result = result + send_z(piece(low, partner(z_count, z_rank, k)), z_count, k).astype(F32)
+        piece = low[:, k * width : (k + 1) * width]
+        result = result + send_z(piece, *sizes, k, cross=True).astype(F32)
     return result.astype(BF16), new_state, new_conv
 
 

time: 61.5 us -> 58.4 us (0.950); the launches traced: 61.4 us -> 57.3 us
  waiting for transfers between devices: 19.2 us -> 17 us
  starting transfers between devices: 25 us -> 23.2 us
  Pallas kernels: 13.1 us -> 12.2 us
  local copies, waits for them, and re-layouts: 2.3 us -> 3.09 us
    ppermute x18, starting transfers between devices: 24.1 us -> 21.6 us  [hop(): return lax.ppermute(block, ('ep', 'tp'), pairs)]
    ppermute x18, waiting for transfers between devices: 15.7 us -> 14.4 us  [hop(): return lax.ppermute(block, ('ep', 'tp'), pairs)]
    ppermute x4 -> x6, waiting for transfers between devices: 3.56 us -> 2.61 us  [send_core(): return lax.ppermute(block, 'tp', [(i, i ^ 1) for i in range(count)])]
    pallas_call x8, Pallas kernels: 13.1 us -> 12.2 us  [local_kernel(): call(*(pltpu.with_memory_space_constraint(x, pltpu.HBM) if i in remote el...]
    dynamic_slice x1, local copies, waits for them, and re-layouts: 0.02 us -> 0.81 us  [layer(): lax.dynamic_slice_in_dim(residual, partner(ep_count, ep_rank, k) * depth,...]
    ppermute x4 -> x6, starting transfers between devices: 0.84 us -> 1.55 us  [send_core(): return lax.ppermute(block, 'tp', [(i, i ^ 1) for i in range(count)])]
    unnamed x22 -> x20, local copies, waits for them, and re-layouts: 2.25 us -> 2.25 us
  transfers between devices with their start and end apart: 22 -> 24, of which waited for: 12 -> 11; matrix products, arithmetic and copies ran while one was open for 0% -> 0% of each run, Pallas kernels for 15% -> 17%
where the time goes in v3:
time: 58.4 us; the launch traced here: 57.3 us
  starting transfers between devices  23.2 us (40%)
  waiting for transfers between devices  17 us (29%)
  Pallas kernels  12.2 us (21%)
  local copies, waits for them, and re-layouts  3.09 us (5%)
  between operations  0.97 us (2%)
  other arithmetic  0.81 us (1%)
    ppermute x18, starting transfers between devices, hop(): return lax.ppermute(block, ('ep', 'tp'), pairs)  21.6 us
    ppermute x18, waiting for transfers between devices, hop(): return lax.ppermute(block, ('ep', 'tp'), pairs)  14.4 us
    pallas_call x8, Pallas kernels, local_kernel(): call(*(pltpu.with_memory_space_constraint(x, pltpu.HBM) if i in remote el...  12.2 us
    ppermute x6, waiting for transfers between devices, send_core(): return lax.ppermute(block, 'tp', [(i, i ^ 1) for i in range(count)])  2.61 us
    unnamed x20, local copies, waits for them, and re-layouts  2.25 us
    ppermute x6, starting transfers between devices, send_core(): return lax.ppermute(block, 'tp', [(i, i ^ 1) for i in range(count)])  1.55 us
  transfers between devices with their start and end apart: 24, of which 11 were waited for; matrix products, arithmetic and copies ran while one was open for 0% of the time, Pallas kernels for 17%

profile of v3, /device:TPU:0, one launch (start us, length us, event | category | flops | bytes accessed | tf_op | source)
XLA Modules:
  0.0 57.3 jit_solution(2516599598723004035)
XLA Ops:
  1.5 2.5 %collective-permute-start = (bf16[32,512]{1,0:T(8,128)(2,1)S(1)}, bf16[32,512]{1,0:T(8,128)(2,1)S(1)}, u32[]{:S(2)}, u32[]{:S(2)}) collective-permute-start(bf16[32,512]{1,0:T(8,128)(2,1)S(1)} %get-tuple-element.75), channel_id=1, source_target_pairs={{0,9},{1,8},{2,11},{3,10},{4,13},{5,12},{6,15},{7,14},{8,1},{9,0},... | collective-permute-start | bytes 98312 | tf_op jit(solution)/shard_map/ppermute | solution.py:22
  3.9 1.8 %collective-permute-start.1 = (bf16[32,512]{1,0:T(8,128)(2,1)S(1)}, bf16[32,512]{1,0:T(8,128)(2,1)S(1)}, u32[]{:S(2)}, u32[]{:S(2)}) collective-permute-start(bf16[32,512]{1,0:T(8,128)(2,1)S(1)} %get-tuple-element.76), channel_id=1, source_target_pairs={{0,17},{1,16},{2,19},{3,18},{4,21},{5,20},{6,23},{7,22},{8,25},{9,... | collective-permute-start | bytes 98312 | tf_op jit(solution)/shard_map/ppermute | solution.py:22
  5.7 1.9 %shard_map.256 = (f32[32,128]{1,0:T(8,128)S(1)}, f32[32,256]{1,0:T(8,128)S(1)}, f32[32,512]{1,0:T(8,128)S(1)}, f32[8,256]{1,0:T(8,128)S(1)}, bf16[32,1024]{1,0:T...) custom-call(bf16[32,2048]{1,0:T(8,128)(2,1)} %refs_0_.2, ...), custom_call_target="tpu_custom_call" | custom-call | flops 4194304 | tf_op jit(solution)/shard_map/pallas_call | solution.py:60
  7.6 2.7 %collective-permute-done.2.refs_3_ = bf16[32,512]{1,0:T(8,128)(2,1)S(1)} collective-permute-done((bf16[32,512]{1,0:T(8,128)(2,1)S(1)}, bf16[32,512]{1,0:T(8,128)(2,1)S(1)}, u32[]{:S(2)}, u32[]{:S(2)}) %collective-permute-start.2) | collective-permute-done | bytes 32800 | tf_op jit(solution)/shard_map/ppermute | solution.py:22
  11.2 3.0 %collective-permute-start.5 = (bf16[32,1024]{1,0:T(8,128)(2,1)S(1)}, bf16[32,1024]{1,0:T(8,128)(2,1)S(1)}, u32[]{:S(2)}, u32[]{:S(2)}) collective-permute-start(bf16[32,1024]{1,0:T(8,128)(2,1)S(1)} %get-tuple-element.45), channel_id=1, source_target_pairs={{24,0},{25,1},{26,2},{27,3},{28,4},{29,5},{30,6},{31,7},{16,8},{17... | collective-permute-start | bytes 196616 | tf_op jit(solution)/shard_map/ppermute | solution.py:22
  14.2 2.5 %shard_map.258 = (f32[32,4,64,128]{3,2,1,0:T(8,128)S(1)}, bf16[256,2048]{1,0:T(8,128)(2,1)S(1)}) custom-call(f32[32,4,64,128]{3,2,1,0:T(8,128)} %refs_0_.3, bf16[256,2048]{1,0:T(8,128)(2,1)} %refs_1_.1), custom_call_target="tpu_custom_call" | custom-call | tf_op jit(solution)/shard_map/pallas_call | solution.py:60
  16.8 1.1 %shard_map.259 = (bf16[32,1024]{1,0:T(8,128)(2,1)S(1)}, f32[32,256]{1,0:T(8,128)S(1)}, f32[32,256]{1,0:T(8,128)S(1)}, f32[32,1024]{1,0:T(8,128)S(1)}, bf16[32,1024]{1,0:T(8,128)(2,1)S(1)}) custom-call(f32[32,1024]{1,0:T(8,128)S(1)} %get-tuple-element.42.refs_0_, bf16[32,1024]{1,0:T(8,128)(2,1)S(1)} %collective-permute-done.3.refs_1_, ...), custom_call_target="tpu_custom_call" | custom-call | flops 33554432 | tf_op jit(solution)/shard_map/pallas_call | solution.py:60
  17.9 1.2 %collective-permute-done.6 = bf16[32,1024]{1,0:T(8,128)(2,1)S(1)} collective-permute-done((bf16[32,1024]{1,0:T(8,128)(2,1)S(1)}, bf16[32,1024]{1,0:T(8,128)(2,1)S(1)}, u32[]{:S(2)}, u32[]{:S(2)}) %collective-permute-start.6) | collective-permute-done | bytes 65568 | tf_op jit(solution)/shard_map/ppermute | solution.py:46
  19.2 3.7 %collective-permute-start.9 = (bf16[32,1024]{1,0:T(8,128)(2,1)S(1)}, bf16[32,1024]{1,0:T(8,128)(2,1)S(1)}, u32[]{:S(2)}, u32[]{:S(2)}) collective-permute-start(bf16[32,1024]{1,0:T(8,128)(2,1)S(1)} %fusion.2), channel_id=1, source_target_pairs={{0,6},{1,7},{2,4},{3,5},{4,2},{5,3},{6,0},{7,1},{8,14},{9,15},{10,... | collective-permute-start | bytes 196616 | tf_op jit(solution)/shard_map/ppermute | solution.py:22
  23.6 1.8 %collective-permute-done.9 = bf16[32,1024]{1,0:T(8,128)(2,1)S(1)} collective-permute-done((bf16[32,1024]{1,0:T(8,128)(2,1)S(1)}, bf16[32,1024]{1,0:T(8,128)(2,1)S(1)}, u32[]{:S(2)}, u32[]{:S(2)}) %collective-permute-start.9) | collective-permute-done | bytes 65568 | tf_op jit(solution)/shard_map/ppermute | solution.py:22
  25.5 3.3 %collective-permute-done.8 = bf16[32,1024]{1,0:T(8,128)(2,1)S(1)} collective-permute-done((bf16[32,1024]{1,0:T(8,128)(2,1)S(1)}, bf16[32,1024]{1,0:T(8,128)(2,1)S(1)}, u32[]{:S(2)}, u32[]{:S(2)}) %collective-permute-start.8) | collective-permute-done | bytes 65568 | tf_op jit(solution)/shard_map/ppermute | solution.py:22
  28.8 0.9 %collective-permute-start.10 = (bf16[32,1152]{1,0:T(8,128)(2,1)S(1)}, bf16[32,1152]{1,0:T(8,128)(2,1)S(1)}, u32[]{:S(2)}, u32[]{:S(2)}) collective-permute-start(bf16[32,1152]{1,0:T(8,128)(2,1)S(1)} %pad_maximum_fusion.mine_ref.refs_0_), channel_id=1, source_target_pairs={{0,9},{1,8},{2,11},{3,10},{4,13},{5,12},{6,15},{7,14},{8,1},{9,0},... | collective-permute-start | bytes 221192 | tf_op jit(solution)/shard_map/ppermute | solution.py:22
  29.7 2.0 %collective-permute-start.12 = (bf16[32,1152]{1,0:T(8,128)(2,1)S(1)}, bf16[32,1152]{1,0:T(8,128)(2,1)S(1)}, u32[]{:S(2)}, u32[]{:S(2)}) collective-permute-start(bf16[32,1152]{1,0:T(8,128)(2,1)S(1)} %pad_maximum_fusion.mine_ref.refs_0_), channel_id=1, source_target_pairs={{0,17},{1,16},{2,19},{3,18},{4,21},{5,20},{6,23},{7,22},{8,25},{9,... | collective-permute-start | bytes 221192 | tf_op jit(solution)/shard_map/ppermute | solution.py:22
  32.2 1.2 %collective-permute-done.10.refs_5_ = bf16[32,1152]{1,0:T(8,128)(2,1)S(1)} collective-permute-done((bf16[32,1152]{1,0:T(8,128)(2,1)S(1)}, bf16[32,1152]{1,0:T(8,128)(2,1)S(1)}, u32[]{:S(2)}, u32[]{:S(2)}) %collective-permute-start.10) | collective-permute-done | bytes 73760 | tf_op jit(solution)/shard_map/ppermute | solution.py:22
  34.3 2.7 %collective-permute-done.14.refs_7_ = bf16[32,1152]{1,0:T(8,128)(2,1)S(1)} collective-permute-done((bf16[32,1152]{1,0:T(8,128)(2,1)S(1)}, bf16[32,1152]{1,0:T(8,128)(2,1)S(1)}, u32[]{:S(2)}, u32[]{:S(2)}) %collective-permute-start.14) | collective-permute-done | bytes 73760 | tf_op jit(solution)/shard_map/ppermute | solution.py:22
  38.3 1.2 %shard_map.261 = (bf16[128,512]{1,0:T(8,128)(2,1)S(1)}, bf16[128,1024]{1,0:T(8,128)(2,1)S(1)}) custom-call(bf16[32,1152]{1,0:T(8,128)(2,1)S(1)} %pad_maximum_fusion.mine_ref.refs_0_, bf16[32,1152]{1,0:T(8,128)(2,1)S(1)} %collective-permute-done.11.refs_1_, bf16[32,1152]{1,0:T(8,128)(2,1)S(1)} %collective-permute-done.13.refs_2_, ...), custom_call_target="tpu_custom_call" | custom-call | flops 671088640 | tf_op jit(solution)/shard_map/pallas_call | solution.py:60
  40.1 1.0 %collective-permute-done.17 = bf16[128,1024]{1,0:T(8,128)(2,1)S(1)} collective-permute-done((bf16[128,1024]{1,0:T(8,128)(2,1)S(1)}, bf16[128,1024]{1,0:T(8,128)(2,1)S(1)}, u32[]{:S(2)}, u32[]{:S(2)}) %collective-permute-start.17) | collective-permute-done | bytes 262176 | tf_op jit(solution)/shard_map/ppermute | solution.py:46
  41.7 1.3 %collective-permute-start.19 = (bf16[32,1024]{1,0:T(8,128)(2,1)S(1)}, bf16[32,1024]{1,0:T(8,128)(2,1)S(1)}, u32[]{:S(2)}, u32[]{:S(2)}) collective-permute-start(bf16[32,1024]{1,0:T(8,128)(2,1)S(1)} %get-tuple-element.73), channel_id=1, source_target_pairs={{16,0},{17,1},{18,2},{19,3},{20,4},{21,5},{22,6},{23,7},{24,8},{25... | collective-permute-start | bytes 196616 | tf_op jit(solution)/shard_map/ppermute | solution.py:22
  43.1 1.7 %collective-permute-start.18 = (bf16[32,1024]{1,0:T(8,128)(2,1)S(1)}, bf16[32,1024]{1,0:T(8,128)(2,1)S(1)}, u32[]{:S(2)}, u32[]{:S(2)}) collective-permute-start(bf16[32,1024]{1,0:T(8,128)(2,1)S(1)} %get-tuple-element.71), channel_id=1, source_target_pairs={{8,0},{9,1},{10,2},{11,3},{12,4},{13,5},{14,6},{15,7},{0,8},{1,9},... | collective-permute-start | bytes 196616 | tf_op jit(solution)/shard_map/ppermute | solution.py:22
  44.8 2.3 %collective-permute-done.20 = bf16[32,1024]{1,0:T(8,128)(2,1)S(1)} collective-permute-done((bf16[32,1024]{1,0:T(8,128)(2,1)S(1)}, bf16[32,1024]{1,0:T(8,128)(2,1)S(1)}, u32[]{:S(2)}, u32[]{:S(2)}) %collective-permute-start.20) | collective-permute-done | bytes 65568 | tf_op jit(solution)/shard_map/ppermute | solution.py:22
  47.4 1.5 %collective-permute-start.23 = (bf16[32,256]{1,0:T(8,128)(2,1)S(1)}, bf16[32,256]{1,0:T(8,128)(2,1)S(1)}, u32[]{:S(2)}, u32[]{:S(2)}) collective-permute-start(bf16[32,256]{1,0:T(8,128)(2,1)S(1)} %get-tuple-element.78), channel_id=1, source_target_pairs={{0,7},{1,6},{2,5},{3,4},{4,3},{5,2},{6,1},{7,0},{8,15},{9,14},{10,... | collective-permute-start | bytes 49160 | tf_op jit(solution)/shard_map/ppermute | solution.py:22
  48.9 0.9 %collective-permute-start.22 = (bf16[32,256]{1,0:T(8,128)(2,1)S(1)}, bf16[32,256]{1,0:T(8,128)(2,1)S(1)}, u32[]{:S(2)}, u32[]{:S(2)}) collective-permute-start(bf16[32,256]{1,0:T(8,128)(2,1)S(1)} %get-tuple-element.79), channel_id=1, source_target_pairs={{0,5},{1,4},{2,7},{3,6},{4,1},{5,0},{6,3},{7,2},{8,13},{9,12},{10,... | collective-permute-start | bytes 49160 | tf_op jit(solution)/shard_map/ppermute | solution.py:22
  50.3 2.2 %copy-done.1 = f32[32,4,64,128]{3,2,1,0:T(8,128)S(1)} copy-done((f32[32,4,64,128]{3,2,1,0:T(8,128)S(1)}, f32[32,4,64,128]{3,2,1,0:T(8,128)}, u32[]{:S(2)}) %copy-start.1) | copy-done | bytes 4194328
  52.5 4.1 %shard_map.263 = (f32[32,4,64,128]{3,2,1,0:T(8,128)}, bf16[3,3,32,256]{3,2,1,0:T(8,128)(2,1)}) custom-call(f32[32,4,64,128]{3,2,1,0:T(8,128)S(1)} %copy-done.1, f32[32,512]{1,0:T(8,128)S(1)} %get-tuple-element.48.refs_6_.decay_ref, f32[32,256]{1,0:T(8,128)S(1)} %get-tuple-element.62.fed_ref, f32[32,256]{1,0:T(8,128)S(1)} %get-tuple-element.63.write_ref, ...), custom_call_target="tpu_custom_call" | custom-call | flops 8388608 | tf_op jit(solution)/shard_map/pallas_call | solution.py:60
  (62 shorter events, 7.9 us)
Async XLA Ops:
  1.5 6.2 %collective-permute-start = (bf16[32,512]{1,0:T(8,128)(2,1)S(1)}, bf16[32,512]{1,0:T(8,128)(2,1)S(1)}, u32[]{:S(2)}, u32[]{:S(2)}) collective-permute-start(bf16[32,512]{1,0:T(8,128)(2,1)S(1)} %get-tuple-element.75), channel_id=1, source_target_pairs={{0,9},{1,8},{2,11},{3,10},{4,13},{5,12},{6,15},{7,14},{8,1},{9,0},... | collective-permute-start | bytes 98312 | tf_op jit(solution)/shard_map/ppermute | solution.py:22
  3.9 3.7 %collective-permute-start.1 = (bf16[32,512]{1,0:T(8,128)(2,1)S(1)}, bf16[32,512]{1,0:T(8,128)(2,1)S(1)}, u32[]{:S(2)}, u32[]{:S(2)}) collective-permute-start(bf16[32,512]{1,0:T(8,128)(2,1)S(1)} %get-tuple-element.76), channel_id=1, source_target_pairs={{0,17},{1,16},{2,19},{3,18},{4,21},{5,20},{6,23},{7,22},{8,25},{9,... | collective-permute-start | bytes 98312 | tf_op jit(solution)/shard_map/ppermute | solution.py:22
  5.7 4.6 %collective-permute-start.2 = (bf16[32,512]{1,0:T(8,128)(2,1)S(1)}, bf16[32,512]{1,0:T(8,128)(2,1)S(1)}, u32[]{:S(2)}, u32[]{:S(2)}) collective-permute-start(bf16[32,512]{1,0:T(8,128)(2,1)S(1)} %get-tuple-element.74), channel_id=1, source_target_pairs={{0,25},{1,24},{2,27},{3,26},{4,29},{5,28},{6,31},{7,30},{8,17},{9,... | collective-permute-start | bytes 98312 | tf_op jit(solution)/shard_map/ppermute | solution.py:22
  10.6 6.1 %collective-permute-start.3 = (bf16[32,1024]{1,0:T(8,128)(2,1)S(1)}, bf16[32,1024]{1,0:T(8,128)(2,1)S(1)}, u32[]{:S(2)}, u32[]{:S(2)}) collective-permute-start(bf16[32,1024]{1,0:T(8,128)(2,1)S(1)} %get-tuple-element.43), channel_id=1, source_target_pairs={{8,0},{9,1},{10,2},{11,3},{12,4},{13,5},{14,6},{15,7},{0,8},{1,9},... | collective-permute-start | bytes 196616 | tf_op jit(solution)/shard_map/ppermute | solution.py:22
  11.1 5.7 %collective-permute-start.4 = (bf16[32,1024]{1,0:T(8,128)(2,1)S(1)}, bf16[32,1024]{1,0:T(8,128)(2,1)S(1)}, u32[]{:S(2)}, u32[]{:S(2)}) collective-permute-start(bf16[32,1024]{1,0:T(8,128)(2,1)S(1)} %get-tuple-element.44), channel_id=1, source_target_pairs={{16,0},{17,1},{18,2},{19,3},{20,4},{21,5},{22,6},{23,7},{24,8},{25... | collective-permute-start | bytes 196616 | tf_op jit(solution)/shard_map/ppermute | solution.py:22
  11.2 5.6 %collective-permute-start.5 = (bf16[32,1024]{1,0:T(8,128)(2,1)S(1)}, bf16[32,1024]{1,0:T(8,128)(2,1)S(1)}, u32[]{:S(2)}, u32[]{:S(2)}) collective-permute-start(bf16[32,1024]{1,0:T(8,128)(2,1)S(1)} %get-tuple-element.45), channel_id=1, source_target_pairs={{24,0},{25,1},{26,2},{27,3},{28,4},{29,5},{30,6},{31,7},{16,8},{17... | collective-permute-start | bytes 196616 | tf_op jit(solution)/shard_map/ppermute | solution.py:22
  17.9 1.3 %collective-permute-start.6 = (bf16[32,1024]{1,0:T(8,128)(2,1)S(1)}, bf16[32,1024]{1,0:T(8,128)(2,1)S(1)}, u32[]{:S(2)}, u32[]{:S(2)}) collective-permute-start(bf16[32,1024]{1,0:T(8,128)(2,1)S(1)} %get-tuple-element.56), channel_id=1, source_target_pairs={{0,1},{1,0},{2,3},{3,2},{4,5},{5,4},{6,7},{7,6},{8,9},{9,8},{10,11... | collective-permute-start | bytes 196616 | tf_op jit(solution)/shard_map/ppermute | solution.py:46
  19.2 6.3 %collective-permute-start.9 = (bf16[32,1024]{1,0:T(8,128)(2,1)S(1)}, bf16[32,1024]{1,0:T(8,128)(2,1)S(1)}, u32[]{:S(2)}, u32[]{:S(2)}) collective-permute-start(bf16[32,1024]{1,0:T(8,128)(2,1)S(1)} %fusion.2), channel_id=1, source_target_pairs={{0,6},{1,7},{2,4},{3,5},{4,2},{5,3},{6,0},{7,1},{8,14},{9,15},{10,... | collective-permute-start | bytes 196616 | tf_op jit(solution)/shard_map/ppermute | solution.py:22
  22.9 5.9 %collective-permute-start.8 = (bf16[32,1024]{1,0:T(8,128)(2,1)S(1)}, bf16[32,1024]{1,0:T(8,128)(2,1)S(1)}, u32[]{:S(2)}, u32[]{:S(2)}) collective-permute-start(bf16[32,1024]{1,0:T(8,128)(2,1)S(1)} %fusion.2), channel_id=1, source_target_pairs={{0,4},{1,5},{2,6},{3,7},{4,0},{5,1},{6,2},{7,3},{8,12},{9,13},{10,... | collective-permute-start | bytes 196616 | tf_op jit(solution)/shard_map/ppermute | solution.py:22
  22.9 5.9 %collective-permute-start.7 = (bf16[32,1024]{1,0:T(8,128)(2,1)S(1)}, bf16[32,1024]{1,0:T(8,128)(2,1)S(1)}, u32[]{:S(2)}, u32[]{:S(2)}) collective-permute-start(bf16[32,1024]{1,0:T(8,128)(2,1)S(1)} %fusion.2), channel_id=1, source_target_pairs={{0,2},{1,3},{2,0},{3,1},{4,6},{5,7},{6,4},{7,5},{8,10},{9,11},{10,... | collective-permute-start | bytes 196616 | tf_op jit(solution)/shard_map/ppermute | solution.py:22
  28.8 4.6 %collective-permute-start.10 = (bf16[32,1152]{1,0:T(8,128)(2,1)S(1)}, bf16[32,1152]{1,0:T(8,128)(2,1)S(1)}, u32[]{:S(2)}, u32[]{:S(2)}) collective-permute-start(bf16[32,1152]{1,0:T(8,128)(2,1)S(1)} %pad_maximum_fusion.mine_ref.refs_0_), channel_id=1, source_target_pairs={{0,9},{1,8},{2,11},{3,10},{4,13},{5,12},{6,15},{7,14},{8,1},{9,0},... | collective-permute-start | bytes 221192 | tf_op jit(solution)/shard_map/ppermute | solution.py:22
  29.7 4.1 %collective-permute-start.12 = (bf16[32,1152]{1,0:T(8,128)(2,1)S(1)}, bf16[32,1152]{1,0:T(8,128)(2,1)S(1)}, u32[]{:S(2)}, u32[]{:S(2)}) collective-permute-start(bf16[32,1152]{1,0:T(8,128)(2,1)S(1)} %pad_maximum_fusion.mine_ref.refs_0_), channel_id=1, source_target_pairs={{0,17},{1,16},{2,19},{3,18},{4,21},{5,20},{6,23},{7,22},{8,25},{9,... | collective-permute-start | bytes 221192 | tf_op jit(solution)/shard_map/ppermute | solution.py:22
  31.7 5.3 %collective-permute-start.14 = (bf16[32,1152]{1,0:T(8,128)(2,1)S(1)}, bf16[32,1152]{1,0:T(8,128)(2,1)S(1)}, u32[]{:S(2)}, u32[]{:S(2)}) collective-permute-start(bf16[32,1152]{1,0:T(8,128)(2,1)S(1)} %pad_maximum_fusion.mine_ref.refs_0_), channel_id=1, source_target_pairs={{0,25},{1,24},{2,27},{3,26},{4,29},{5,28},{6,31},{7,30},{8,17},{9,... | collective-permute-start | bytes 221192 | tf_op jit(solution)/shard_map/ppermute | solution.py:22
  31.7 5.4 %collective-permute-start.16 = (bf16[32,1152]{1,0:T(8,128)(2,1)S(1)}, bf16[32,1152]{1,0:T(8,128)(2,1)S(1)}, u32[]{:S(2)}, u32[]{:S(2)}) collective-permute-start(bf16[32,1152]{1,0:T(8,128)(2,1)S(1)} %pad_maximum_fusion.mine_ref.refs_0_), channel_id=1, source_target_pairs={{0,1},{1,0},{2,3},{3,2},{4,5},{5,4},{6,7},{7,6},{8,9},{9,8},{10,11... | collective-permute-start | bytes 221192 | tf_op jit(solution)/shard_map/ppermute | solution.py:46
  33.4 4.5 %collective-permute-start.11 = (bf16[32,1152]{1,0:T(8,128)(2,1)S(1)}, bf16[32,1152]{1,0:T(8,128)(2,1)S(1)}, u32[]{:S(2)}, u32[]{:S(2)}) collective-permute-start(bf16[32,1152]{1,0:T(8,128)(2,1)S(1)} %collective-permute-done.10.refs_5_), channel_id=1, source_target_pairs={{0,1},{1,0},{2,3},{3,2},{4,5},{5,4},{6,7},{7,6},{8,9},{9,8},{10,11... | collective-permute-start | bytes 221192 | tf_op jit(solution)/shard_map/ppermute | solution.py:46
  33.8 4.2 %collective-permute-start.13 = (bf16[32,1152]{1,0:T(8,128)(2,1)S(1)}, bf16[32,1152]{1,0:T(8,128)(2,1)S(1)}, u32[]{:S(2)}, u32[]{:S(2)}) collective-permute-start(bf16[32,1152]{1,0:T(8,128)(2,1)S(1)} %collective-permute-done.12.refs_6_), channel_id=1, source_target_pairs={{0,1},{1,0},{2,3},{3,2},{4,5},{5,4},{6,7},{7,6},{8,9},{9,8},{10,11... | collective-permute-start | bytes 221192 | tf_op jit(solution)/shard_map/ppermute | solution.py:46
  37.0 1.3 %collective-permute-start.15 = (bf16[32,1152]{1,0:T(8,128)(2,1)S(1)}, bf16[32,1152]{1,0:T(8,128)(2,1)S(1)}, u32[]{:S(2)}, u32[]{:S(2)}) collective-permute-start(bf16[32,1152]{1,0:T(8,128)(2,1)S(1)} %collective-permute-done.14.refs_7_), channel_id=1, source_target_pairs={{0,1},{1,0},{2,3},{3,2},{4,5},{5,4},{6,7},{7,6},{8,9},{9,8},{10,11... | collective-permute-start | bytes 221192 | tf_op jit(solution)/shard_map/ppermute | solution.py:46
  39.5 1.6 %collective-permute-start.17 = (bf16[128,1024]{1,0:T(8,128)(2,1)S(1)}, bf16[128,1024]{1,0:T(8,128)(2,1)S(1)}, u32[]{:S(2)}, u32[]{:S(2)}) collective-permute-start(bf16[128,1024]{1,0:T(8,128)(2,1)S(1)} %get-tuple-element.61), channel_id=1, source_target_pairs={{0,1},{1,0},{2,3},{3,2},{4,5},{5,4},{6,7},{7,6},{8,9},{9,8},{10,11... | collective-permute-start | bytes 786440 | tf_op jit(solution)/shard_map/ppermute | solution.py:46
  41.2 5.9 %collective-permute-start.20 = (bf16[32,1024]{1,0:T(8,128)(2,1)S(1)}, bf16[32,1024]{1,0:T(8,128)(2,1)S(1)}, u32[]{:S(2)}, u32[]{:S(2)}) collective-permute-start(bf16[32,1024]{1,0:T(8,128)(2,1)S(1)} %get-tuple-element.72), channel_id=1, source_target_pairs={{24,0},{25,1},{26,2},{27,3},{28,4},{29,5},{30,6},{31,7},{16,8},{17... | collective-permute-start | bytes 196616 | tf_op jit(solution)/shard_map/ppermute | solution.py:22
  41.7 5.4 %collective-permute-start.19 = (bf16[32,1024]{1,0:T(8,128)(2,1)S(1)}, bf16[32,1024]{1,0:T(8,128)(2,1)S(1)}, u32[]{:S(2)}, u32[]{:S(2)}) collective-permute-start(bf16[32,1024]{1,0:T(8,128)(2,1)S(1)} %get-tuple-element.73), channel_id=1, source_target_pairs={{16,0},{17,1},{18,2},{19,3},{20,4},{21,5},{22,6},{23,7},{24,8},{25... | collective-permute-start | bytes 196616 | tf_op jit(solution)/shard_map/ppermute | solution.py:22
  43.1 4.3 %collective-permute-start.18 = (bf16[32,1024]{1,0:T(8,128)(2,1)S(1)}, bf16[32,1024]{1,0:T(8,128)(2,1)S(1)}, u32[]{:S(2)}, u32[]{:S(2)}) collective-permute-start(bf16[32,1024]{1,0:T(8,128)(2,1)S(1)} %get-tuple-element.71), channel_id=1, source_target_pairs={{8,0},{9,1},{10,2},{11,3},{12,4},{13,5},{14,6},{15,7},{0,8},{1,9},... | collective-permute-start | bytes 196616 | tf_op jit(solution)/shard_map/ppermute | solution.py:22
  47.4 9.2 %collective-permute-start.23 = (bf16[32,256]{1,0:T(8,128)(2,1)S(1)}, bf16[32,256]{1,0:T(8,128)(2,1)S(1)}, u32[]{:S(2)}, u32[]{:S(2)}) collective-permute-start(bf16[32,256]{1,0:T(8,128)(2,1)S(1)} %get-tuple-element.78), channel_id=1, source_target_pairs={{0,7},{1,6},{2,5},{3,4},{4,3},{5,2},{6,1},{7,0},{8,15},{9,14},{10,... | collective-permute-start | bytes 49160 | tf_op jit(solution)/shard_map/ppermute | solution.py:22
  48.9 7.8 %collective-permute-start.22 = (bf16[32,256]{1,0:T(8,128)(2,1)S(1)}, bf16[32,256]{1,0:T(8,128)(2,1)S(1)}, u32[]{:S(2)}, u32[]{:S(2)}) collective-permute-start(bf16[32,256]{1,0:T(8,128)(2,1)S(1)} %get-tuple-element.79), channel_id=1, source_target_pairs={{0,5},{1,4},{2,7},{3,6},{4,1},{5,0},{6,3},{7,2},{8,13},{9,12},{10,... | collective-permute-start | bytes 49160 | tf_op jit(solution)/shard_map/ppermute | solution.py:22
  49.8 6.9 %collective-permute-start.21 = (bf16[32,256]{1,0:T(8,128)(2,1)S(1)}, bf16[32,256]{1,0:T(8,128)(2,1)S(1)}, u32[]{:S(2)}, u32[]{:S(2)}) collective-permute-start(bf16[32,256]{1,0:T(8,128)(2,1)S(1)} %get-tuple-element.77), channel_id=1, source_target_pairs={{0,3},{1,2},{2,1},{3,0},{4,7},{5,6},{6,5},{7,4},{8,11},{9,10},{10,... | collective-permute-start | bytes 49160 | tf_op jit(solution)/shard_map/ppermute | solution.py:22
  (10 other events, 189.8 us)

commit v4 on v3

--- a/solution.py
+++ b/solution.py
@@ -84,13 +84,15 @@
     return jnp.where(first, even, odd), jnp.where(first, odd, even)
 
 
-def interleave(mine, other, core, width):
-    first = core == 0
-    even, odd = jnp.where(first, mine, other), jnp.where(first, other, mine)
-    parts = []
-    for i in range(mine.shape[1] // width):
-        parts += [even[:, i * width : (i + 1) * width], odd[:, i * width : (i + 1) * width]]
-    return jnp.concatenate(parts, 1)
+def interleave(joined, mine, other, core, width):
+    for array, parity in ((mine, core), (other, 1 - core)):
+        top = 0
+        for ref in array:
+            rows = ref.shape[0]
+            for i in range(joined.shape[1] // width // CORES):
+                start = pl.multiple_of((i * CORES + parity) * width, LANES)
+                joined[top : top + rows, pl.ds(start, width)] = ref[:, i * width : (i + 1) * width]
+            top += rows
 
 
 def project(blocks, gain, weights):
@@ -126,30 +128,31 @@
     depth = weights[0].shape[0]
     side = -(-2 * expert_total // LANES) * LANES
     fetched = (
-        residual, mixer_gain, step_proj, step_bias, log_rate, skip_gain, conv_state, routes, route_weight,
+        residual, mixer_gain, step_proj, step_bias, log_rate, skip_gain, routes, route_weight,
     )
 
     def body(*refs):
         sources, refs = refs[: len(fetched)], refs[len(fetched) :]
-        tap_hbm, group_hbm, refs = refs[0], refs[1], refs[2:]
+        conv_hbm, tap_hbm, group_hbm, refs = refs[0], refs[1], refs[2], refs[3:]
         weight_hbm, refs = refs[:count], refs[count:]
         (scale, step, decay, skip, half, old, last, gain_out), refs = refs[:8], refs[8:]
-        (own_out, depth_gain, table_out), refs = refs[:3], refs[3:]
+        (own_out, depth_gain, table_out, conv_ref), refs = refs[:4], refs[4:]
         weight_outs, refs = refs[:count], refs[count:]
         held, (tap_ref, sems) = refs[: len(fetched)], refs[len(fetched) :]
-        res_ref, gain_ref, proj_ref, bias_ref, rate_ref, skip_ref, conv_ref, routes_ref, share_ref = held
+        res_ref, gain_ref, proj_ref, bias_ref, rate_ref, skip_ref, routes_ref, share_ref = held
         rank = lax.axis_index("tp")
         mine = pl.ds(pl.multiple_of(rank * width, LANES), width)
         copies = fetch(
             (
                 *zip(sources, held),
+                (conv_hbm, conv_ref),
                 (tap_hbm.at[:, :, mine], tap_ref),
                 (group_hbm.at[:, mine], gain_out),
                 *zip(weight_hbm, weight_outs),
             ),
             sems,
         )
-        local = len(fetched) + 2
+        local = len(fetched) + 3
         for copy in copies[:local]:
             copy.wait()
         head_start = rank * heads
@@ -207,9 +210,10 @@
         jax.ShapeDtypeStruct((rows, depth), BF16),
         jax.ShapeDtypeStruct((1, depth), F32),
         jax.ShapeDtypeStruct((rows, side), BF16),
+        jax.ShapeDtypeStruct(conv_state.shape, conv_state.dtype),
         *(jax.ShapeDtypeStruct(w.shape, w.dtype) for w in weights),
     ]
-    operands = (*fetched, conv_weight, group_gain, *weights)
+    operands = (*fetched, conv_state, conv_weight, group_gain, *weights)
     scratch = [
         *(pltpu.VMEM(x.shape, x.dtype) for x in fetched),
         pltpu.VMEM((kinds, taps, width), F32),
@@ -219,16 +223,32 @@
     return local_kernel(body, outs, operands, flops, scratch, range(len(operands)))
 
 
-def load(arrays):
-    count = len(arrays)
-
-    def body(*refs):
-        for copy in fetch(list(zip(refs[:count], refs[count : 2 * count])), refs[-1]):
+def load_state(ssm_state, out_proj):
+    rows, heads, head_dim, state = ssm_state.shape
+    width = heads * head_dim
+    chunk = 8
+    pieces = rows // chunk
+
+    def body(state_hbm, proj_hbm, state_out, low_out, proj_out, sems):
+        spans = [pl.ds(i * chunk, chunk) for i in range(pieces)]
+        copies = fetch(
+            [(state_hbm.at[s], state_out.at[s]) for s in spans] + [(proj_hbm, proj_out)], sems
+        )
+        for copy, span in zip(copies, spans):
             copy.wait()
-
-    outs = [jax.ShapeDtypeStruct(x.shape, x.dtype) for x in arrays]
-    scratch = [pltpu.SemaphoreType.DMA((count,))]
-    return local_kernel(body, outs, arrays, 0, scratch, range(count))
+            low = state_out[span].reshape(chunk // 2, 2, width, state).astype(BF16)
+            pair = pl.ds(span.start // 2, chunk // 2)
+            low_out[pair, :, :state] = low[:, 0]
+            low_out[pair, :, state:] = low[:, 1]
+        copies[-1].wait()
+
+    outs = [
+        jax.ShapeDtypeStruct(ssm_state.shape, F32),
+        jax.ShapeDtypeStruct((rows // 2, width, 2 * state), BF16),
+        jax.ShapeDtypeStruct(out_proj.shape, out_proj.dtype),
+    ]
+    scratch = [pltpu.SemaphoreType.DMA((pieces + 1,))]
+    return local_kernel(body, outs, (ssm_state, out_proj), 0, scratch, range(2))
 
 
 def silu(values):
@@ -236,8 +256,10 @@
 
 
 def mix(partials, scale, step, decay, skip, conv_old, conv_last, ssm_state, group_gain, out_proj):
-    rows, heads, head_dim, state = ssm_state.shape
-    width = heads * head_dim
+    width, state = ssm_state.shape[1], ssm_state.shape[2] // 2
+    rows = ssm_state.shape[0] * 2
+    heads = decay.shape[1] // state
+    head_dim = width // heads
     model = out_proj.shape[1]
     groups = width // state
     count = len(partials)
@@ -266,17 +288,25 @@
         c_low = c_act.astype(BF16)
         read_buf[...] = c_low.astype(F32)
         lane = lax.broadcasted_iota(jnp.int32, (1, width), 1)
-        for s in range(rows):
-            block = state_ref[s].reshape(width, state).astype(BF16)
-            reads = [read_buf[s : s + 1, g * state : (g + 1) * state] for g in range(groups)]
-            reads = jnp.concatenate(reads + [jnp.zeros((8 - groups, state), F32)], 0).astype(BF16)
+        empty = jnp.zeros((1, state), F32)
+        for s in range(0, rows, 2):
+            reads = []
+            for t in range(2):
+                for g in range(groups):
+                    read = read_buf[s + t : s + t + 1, g * state : (g + 1) * state]
+                    reads.append(jnp.concatenate([empty, read] if t else [read, empty], 1))
+            reads.append(jnp.zeros((8 - 2 * groups, 2 * state), F32))
             found = lax.dot_general(
-                reads, block, (((1,), (1,)), ((), ())), preferred_element_type=F32
+                jnp.concatenate(reads, 0).astype(BF16),
+                state_ref[s // 2],
+                (((1,), (1,)), ((), ())),
+                preferred_element_type=F32,
             )
-            row = found[0:1]
-            for g in range(1, groups):
-                row = jnp.where(lane >= g * state, found[g : g + 1], row)
-            sum_buf[s : s + 1, :] = row
+            for t in range(2):
+                row = found[t * groups : t * groups + 1]
+                for g in range(1, groups):
+                    row = jnp.where(lane >= g * state, found[t * groups + g : t * groups + g + 1], row)
+                sum_buf[s + t : s + t + 1, :] = row
         old_part = sum_buf[...]
         decay_ch = jnp.concatenate(
             [decay_ref[:, h * state : h * state + head_dim] for h in range(heads)], 1
@@ -294,10 +324,12 @@
             cols = slice(g * state, (g + 1) * state)
             mixed.append(gated[:, cols] * row_scale(gated[:, cols]) * gain[:, cols])
         mixed = jnp.concatenate(mixed, 1).astype(BF16)
-        result = jnp.dot(mixed, out_ref[...], preferred_element_type=F32)
-        mine, other = halves(result, rank % CORES, width)
-        mine_out[...] = mine
-        other_out[...] = other.astype(BF16)
+        core = rank % CORES
+        for out, parity in ((other_out, 1 - core), (mine_out, core)):
+            for i in range(model // width // CORES):
+                start = pl.multiple_of((i * CORES + parity) * width, LANES)
+                part = jnp.dot(mixed, out_ref[:, pl.ds(start, width)], preferred_element_type=F32)
+                out[:, i * width : (i + 1) * width] = part.astype(out.dtype)
 
     outs = [
         jax.ShapeDtypeStruct((rows, partials[0].shape[1]), BF16),
@@ -321,10 +353,10 @@
     taps, kinds = conv_state.shape[:2]
     chunk = 8
 
-    def body(state_ref, decay_ref, fed_ref, write_ref, proj_ref, conv_hbm, out_hbm, conv_out, *scratch):
+    def body(state_ref, decay_ref, fed_ref, write_ref, proj_ref, conv_ref, out_hbm, conv_out, *scratch):
         buf, fresh, sems = scratch
         shift = pltpu.make_async_copy(
-            conv_hbm.at[1:], conv_out.at[: taps - 1], sems.at[rows // chunk]
+            conv_ref.at[1:], conv_out.at[: taps - 1], sems.at[rows // chunk]
         )
         shift.start()
         for j in range(kinds):
@@ -358,7 +390,7 @@
         pltpu.SemaphoreType.DMA((rows // chunk + 2,)),
     ]
     operands = (ssm_state, decay, fed, written, projected, conv_state)
-    return local_kernel(body, outs, operands, 8 << 20, scratch, (5,), (0, 1))
+    return local_kernel(body, outs, operands, 8 << 20, scratch, (), (0, 1))
 
 
 def column_blocks(width, z_count, kept):
@@ -380,11 +412,11 @@
     width = model // tp_count
     z_count = tp_count // CORES
 
-    def body(mine_ref, other_ref, gain_ref, gate_ref, up_ref, down_ref, blend_ref, mine_out, other_out):
-        core = lax.axis_index("tp") % CORES
-        values = interleave(
-            mine_ref[:, :half].astype(F32), other_ref[:, :half].astype(F32), core, width
-        )
+    def body(
+        mine_ref, other_ref, gain_ref, gate_ref, up_ref, down_ref, blend_ref, mine_out, other_out, joined
+    ):
+        interleave(joined, [mine_ref], [other_ref], lax.axis_index("tp") % CORES, width)
+        values = joined[...].astype(F32)
         normed = (values * row_scale(values) * gain_ref[...]).astype(BF16)
         gated = jnp.dot(normed, gate_ref[...], preferred_element_type=F32)
         raised = jnp.dot(normed, up_ref[...], preferred_element_type=F32)
@@ -399,7 +431,9 @@
 
     outs = [jax.ShapeDtypeStruct((rows, half), F32)] * 2
     operands = (mine, other, ffn_gain, gate, up, down, blend)
-    return local_kernel(body, outs, operands, 6 * rows * model * gate.shape[1])
+    flops = 6 * rows * model * gate.shape[1]
+    scratch = [pltpu.VMEM((rows, model), BF16)]
+    return local_kernel(body, outs, operands, flops, scratch)
 
 
 def down_blocks(hidden, down_ref, width, z_count, kept):
@@ -416,9 +450,49 @@
         yield slice(i * width, (i + 1) * width), result
 
 
-def expert_sent(first, second, ffn_gain, gate, up, down, dense_other):
+def half_rows(width, core_parity, blocks):
+    return [pl.multiple_of((i * CORES + core_parity) * width, LANES) for i in range(blocks)]
+
+
+def half_product(refs, gain_ref, mats, starts, width):
+    half = width * len(starts)
+    values = jnp.concatenate([r[:, :half] for r in refs], 0).astype(F32)
+    gain = jnp.concatenate([gain_ref[:, pl.ds(s, width)] for s in starts], 1)
+    scaled = (values * gain).astype(BF16)
+    products = []
+    for ref, j in mats:
+        weights = jnp.concatenate([ref[j, pl.ds(s, width), :] for s in starts], 0)
+        products.append(jnp.dot(scaled, weights, preferred_element_type=F32))
+    return products, jnp.sum(values * values, axis=-1, keepdims=True)
+
+
+def expert_first(first, ffn_gain, gate, up, down):
     count = len(first)
-    rows = first[0].shape[0]
+    every = first[0].shape[0] * count
+    experts, model, ffe = gate.shape
+    tp_count = lax.axis_size("tp")
+    width = model // tp_count
+
+    def body(*refs):
+        gain_ref, gate_ref, up_ref, _, partial_out, square_out = refs[count:]
+        starts = half_rows(width, lax.axis_index("tp") % CORES, tp_count // CORES)
+        mats = [(ref, j) for j in range(experts) for ref in (gate_ref, up_ref)]
+        products, squares = half_product(refs[:count], gain_ref, mats, starts, width)
+        for i, product in enumerate(products):
+            partial_out[:, i * ffe : (i + 1) * ffe] = product
+        square_out[...] = jnp.broadcast_to(squares, square_out.shape)
+
+    outs = [
+        jax.ShapeDtypeStruct((every, 2 * experts * ffe), F32),
+        jax.ShapeDtypeStruct((every, LANES), F32),
+    ]
+    flops = 2 * every * model * ffe * experts
+    return local_kernel(body, outs, (*first, ffn_gain, gate, up, down), flops)
+
+
+def expert_sent(partial, squares, tables, second, ffn_gain, gate, up, down, dense_other):
+    count = len(second)
+    rows = second[0].shape[0]
     experts, model, ffe = gate.shape
     half = model // CORES
     tp_count = lax.axis_size("tp")
@@ -426,20 +500,21 @@
     z_count = tp_count // CORES
     total = experts * lax.axis_size("ep")
 
-    def body(*refs):
-        mine_refs, other_refs, refs = refs[:count], refs[count : 2 * count], refs[2 * count :]
+    def body(partial_ref, square_ref, *refs):
+        table_refs, other_refs, refs = refs[:count], refs[count : 2 * count], refs[2 * count :]
         gain_ref, gate_ref, up_ref, down_ref, dense_ref, hidden_out, other_out = refs
-        core = lax.axis_index("tp") % CORES
+        starts = half_rows(width, 1 - lax.axis_index("tp") % CORES, z_count)
+        mats = [(ref, j) for j in range(experts) for ref in (gate_ref, up_ref)]
+        products, others = half_product(other_refs, gain_ref, mats, starts, width)
+        scale = lax.rsqrt((square_ref[:, :1] + others) / model + epsilon)
+        products = [
+            (p + partial_ref[:, i * ffe : (i + 1) * ffe]) * scale for i, p in enumerate(products)
+        ]
         start = lax.axis_index("ep") * experts
-        mine = jnp.concatenate([r[:, :half].astype(F32) for r in mine_refs], 0)
-        other = jnp.concatenate([r[:, :half].astype(F32) for r in other_refs], 0)
-        values = interleave(mine, other, core, width)
-        normed = (values * row_scale(values) * gain_ref[...]).astype(BF16)
-        table = jnp.concatenate([r[:, half:].astype(F32) for r in mine_refs], 0)
+        table = jnp.concatenate([r[:, half:].astype(F32) for r in table_refs], 0)
         lane = lax.broadcasted_iota(jnp.int32, table.shape, 1)
         for j in range(experts):
-            gated = jnp.dot(normed, gate_ref[j], preferred_element_type=F32)
-            raised = jnp.dot(normed, up_ref[j], preferred_element_type=F32)
+            gated, raised = products[2 * j], products[2 * j + 1]
             picked = (lane == start + j) | (lane == start + j + total)
             share = jnp.sum(jnp.where(picked, table, 0.0), axis=-1, keepdims=True)
             hidden_out[:, j * ffe : (j + 1) * ffe] = (silu(gated) * raised * share).astype(BF16)
@@ -452,8 +527,8 @@
         jax.ShapeDtypeStruct((every, experts * ffe), BF16),
         jax.ShapeDtypeStruct((every, half), BF16),
     ]
-    operands = (*first, *second, ffn_gain, gate, up, down, dense_other)
-    return local_kernel(body, outs, operands, 5 * every * model * ffe * experts)
+    operands = (partial, squares, *tables, *second, ffn_gain, gate, up, down, dense_other)
+    return local_kernel(body, outs, operands, 3 * every * model * ffe * experts)
 
 
 def expert_kept(hidden, down, dense_mine):
@@ -520,7 +595,8 @@
     blocks = [send_ep(s, *sizes, k, cross=True) for k, s in zip(ep_steps, slices)]
     conv_rows = conv_state.transpose(1, 2, 0, 3)
     (
-        scale, step, decay, skip, resid_half, conv_old, conv_last, gain, own, depth_gain, table, *weights
+        scale, step, decay, skip, resid_half, conv_old, conv_last, gain, own, depth_gain, table, conv_held,
+        *weights,
     ) = head_terms(
         residual, as_row(mixer_gain), step_proj.T, as_row(step_bias), as_row(log_rate),
         as_row(skip_gain), conv_rows, routes.T, route_weight.T, conv_weight.transpose(1, 0, 2),
@@ -528,30 +604,35 @@
     )
     partials = project((own, *blocks), depth_gain, weights)
     parts = [partials[0]] + [send_ep(partials[k], *sizes, k, back=True) for k in ep_steps]
-    state, out_weight = load((ssm_state, out_proj))
+    state, low_state, out_weight = load_state(ssm_state, out_proj)
     projected, fed, written, mine, other = mix(
-        parts, scale, step, decay, skip, conv_old, conv_last, state, gain, out_weight
+        parts, scale, step, decay, skip, conv_old, conv_last, low_state, gain, out_weight
     )
 
     mine = mine + send_core(other, tp_count).astype(F32)
     shared = mine.astype(BF16)
     gathered = [send_z(shared, *sizes, k) for k in z_steps]
-    new_state, new_conv = advance_state(state, decay, fed, written, projected, conv_rows)
+    new_state, new_conv = advance_state(state, decay, fed, written, projected, conv_held)
     new_conv = new_conv.transpose(2, 0, 1, 3)
     for part in gathered:
         mine = mine + part.astype(F32)
     resid_mid = (resid_half.astype(F32) + mine).astype(BF16)
     packed = jnp.concatenate((resid_mid, table), 1)
 
-    seconds = [send_ep(packed, *sizes, k, cross=True) for k in ep_steps]
+    seconds = [send_ep(packed, *sizes, k) for k in ep_steps]
     own_other = send_core(packed, tp_count)
     dense_mine, dense_other = dense_branch(
         packed, own_other, as_row(ffn_gain), dense_gate, dense_up, dense_down, as_row(blend_weight)
     )
-    firsts = [send_core(second, tp_count) for second in seconds]
+    firsts = []
+    for k, second in zip(ep_steps, seconds):
+        cut = second[:, : resid_mid.shape[1]]
+        firsts.append(send_core(cut, tp_count))
+    tokens = (packed, *seconds)
+    partial, squares = expert_first(tokens, as_row(ffn_gain), expert_gate, expert_up, expert_down)
     hidden, other = expert_sent(
-        (packed, *firsts), (own_other, *seconds), as_row(ffn_gain), expert_gate, expert_up, expert_down,
-        dense_other,
+        partial, squares, tokens, (own_other, *firsts), as_row(ffn_gain), expert_gate, expert_up,
+        expert_down, dense_other,
     )
     summed = send_core(other, tp_count)
     mine = expert_kept(hidden, expert_down, dense_mine) + summed.astype(F32)

time: 58.4 us -> 58 us (level)
  local copies, waits for them, and re-layouts: 3.09 us -> 5.1 us
  Pallas kernels: 12.2 us -> 10.8 us
  waiting for transfers between devices: 17 us -> 16 us
    unnamed x20, local copies, waits for them, and re-layouts: 2.25 us -> 4.24 us
    pallas_call x8 -> x9, Pallas kernels: 12.2 us -> 10.8 us  [local_kernel(): call(*(pltpu.with_memory_space_constraint(x, pltpu.HBM) if i in remote el...]
    ppermute x18, starting transfers between devices: 21.6 us -> 22.3 us  [hop(): return lax.ppermute(block, ('ep', 'tp'), pairs)]
    ppermute x6, starting transfers between devices: 1.55 us -> 0.91 us  [send_core(): return lax.ppermute(block, 'tp', [(i, i ^ 1) for i in range(count)])]
  transfers between devices with their start and end apart: 24 -> 24, of which waited for: 11 -> 11; matrix products, arithmetic and copies ran while one was open for 0% -> 0% of each run, Pallas kernels for 17% -> 15%
where the time goes in v4:
time: 58 us; the launch traced here: 56.9 us
  starting transfers between devices  23.2 us (40%)
  waiting for transfers between devices  16 us (28%)
  Pallas kernels  10.8 us (19%)
  local copies, waits for them, and re-layouts  5.1 us (9%)
  between operations  0.98 us (2%)
  other arithmetic  0.81 us (1%)
    ppermute x18, starting transfers between devices, hop(): return lax.ppermute(block, ('ep', 'tp'), pairs)  22.3 us
    ppermute x18, waiting for transfers between devices, hop(): return lax.ppermute(block, ('ep', 'tp'), pairs)  13.9 us
    pallas_call x9, Pallas kernels, local_kernel(): call(*(pltpu.with_memory_space_constraint(x, pltpu.HBM) if i in remote el...  10.8 us
    unnamed x20, local copies, waits for them, and re-layouts  4.24 us
    ppermute x6, waiting for transfers between devices, send_core(): return lax.ppermute(block, 'tp', [(i, i ^ 1) for i in range(count)])  2.09 us
  transfers between devices with their start and end apart: 24, of which 11 were waited for; matrix products, arithmetic and copies ran while one was open for 0% of the time, Pallas kernels for 15%

profile of v4, /device:TPU:0, one launch (start us, length us, event | category | flops | bytes accessed | tf_op | source)
XLA Modules:
  0.0 56.9 jit_solution(16102209795927191361)
XLA Ops:
  0.7 0.8 %constant_dynamic-slice_fusion = (bf16[32,512]{1,0:T(8,128)(2,1)S(1)}, bf16[32,512]{1,0:T(8,128)(2,1)S(1)}, bf16[32,512]{1,0:T(8,128)(2,1)S(1)}) fusion(bf16[32,2048]{1,0:T(8,128)(2,1)} %refs_0_.1, s32[]{:T(128)S(6)} %select_n.19, s32[]{:T(128)S(6)} %select_n.17, s32[]{:T(128)S(6)} %select_n.18), kind=kLoop, calls=%fused_computation.13 | loop fusion | bytes 196620 | tf_op jit(solution)/shard_map/dynamic_slice | solution.py:592
  1.5 2.5 %collective-permute-start = (bf16[32,512]{1,0:T(8,128)(2,1)S(1)}, bf16[32,512]{1,0:T(8,128)(2,1)S(1)}, u32[]{:S(2)}, u32[]{:S(2)}) collective-permute-start(bf16[32,512]{1,0:T(8,128)(2,1)S(1)} %get-tuple-element.83), channel_id=1, source_target_pairs={{0,9},{1,8},{2,11},{3,10},{4,13},{5,12},{6,15},{7,14},{8,1},{9,0},... | collective-permute-start | bytes 98312 | tf_op jit(solution)/shard_map/ppermute | solution.py:22
  3.9 1.8 %collective-permute-start.1 = (bf16[32,512]{1,0:T(8,128)(2,1)S(1)}, bf16[32,512]{1,0:T(8,128)(2,1)S(1)}, u32[]{:S(2)}, u32[]{:S(2)}) collective-permute-start(bf16[32,512]{1,0:T(8,128)(2,1)S(1)} %get-tuple-element.84), channel_id=1, source_target_pairs={{0,17},{1,16},{2,19},{3,18},{4,21},{5,20},{6,23},{7,22},{8,25},{9,... | collective-permute-start | bytes 98312 | tf_op jit(solution)/shard_map/ppermute | solution.py:22
  5.7 1.9 %shard_map.256 = (f32[32,128]{1,0:T(8,128)S(1)}, f32[32,256]{1,0:T(8,128)S(1)}, f32[32,512]{1,0:T(8,128)S(1)}, f32[8,256]{1,0:T(8,128)S(1)}, bf16[32,1024]{1,0:T...) custom-call(bf16[32,2048]{1,0:T(8,128)(2,1)} %refs_0_.1, ...), custom_call_target="tpu_custom_call" | custom-call | flops 4194304 | tf_op jit(solution)/shard_map/pallas_call | solution.py:60
  7.7 2.6 %collective-permute-done.2.refs_3_ = bf16[32,512]{1,0:T(8,128)(2,1)S(1)} collective-permute-done((bf16[32,512]{1,0:T(8,128)(2,1)S(1)}, bf16[32,512]{1,0:T(8,128)(2,1)S(1)}, u32[]{:S(2)}, u32[]{:S(2)}) %collective-permute-start.2) | collective-permute-done | bytes 32800 | tf_op jit(solution)/shard_map/ppermute | solution.py:22
  11.2 3.0 %collective-permute-start.5 = (bf16[32,1024]{1,0:T(8,128)(2,1)S(1)}, bf16[32,1024]{1,0:T(8,128)(2,1)S(1)}, u32[]{:S(2)}, u32[]{:S(2)}) collective-permute-start(bf16[32,1024]{1,0:T(8,128)(2,1)S(1)} %get-tuple-element.49), channel_id=1, source_target_pairs={{24,0},{25,1},{26,2},{27,3},{28,4},{29,5},{30,6},{31,7},{16,8},{17... | collective-permute-start | bytes 196616 | tf_op jit(solution)/shard_map/ppermute | solution.py:22
  14.2 2.7 %shard_map.258 = (f32[32,4,64,128]{3,2,1,0:T(8,128)S(1)}, bf16[16,256,256]{2,1,0:T(8,128)(2,1)S(1)}, bf16[256,2048]{1,0:T(8,128)(2,1)S(1)}) custom-call(f32[32,4,64,128]{3,2,1,0:T(8,128)} %state_hbm.1, bf16[256,2048]{1,0:T(8,128)(2,1)} %proj_hbm.1), custom_call_target="tpu_custom_call" | custom-call | tf_op jit(solution)/shard_map/pallas_call | solution.py:60
  16.9 2.0 %copy-done.3 = f32[32,4,64,128]{3,2,1,0:T(8,128)} copy-done((f32[32,4,64,128]{3,2,1,0:T(8,128)}, f32[32,4,64,128]{3,2,1,0:T(8,128)S(1)}, u32[]{:S(2)}) %copy-start.3) | copy-done | bytes 4194328
  18.9 1.0 %shard_map.259 = (bf16[32,1024]{1,0:T(8,128)(2,1)S(1)}, f32[32,256]{1,0:T(8,128)S(1)}, f32[32,256]{1,0:T(8,128)S(1)}, f32[32,1024]{1,0:T(8,128)S(1)}, bf16[32,1024]{1,0:T(8,128)(2,1)S(1)}) custom-call(f32[32,1024]{1,0:T(8,128)S(1)} %get-tuple-element.46.refs_0_, bf16[32,1024]{1,0:T(8,128)(2,1)S(1)} %collective-permute-done.3.refs_1_, ...), custom_call_target="tpu_custom_call" | custom-call | flops 33554432 | tf_op jit(solution)/shard_map/pallas_call | solution.py:60
  20.0 1.2 %collective-permute-done.6 = bf16[32,1024]{1,0:T(8,128)(2,1)S(1)} collective-permute-done((bf16[32,1024]{1,0:T(8,128)(2,1)S(1)}, bf16[32,1024]{1,0:T(8,128)(2,1)S(1)}, u32[]{:S(2)}, u32[]{:S(2)}) %collective-permute-start.6) | collective-permute-done | bytes 65568 | tf_op jit(solution)/shard_map/ppermute | solution.py:46
  21.3 3.7 %collective-permute-start.9 = (bf16[32,1024]{1,0:T(8,128)(2,1)S(1)}, bf16[32,1024]{1,0:T(8,128)(2,1)S(1)}, u32[]{:S(2)}, u32[]{:S(2)}) collective-permute-start(bf16[32,1024]{1,0:T(8,128)(2,1)S(1)} %fusion.2), channel_id=1, source_target_pairs={{0,6},{1,7},{2,4},{3,5},{4,2},{5,3},{6,0},{7,1},{8,14},{9,15},{10,... | collective-permute-start | bytes 196616 | tf_op jit(solution)/shard_map/ppermute | solution.py:22
  25.7 1.8 %collective-permute-done.9 = bf16[32,1024]{1,0:T(8,128)(2,1)S(1)} collective-permute-done((bf16[32,1024]{1,0:T(8,128)(2,1)S(1)}, bf16[32,1024]{1,0:T(8,128)(2,1)S(1)}, u32[]{:S(2)}, u32[]{:S(2)}) %collective-permute-start.9) | collective-permute-done | bytes 65568 | tf_op jit(solution)/shard_map/ppermute | solution.py:22
  27.5 3.3 %collective-permute-done.8 = bf16[32,1024]{1,0:T(8,128)(2,1)S(1)} collective-permute-done((bf16[32,1024]{1,0:T(8,128)(2,1)S(1)}, bf16[32,1024]{1,0:T(8,128)(2,1)S(1)}, u32[]{:S(2)}, u32[]{:S(2)}) %collective-permute-start.8) | collective-permute-done | bytes 65568 | tf_op jit(solution)/shard_map/ppermute | solution.py:22
  31.9 2.5 %collective-permute-start.12 = (bf16[32,1152]{1,0:T(8,128)(2,1)S(1)}, bf16[32,1152]{1,0:T(8,128)(2,1)S(1)}, u32[]{:S(2)}, u32[]{:S(2)}) collective-permute-start(bf16[32,1152]{1,0:T(8,128)(2,1)S(1)} %pad_maximum_fusion.refs_0_.mine_ref), channel_id=1, source_target_pairs={{0,24},{1,25},{2,26},{3,27},{4,28},{5,29},{6,30},{7,31},{8,16},{9,... | collective-permute-start | bytes 221192 | tf_op jit(solution)/shard_map/ppermute | solution.py:22
  34.5 1.6 %collective-permute-done.10.refs_1_ = bf16[32,1152]{1,0:T(8,128)(2,1)S(1)} collective-permute-done((bf16[32,1152]{1,0:T(8,128)(2,1)S(1)}, bf16[32,1152]{1,0:T(8,128)(2,1)S(1)}, u32[]{:S(2)}, u32[]{:S(2)}) %collective-permute-start.10) | collective-permute-done | bytes 73760 | tf_op jit(solution)/shard_map/ppermute | solution.py:22
  37.3 0.8 %shard_map.261 = (f32[32,1024]{1,0:T(8,128)S(1)}, f32[32,1024]{1,0:T(8,128)S(1)}) custom-call(bf16[32,1152]{1,0:T(8,128)(2,1)S(1)} %pad_maximum_fusion.refs_0_.mine_ref, bf16[32,1152]{1,0:T(8,128)(2,1)S(1)} %collective-permute-done.13.other_ref.refs_4_, f32[1,2048]{1,0:T(1,128)S(1)} %bitcast.12, bf16[2048,256]{1,0:T(8,128)(2,1)S(1)} %copy-done.5, ...), custom_call_target="tpu_custom_call" | custom-call | flops 100663296 | tf_op jit(solution)/shard_map/pallas_call | solution.py:60
  40.3 0.8 %collective-permute-done.17 = bf16[128,1024]{1,0:T(8,128)(2,1)S(1)} collective-permute-done((bf16[128,1024]{1,0:T(8,128)(2,1)S(1)}, bf16[128,1024]{1,0:T(8,128)(2,1)S(1)}, u32[]{:S(2)}, u32[]{:S(2)}) %collective-permute-start.17) | collective-permute-done | bytes 262176 | tf_op jit(solution)/shard_map/ppermute | solution.py:46
  41.3 2.6 %collective-permute-start.20 = (bf16[32,1024]{1,0:T(8,128)(2,1)S(1)}, bf16[32,1024]{1,0:T(8,128)(2,1)S(1)}, u32[]{:S(2)}, u32[]{:S(2)}) collective-permute-start(bf16[32,1024]{1,0:T(8,128)(2,1)S(1)} %get-tuple-element.80), channel_id=1, source_target_pairs={{24,0},{25,1},{26,2},{27,3},{28,4},{29,5},{30,6},{31,7},{16,8},{17... | collective-permute-start | bytes 196616 | tf_op jit(solution)/shard_map/ppermute | solution.py:22
  44.8 1.8 %collective-permute-done.20 = bf16[32,1024]{1,0:T(8,128)(2,1)S(1)} collective-permute-done((bf16[32,1024]{1,0:T(8,128)(2,1)S(1)}, bf16[32,1024]{1,0:T(8,128)(2,1)S(1)}, u32[]{:S(2)}, u32[]{:S(2)}) %collective-permute-start.20) | collective-permute-done | bytes 65568 | tf_op jit(solution)/shard_map/ppermute | solution.py:22
  46.6 1.5 %collective-permute-done.19 = bf16[32,1024]{1,0:T(8,128)(2,1)S(1)} collective-permute-done((bf16[32,1024]{1,0:T(8,128)(2,1)S(1)}, bf16[32,1024]{1,0:T(8,128)(2,1)S(1)}, u32[]{:S(2)}, u32[]{:S(2)}) %collective-permute-start.19) | collective-permute-done | bytes 65568 | tf_op jit(solution)/shard_map/ppermute | solution.py:22
  48.6 0.8 %collective-permute-start.23 = (bf16[32,256]{1,0:T(8,128)(2,1)S(1)}, bf16[32,256]{1,0:T(8,128)(2,1)S(1)}, u32[]{:S(2)}, u32[]{:S(2)}) collective-permute-start(bf16[32,256]{1,0:T(8,128)(2,1)S(1)} %get-tuple-element.86), channel_id=1, source_target_pairs={{0,7},{1,6},{2,5},{3,4},{4,3},{5,2},{6,1},{7,0},{8,15},{9,14},{10,... | collective-permute-start | bytes 49160 | tf_op jit(solution)/shard_map/ppermute | solution.py:22
  49.4 1.6 %collective-permute-start.22 = (bf16[32,256]{1,0:T(8,128)(2,1)S(1)}, bf16[32,256]{1,0:T(8,128)(2,1)S(1)}, u32[]{:S(2)}, u32[]{:S(2)}) collective-permute-start(bf16[32,256]{1,0:T(8,128)(2,1)S(1)} %get-tuple-element.87), channel_id=1, source_target_pairs={{0,5},{1,4},{2,7},{3,6},{4,1},{5,0},{6,3},{7,2},{8,13},{9,12},{10,... | collective-permute-start | bytes 49160 | tf_op jit(solution)/shard_map/ppermute | solution.py:22
  51.5 2.2 %copy-done.4 = f32[32,4,64,128]{3,2,1,0:T(8,128)S(1)} copy-done((f32[32,4,64,128]{3,2,1,0:T(8,128)S(1)}, f32[32,4,64,128]{3,2,1,0:T(8,128)}, u32[]{:S(2)}) %copy-start.4) | copy-done | bytes 4194328
  53.7 2.5 %shard_map.264 = (f32[32,4,64,128]{3,2,1,0:T(8,128)}, bf16[3,3,32,256]{3,2,1,0:T(8,128)(2,1)}) custom-call(f32[32,4,64,128]{3,2,1,0:T(8,128)S(1)} %copy-done.4, f32[32,512]{1,0:T(8,128)S(1)} %get-tuple-element.52.refs_6_.decay_ref, f32[32,256]{1,0:T(8,128)S(1)} %get-tuple-element.69.fed_ref, f32[32,256]{1,0:T(8,128)S(1)} %get-tuple-element.70.write_ref, ...), custom_call_target="tpu_custom_call" | custom-call | flops 8388608 | tf_op jit(solution)/shard_map/pallas_call | solution.py:60
  (66 shorter events, 9.0 us)
Async XLA Ops:
  1.5 6.2 %collective-permute-start = (bf16[32,512]{1,0:T(8,128)(2,1)S(1)}, bf16[32,512]{1,0:T(8,128)(2,1)S(1)}, u32[]{:S(2)}, u32[]{:S(2)}) collective-permute-start(bf16[32,512]{1,0:T(8,128)(2,1)S(1)} %get-tuple-element.83), channel_id=1, source_target_pairs={{0,9},{1,8},{2,11},{3,10},{4,13},{5,12},{6,15},{7,14},{8,1},{9,0},... | collective-permute-start | bytes 98312 | tf_op jit(solution)/shard_map/ppermute | solution.py:22
  3.9 3.7 %collective-permute-start.1 = (bf16[32,512]{1,0:T(8,128)(2,1)S(1)}, bf16[32,512]{1,0:T(8,128)(2,1)S(1)}, u32[]{:S(2)}, u32[]{:S(2)}) collective-permute-start(bf16[32,512]{1,0:T(8,128)(2,1)S(1)} %get-tuple-element.84), channel_id=1, source_target_pairs={{0,17},{1,16},{2,19},{3,18},{4,21},{5,20},{6,23},{7,22},{8,25},{9,... | collective-permute-start | bytes 98312 | tf_op jit(solution)/shard_map/ppermute | solution.py:22
  5.7 4.6 %collective-permute-start.2 = (bf16[32,512]{1,0:T(8,128)(2,1)S(1)}, bf16[32,512]{1,0:T(8,128)(2,1)S(1)}, u32[]{:S(2)}, u32[]{:S(2)}) collective-permute-start(bf16[32,512]{1,0:T(8,128)(2,1)S(1)} %get-tuple-element.82), channel_id=1, source_target_pairs={{0,25},{1,24},{2,27},{3,26},{4,29},{5,28},{6,31},{7,30},{8,17},{9,... | collective-permute-start | bytes 98312 | tf_op jit(solution)/shard_map/ppermute | solution.py:22
  10.6 8.3 %collective-permute-start.3 = (bf16[32,1024]{1,0:T(8,128)(2,1)S(1)}, bf16[32,1024]{1,0:T(8,128)(2,1)S(1)}, u32[]{:S(2)}, u32[]{:S(2)}) collective-permute-start(bf16[32,1024]{1,0:T(8,128)(2,1)S(1)} %get-tuple-element.47), channel_id=1, source_target_pairs={{8,0},{9,1},{10,2},{11,3},{12,4},{13,5},{14,6},{15,7},{0,8},{1,9},... | collective-permute-start | bytes 196616 | tf_op jit(solution)/shard_map/ppermute | solution.py:22
  11.1 7.8 %collective-permute-start.4 = (bf16[32,1024]{1,0:T(8,128)(2,1)S(1)}, bf16[32,1024]{1,0:T(8,128)(2,1)S(1)}, u32[]{:S(2)}, u32[]{:S(2)}) collective-permute-start(bf16[32,1024]{1,0:T(8,128)(2,1)S(1)} %get-tuple-element.48), channel_id=1, source_target_pairs={{16,0},{17,1},{18,2},{19,3},{20,4},{21,5},{22,6},{23,7},{24,8},{25... | collective-permute-start | bytes 196616 | tf_op jit(solution)/shard_map/ppermute | solution.py:22
  11.2 7.7 %collective-permute-start.5 = (bf16[32,1024]{1,0:T(8,128)(2,1)S(1)}, bf16[32,1024]{1,0:T(8,128)(2,1)S(1)}, u32[]{:S(2)}, u32[]{:S(2)}) collective-permute-start(bf16[32,1024]{1,0:T(8,128)(2,1)S(1)} %get-tuple-element.49), channel_id=1, source_target_pairs={{24,0},{25,1},{26,2},{27,3},{28,4},{29,5},{30,6},{31,7},{16,8},{17... | collective-permute-start | bytes 196616 | tf_op jit(solution)/shard_map/ppermute | solution.py:22
  19.9 1.3 %collective-permute-start.6 = (bf16[32,1024]{1,0:T(8,128)(2,1)S(1)}, bf16[32,1024]{1,0:T(8,128)(2,1)S(1)}, u32[]{:S(2)}, u32[]{:S(2)}) collective-permute-start(bf16[32,1024]{1,0:T(8,128)(2,1)S(1)} %get-tuple-element.60), channel_id=1, source_target_pairs={{0,1},{1,0},{2,3},{3,2},{4,5},{5,4},{6,7},{7,6},{8,9},{9,8},{10,11... | collective-permute-start | bytes 196616 | tf_op jit(solution)/shard_map/ppermute | solution.py:46
  21.3 6.3 %collective-permute-start.9 = (bf16[32,1024]{1,0:T(8,128)(2,1)S(1)}, bf16[32,1024]{1,0:T(8,128)(2,1)S(1)}, u32[]{:S(2)}, u32[]{:S(2)}) collective-permute-start(bf16[32,1024]{1,0:T(8,128)(2,1)S(1)} %fusion.2), channel_id=1, source_target_pairs={{0,6},{1,7},{2,4},{3,5},{4,2},{5,3},{6,0},{7,1},{8,14},{9,15},{10,... | collective-permute-start | bytes 196616 | tf_op jit(solution)/shard_map/ppermute | solution.py:22
  24.9 5.9 %collective-permute-start.8 = (bf16[32,1024]{1,0:T(8,128)(2,1)S(1)}, bf16[32,1024]{1,0:T(8,128)(2,1)S(1)}, u32[]{:S(2)}, u32[]{:S(2)}) collective-permute-start(bf16[32,1024]{1,0:T(8,128)(2,1)S(1)} %fusion.2), channel_id=1, source_target_pairs={{0,4},{1,5},{2,6},{3,7},{4,0},{5,1},{6,2},{7,3},{8,12},{9,13},{10,... | collective-permute-start | bytes 196616 | tf_op jit(solution)/shard_map/ppermute | solution.py:22
  24.9 5.9 %collective-permute-start.7 = (bf16[32,1024]{1,0:T(8,128)(2,1)S(1)}, bf16[32,1024]{1,0:T(8,128)(2,1)S(1)}, u32[]{:S(2)}, u32[]{:S(2)}) collective-permute-start(bf16[32,1024]{1,0:T(8,128)(2,1)S(1)} %fusion.2), channel_id=1, source_target_pairs={{0,2},{1,3},{2,0},{3,1},{4,6},{5,7},{6,4},{7,5},{8,10},{9,11},{10,... | collective-permute-start | bytes 196616 | tf_op jit(solution)/shard_map/ppermute | solution.py:22
  30.9 5.1 %collective-permute-start.10 = (bf16[32,1152]{1,0:T(8,128)(2,1)S(1)}, bf16[32,1152]{1,0:T(8,128)(2,1)S(1)}, u32[]{:S(2)}, u32[]{:S(2)}) collective-permute-start(bf16[32,1152]{1,0:T(8,128)(2,1)S(1)} %pad_maximum_fusion.refs_0_.mine_ref), channel_id=1, source_target_pairs={{0,8},{1,9},{2,10},{3,11},{4,12},{5,13},{6,14},{7,15},{8,0},{9,1},... | collective-permute-start | bytes 221192 | tf_op jit(solution)/shard_map/ppermute | solution.py:22
  31.4 5.0 %collective-permute-start.11 = (bf16[32,1152]{1,0:T(8,128)(2,1)S(1)}, bf16[32,1152]{1,0:T(8,128)(2,1)S(1)}, u32[]{:S(2)}, u32[]{:S(2)}) collective-permute-start(bf16[32,1152]{1,0:T(8,128)(2,1)S(1)} %pad_maximum_fusion.refs_0_.mine_ref), channel_id=1, source_target_pairs={{0,16},{1,17},{2,18},{3,19},{4,20},{5,21},{6,22},{7,23},{8,24},{9,... | collective-permute-start | bytes 221192 | tf_op jit(solution)/shard_map/ppermute | solution.py:22
  31.9 5.3 %collective-permute-start.12 = (bf16[32,1152]{1,0:T(8,128)(2,1)S(1)}, bf16[32,1152]{1,0:T(8,128)(2,1)S(1)}, u32[]{:S(2)}, u32[]{:S(2)}) collective-permute-start(bf16[32,1152]{1,0:T(8,128)(2,1)S(1)} %pad_maximum_fusion.refs_0_.mine_ref), channel_id=1, source_target_pairs={{0,24},{1,25},{2,26},{3,27},{4,28},{5,29},{6,30},{7,31},{8,16},{9,... | collective-permute-start | bytes 221192 | tf_op jit(solution)/shard_map/ppermute | solution.py:22
  34.4 2.8 %collective-permute-start.13 = (bf16[32,1152]{1,0:T(8,128)(2,1)S(1)}, bf16[32,1152]{1,0:T(8,128)(2,1)S(1)}, u32[]{:S(2)}, u32[]{:S(2)}) collective-permute-start(bf16[32,1152]{1,0:T(8,128)(2,1)S(1)} %pad_maximum_fusion.refs_0_.mine_ref), channel_id=1, source_target_pairs={{0,1},{1,0},{2,3},{3,2},{4,5},{5,4},{6,7},{7,6},{8,9},{9,8},{10,11... | collective-permute-start | bytes 221192 | tf_op jit(solution)/shard_map/ppermute | solution.py:46
  36.0 2.6 %collective-permute-start.14 = (bf16[32,1024]{1,0:T(8,128)(2,1)S(1)}, bf16[32,1024]{1,0:T(8,128)(2,1)S(1)}, u32[]{:S(2)}, u32[]{:S(2)}) collective-permute-start(bf16[32,1024]{1,0:T(8,128)(2,1)S(1)} %slice.44), channel_id=1, source_target_pairs={{0,1},{1,0},{2,3},{3,2},{4,5},{5,4},{6,7},{7,6},{8,9},{9,8},{10,11... | collective-permute-start | bytes 196616 | tf_op jit(solution)/shard_map/ppermute | solution.py:46
  36.3 2.3 %collective-permute-start.15 = (bf16[32,1024]{1,0:T(8,128)(2,1)S(1)}, bf16[32,1024]{1,0:T(8,128)(2,1)S(1)}, u32[]{:S(2)}, u32[]{:S(2)}) collective-permute-start(bf16[32,1024]{1,0:T(8,128)(2,1)S(1)} %slice.45), channel_id=1, source_target_pairs={{0,1},{1,0},{2,3},{3,2},{4,5},{5,4},{6,7},{7,6},{8,9},{9,8},{10,11... | collective-permute-start | bytes 196616 | tf_op jit(solution)/shard_map/ppermute | solution.py:46
  37.2 1.5 %collective-permute-start.16 = (bf16[32,1024]{1,0:T(8,128)(2,1)S(1)}, bf16[32,1024]{1,0:T(8,128)(2,1)S(1)}, u32[]{:S(2)}, u32[]{:S(2)}) collective-permute-start(bf16[32,1024]{1,0:T(8,128)(2,1)S(1)} %slice.46), channel_id=1, source_target_pairs={{0,1},{1,0},{2,3},{3,2},{4,5},{5,4},{6,7},{7,6},{8,9},{9,8},{10,11... | collective-permute-start | bytes 196616 | tf_op jit(solution)/shard_map/ppermute | solution.py:46
  39.4 1.7 %collective-permute-start.17 = (bf16[128,1024]{1,0:T(8,128)(2,1)S(1)}, bf16[128,1024]{1,0:T(8,128)(2,1)S(1)}, u32[]{:S(2)}, u32[]{:S(2)}) collective-permute-start(bf16[128,1024]{1,0:T(8,128)(2,1)S(1)} %get-tuple-element.67), channel_id=1, source_target_pairs={{0,1},{1,0},{2,3},{3,2},{4,5},{5,4},{6,7},{7,6},{8,9},{9,8},{10,11... | collective-permute-start | bytes 786440 | tf_op jit(solution)/shard_map/ppermute | solution.py:46
  41.3 5.3 %collective-permute-start.20 = (bf16[32,1024]{1,0:T(8,128)(2,1)S(1)}, bf16[32,1024]{1,0:T(8,128)(2,1)S(1)}, u32[]{:S(2)}, u32[]{:S(2)}) collective-permute-start(bf16[32,1024]{1,0:T(8,128)(2,1)S(1)} %get-tuple-element.80), channel_id=1, source_target_pairs={{24,0},{25,1},{26,2},{27,3},{28,4},{29,5},{30,6},{31,7},{16,8},{17... | collective-permute-start | bytes 196616 | tf_op jit(solution)/shard_map/ppermute | solution.py:22
  43.9 4.3 %collective-permute-start.19 = (bf16[32,1024]{1,0:T(8,128)(2,1)S(1)}, bf16[32,1024]{1,0:T(8,128)(2,1)S(1)}, u32[]{:S(2)}, u32[]{:S(2)}) collective-permute-start(bf16[32,1024]{1,0:T(8,128)(2,1)S(1)} %get-tuple-element.81), channel_id=1, source_target_pairs={{16,0},{17,1},{18,2},{19,3},{20,4},{21,5},{22,6},{23,7},{24,8},{25... | collective-permute-start | bytes 196616 | tf_op jit(solution)/shard_map/ppermute | solution.py:22
  44.3 4.3 %collective-permute-start.18 = (bf16[32,1024]{1,0:T(8,128)(2,1)S(1)}, bf16[32,1024]{1,0:T(8,128)(2,1)S(1)}, u32[]{:S(2)}, u32[]{:S(2)}) collective-permute-start(bf16[32,1024]{1,0:T(8,128)(2,1)S(1)} %get-tuple-element.79), channel_id=1, source_target_pairs={{8,0},{9,1},{10,2},{11,3},{12,4},{13,5},{14,6},{15,7},{0,8},{1,9},... | collective-permute-start | bytes 196616 | tf_op jit(solution)/shard_map/ppermute | solution.py:22
  48.6 7.6 %collective-permute-start.23 = (bf16[32,256]{1,0:T(8,128)(2,1)S(1)}, bf16[32,256]{1,0:T(8,128)(2,1)S(1)}, u32[]{:S(2)}, u32[]{:S(2)}) collective-permute-start(bf16[32,256]{1,0:T(8,128)(2,1)S(1)} %get-tuple-element.86), channel_id=1, source_target_pairs={{0,7},{1,6},{2,5},{3,4},{4,3},{5,2},{6,1},{7,0},{8,15},{9,14},{10,... | collective-permute-start | bytes 49160 | tf_op jit(solution)/shard_map/ppermute | solution.py:22
  49.4 6.8 %collective-permute-start.22 = (bf16[32,256]{1,0:T(8,128)(2,1)S(1)}, bf16[32,256]{1,0:T(8,128)(2,1)S(1)}, u32[]{:S(2)}, u32[]{:S(2)}) collective-permute-start(bf16[32,256]{1,0:T(8,128)(2,1)S(1)} %get-tuple-element.87), channel_id=1, source_target_pairs={{0,5},{1,4},{2,7},{3,6},{4,1},{5,0},{6,3},{7,2},{8,13},{9,12},{10,... | collective-permute-start | bytes 49160 | tf_op jit(solution)/shard_map/ppermute | solution.py:22
  51.0 5.2 %collective-permute-start.21 = (bf16[32,256]{1,0:T(8,128)(2,1)S(1)}, bf16[32,256]{1,0:T(8,128)(2,1)S(1)}, u32[]{:S(2)}, u32[]{:S(2)}) collective-permute-start(bf16[32,256]{1,0:T(8,128)(2,1)S(1)} %get-tuple-element.85), channel_id=1, source_target_pairs={{0,3},{1,2},{2,1},{3,0},{4,7},{5,6},{6,5},{7,4},{8,11},{9,10},{10,... | collective-permute-start | bytes 49160 | tf_op jit(solution)/shard_map/ppermute | solution.py:22
  (10 other events, 139.3 us)

commit v5 on v4

--- a/solution.py
+++ b/solution.py
@@ -82,6 +82,10 @@
     odd = jnp.concatenate([array[:, i * width : (i + 1) * width] for i in range(1, count, 2)], 1)
     first = core == 0
     return jnp.where(first, even, odd), jnp.where(first, odd, even)
+
+
+def half_rows(width, core_parity, blocks):
+    return [pl.multiple_of((i * CORES + core_parity) * width, LANES) for i in range(blocks)]
 
 
 def interleave(joined, mine, other, core, width):
@@ -269,7 +273,7 @@
         (scale_ref, step_ref, decay_ref, skip_ref, old_ref, last_ref, state_ref, gain_ref, out_ref) = refs[
             count : count + 9
         ]
-        proj_out, fed_out, write_out, mine_out, other_out, read_buf, sum_buf = refs[count + 9 :]
+        proj_out, fed_out, write_out, mixed_out, other_out, read_buf, sum_buf = refs[count + 9 :]
         rank = lax.axis_index("tp")
         summed = parts[0][...].astype(F32)
         for part in parts[1:]:
@@ -324,18 +328,16 @@
             cols = slice(g * state, (g + 1) * state)
             mixed.append(gated[:, cols] * row_scale(gated[:, cols]) * gain[:, cols])
         mixed = jnp.concatenate(mixed, 1).astype(BF16)
-        core = rank % CORES
-        for out, parity in ((other_out, 1 - core), (mine_out, core)):
-            for i in range(model // width // CORES):
-                start = pl.multiple_of((i * CORES + parity) * width, LANES)
-                part = jnp.dot(mixed, out_ref[:, pl.ds(start, width)], preferred_element_type=F32)
-                out[:, i * width : (i + 1) * width] = part.astype(out.dtype)
+        mixed_out[...] = mixed
+        for i, start in enumerate(half_rows(width, 1 - rank % CORES, model // width // CORES)):
+            part = jnp.dot(mixed, out_ref[:, pl.ds(start, width)], preferred_element_type=F32)
+            other_out[:, i * width : (i + 1) * width] = part.astype(BF16)
 
     outs = [
         jax.ShapeDtypeStruct((rows, partials[0].shape[1]), BF16),
         jax.ShapeDtypeStruct((rows, width), F32),
         jax.ShapeDtypeStruct((rows, width), F32),
-        jax.ShapeDtypeStruct((rows, model // CORES), F32),
+        jax.ShapeDtypeStruct((rows, width), BF16),
         jax.ShapeDtypeStruct((rows, model // CORES), BF16),
     ]
     operands = (
@@ -343,6 +345,21 @@
     )
     scratch = [pltpu.VMEM((rows, width), F32), pltpu.VMEM((rows, width), F32)]
     return local_kernel(body, outs, operands, 2 * rows * width * model, scratch)
+
+
+def mix_kept(mixed, out_proj):
+    rows, width = mixed.shape
+    model = out_proj.shape[1]
+
+    def body(mixed_ref, out_ref, out):
+        core = lax.axis_index("tp") % CORES
+        for i, start in enumerate(half_rows(width, core, model // width // CORES)):
+            out[:, i * width : (i + 1) * width] = jnp.dot(
+                mixed_ref[...], out_ref[:, pl.ds(start, width)], preferred_element_type=F32
+            )
+
+    outs = [jax.ShapeDtypeStruct((rows, model // CORES), F32)]
+    return local_kernel(body, outs, (mixed, out_proj), rows * width * model)[0]
 
 
 def advance_state(ssm_state, decay, fed, written, projected, conv_state):
@@ -450,10 +467,6 @@
         yield slice(i * width, (i + 1) * width), result
 
 
-def half_rows(width, core_parity, blocks):
-    return [pl.multiple_of((i * CORES + core_parity) * width, LANES) for i in range(blocks)]
-
-
 def half_product(refs, gain_ref, mats, starts, width):
     half = width * len(starts)
     values = jnp.concatenate([r[:, :half] for r in refs], 0).astype(F32)
@@ -490,7 +503,7 @@
     return local_kernel(body, outs, (*first, ffn_gain, gate, up, down), flops)
 
 
-def expert_sent(partial, squares, tables, second, ffn_gain, gate, up, down, dense_other):
+def expert_sent(partial, squares, tables, second, ffn_gain, gate, up, down, dense_mine):
     count = len(second)
     rows = second[0].shape[0]
     experts, model, ffe = gate.shape
@@ -502,7 +515,7 @@
 
     def body(partial_ref, square_ref, *refs):
         table_refs, other_refs, refs = refs[:count], refs[count : 2 * count], refs[2 * count :]
-        gain_ref, gate_ref, up_ref, down_ref, dense_ref, hidden_out, other_out = refs
+        gain_ref, gate_ref, up_ref, down_ref, dense_ref, hidden_out, own_out, other_out = refs
         starts = half_rows(width, 1 - lax.axis_index("tp") % CORES, z_count)
         mats = [(ref, j) for j in range(experts) for ref in (gate_ref, up_ref)]
         products, others = half_product(other_refs, gain_ref, mats, starts, width)
@@ -518,34 +531,38 @@
             picked = (lane == start + j) | (lane == start + j + total)
             share = jnp.sum(jnp.where(picked, table, 0.0), axis=-1, keepdims=True)
             hidden_out[:, j * ffe : (j + 1) * ffe] = (silu(gated) * raised * share).astype(BF16)
-        for cols, part in down_blocks(hidden_out, down_ref, width, z_count, False):
-            other_out[:rows, cols] = (part[:rows] + dense_ref[:, cols]).astype(BF16)
-            other_out[rows:, cols] = part[rows:].astype(BF16)
+        for cols, part in down_blocks(hidden_out, down_ref, width, z_count, True):
+            own_out[:, cols] = part[:rows] + dense_ref[:, cols]
+            other_out[:, cols] = part[rows:].astype(BF16)
 
     every = rows * count
     outs = [
         jax.ShapeDtypeStruct((every, experts * ffe), BF16),
-        jax.ShapeDtypeStruct((every, half), BF16),
-    ]
-    operands = (partial, squares, *tables, *second, ffn_gain, gate, up, down, dense_other)
+        jax.ShapeDtypeStruct((rows, half), F32),
+        jax.ShapeDtypeStruct((every - rows, half), BF16),
+    ]
+    operands = (partial, squares, *tables, *second, ffn_gain, gate, up, down, dense_mine)
     return local_kernel(body, outs, operands, 3 * every * model * ffe * experts)
 
 
-def expert_kept(hidden, down, dense_mine):
+def expert_kept(hidden, down, dense_other):
     every = hidden.shape[0]
-    rows, half = dense_mine.shape
+    rows, half = dense_other.shape
     tp_count = lax.axis_size("tp")
     width = half * CORES // tp_count
     z_count = tp_count // CORES
 
-    def body(hidden_ref, down_ref, dense_ref, out):
-        for cols, part in down_blocks(hidden_ref, down_ref, width, z_count, True):
-            out[:rows, cols] = part[:rows] + dense_ref[:, cols]
-            out[rows:, cols] = part[rows:]
-
-    outs = [jax.ShapeDtypeStruct((every, half), F32)]
+    def body(hidden_ref, down_ref, dense_ref, own_out, out):
+        for cols, part in down_blocks(hidden_ref, down_ref, width, z_count, False):
+            own_out[:, cols] = (part[:rows] + dense_ref[:, cols]).astype(BF16)
+            out[:, cols] = part[rows:]
+
+    outs = [
+        jax.ShapeDtypeStruct((rows, half), BF16),
+        jax.ShapeDtypeStruct((every - rows, half), F32),
+    ]
     flops = 2 * every * half * hidden.shape[1]
-    return local_kernel(body, outs, (hidden, down, dense_mine), flops)[0]
+    return local_kernel(body, outs, (hidden, down, dense_other), flops)
 
 
 def layer(
@@ -605,11 +622,12 @@
     partials = project((own, *blocks), depth_gain, weights)
     parts = [partials[0]] + [send_ep(partials[k], *sizes, k, back=True) for k in ep_steps]
     state, low_state, out_weight = load_state(ssm_state, out_proj)
-    projected, fed, written, mine, other = mix(
+    projected, fed, written, mixed, other = mix(
         parts, scale, step, decay, skip, conv_old, conv_last, low_state, gain, out_weight
     )
 
-    mine = mine + send_core(other, tp_count).astype(F32)
+    summed = send_core(other, tp_count)
+    mine = mix_kept(mixed, out_weight) + summed.astype(F32)
     shared = mine.astype(BF16)
     gathered = [send_z(shared, *sizes, k) for k in z_steps]
     new_state, new_conv = advance_state(state, decay, fed, written, projected, conv_held)
@@ -630,17 +648,17 @@
         firsts.append(send_core(cut, tp_count))
     tokens = (packed, *seconds)
     partial, squares = expert_first(tokens, as_row(ffn_gain), expert_gate, expert_up, expert_down)
-    hidden, other = expert_sent(
+    hidden, total, other = expert_sent(
         partial, squares, tokens, (own_other, *firsts), as_row(ffn_gain), expert_gate, expert_up,
-        expert_down, dense_other,
+        expert_down, dense_mine,
     )
     summed = send_core(other, tp_count)
-    mine = expert_kept(hidden, expert_down, dense_mine) + summed.astype(F32)
-    total = mine[:rows]
-    low = mine.astype(BF16)
+    own_sent, kept = expert_kept(hidden, expert_down, dense_other)
+    low = (kept + summed.astype(F32)).astype(BF16)
+    total = total + send_core(own_sent, tp_count).astype(F32)
     for k in ep_steps:
-        piece = low[k * rows : (k + 1) * rows]
-        total = total + send_ep(piece, *sizes, k, back=True).astype(F32)
+        piece = low[(k - 1) * rows : k * rows]
+        total = total + send_ep(piece, *sizes, k, cross=True, back=True).astype(F32)
     low = total.astype(BF16)
     result = lax.dynamic_slice_in_dim(resid_mid, z_rank * width, width, 1).astype(F32)
     result = result + total[:, :width]

time: 58 us -> 57.3 us (0.988); the launches traced: 56.9 us -> 57.1 us
  starting transfers between devices: 23.2 us -> 24.1 us
  waiting for transfers between devices: 16 us -> 15.3 us
    ppermute x18, starting transfers between devices: 22.3 us -> 23.2 us  [hop(): return lax.ppermute(block, ('ep', 'tp'), pairs)]
    ppermute x6 -> x7, waiting for transfers between devices: 2.09 us -> 1.69 us  [send_core(): return lax.ppermute(block, 'tp', [(i, i ^ 1) for i in range(count)])]
    pallas_call x9 -> x10, Pallas kernels: 10.8 us -> 10.7 us  [local_kernel(): call(*(pltpu.with_memory_space_constraint(x, pltpu.HBM) if i in remote el...]
  transfers between devices with their start and end apart: 24 -> 25, of which waited for: 11 -> 10; matrix products, arithmetic and copies ran while one was open for 0% -> 0% of each run, Pallas kernels for 15% -> 15%
where the time goes in v5:
time: 57.3 us; the launch traced here: 57.1 us
  starting transfers between devices  24.1 us (42%)
  waiting for transfers between devices  15.3 us (27%)
  Pallas kernels  10.7 us (19%)
  local copies, waits for them, and re-layouts  5.1 us (9%)
  between operations  1 us (2%)
  other arithmetic  0.79 us (1%)
    ppermute x18, starting transfers between devices, hop(): return lax.ppermute(block, ('ep', 'tp'), pairs)  23.2 us
    ppermute x18, waiting for transfers between devices, hop(): return lax.ppermute(block, ('ep', 'tp'), pairs)  13.6 us
    pallas_call x10, Pallas kernels, local_kernel(): call(*(pltpu.with_memory_space_constraint(x, pltpu.HBM) if i in remote el...  10.7 us
    unnamed x20, local copies, waits for them, and re-layouts  4.25 us
    ppermute x7, waiting for transfers between devices, send_core(): return lax.ppermute(block, 'tp', [(i, i ^ 1) for i in range(count)])  1.69 us
  transfers between devices with their start and end apart: 25, of which 10 were waited for; matrix products, arithmetic and copies ran while one was open for 0% of the time, Pallas kernels for 15%

profile of v5, /device:TPU:0, one launch (start us, length us, event | category | flops | bytes accessed | tf_op | source)
XLA Modules:
  0.0 57.1 jit_solution(17262870442425992491)
XLA Ops:
  0.7 0.8 %constant_dynamic-slice_fusion = (bf16[32,512]{1,0:T(8,128)(2,1)S(1)}, bf16[32,512]{1,0:T(8,128)(2,1)S(1)}, bf16[32,512]{1,0:T(8,128)(2,1)S(1)}) fusion(bf16[32,2048]{1,0:T(8,128)(2,1)} %refs_0_.1, s32[]{:T(128)S(6)} %select_n.19, s32[]{:T(128)S(6)} %select_n.17, s32[]{:T(128)S(6)} %select_n.18), kind=kLoop, calls=%fused_computation.11 | loop fusion | bytes 196620 | tf_op jit(solution)/shard_map/dynamic_slice | solution.py:609
  1.5 2.5 %collective-permute-start = (bf16[32,512]{1,0:T(8,128)(2,1)S(1)}, bf16[32,512]{1,0:T(8,128)(2,1)S(1)}, u32[]{:S(2)}, u32[]{:S(2)}) collective-permute-start(bf16[32,512]{1,0:T(8,128)(2,1)S(1)} %get-tuple-element.87), channel_id=1, source_target_pairs={{0,9},{1,8},{2,11},{3,10},{4,13},{5,12},{6,15},{7,14},{8,1},{9,0},... | collective-permute-start | bytes 98312 | tf_op jit(solution)/shard_map/ppermute | solution.py:22
  3.9 1.8 %collective-permute-start.1 = (bf16[32,512]{1,0:T(8,128)(2,1)S(1)}, bf16[32,512]{1,0:T(8,128)(2,1)S(1)}, u32[]{:S(2)}, u32[]{:S(2)}) collective-permute-start(bf16[32,512]{1,0:T(8,128)(2,1)S(1)} %get-tuple-element.88), channel_id=1, source_target_pairs={{0,17},{1,16},{2,19},{3,18},{4,21},{5,20},{6,23},{7,22},{8,25},{9,... | collective-permute-start | bytes 98312 | tf_op jit(solution)/shard_map/ppermute | solution.py:22
  5.7 1.9 %shard_map.256 = (f32[32,128]{1,0:T(8,128)S(1)}, f32[32,256]{1,0:T(8,128)S(1)}, f32[32,512]{1,0:T(8,128)S(1)}, f32[8,256]{1,0:T(8,128)S(1)}, bf16[32,1024]{1,0:T...) custom-call(bf16[32,2048]{1,0:T(8,128)(2,1)} %refs_0_.1, ...), custom_call_target="tpu_custom_call" | custom-call | flops 4194304 | tf_op jit(solution)/shard_map/pallas_call | solution.py:60
  7.7 2.6 %collective-permute-done.2.refs_3_ = bf16[32,512]{1,0:T(8,128)(2,1)S(1)} collective-permute-done((bf16[32,512]{1,0:T(8,128)(2,1)S(1)}, bf16[32,512]{1,0:T(8,128)(2,1)S(1)}, u32[]{:S(2)}, u32[]{:S(2)}) %collective-permute-start.2) | collective-permute-done | bytes 32800 | tf_op jit(solution)/shard_map/ppermute | solution.py:22
  11.2 3.0 %collective-permute-start.5 = (bf16[32,1024]{1,0:T(8,128)(2,1)S(1)}, bf16[32,1024]{1,0:T(8,128)(2,1)S(1)}, u32[]{:S(2)}, u32[]{:S(2)}) collective-permute-start(bf16[32,1024]{1,0:T(8,128)(2,1)S(1)} %get-tuple-element.52), channel_id=1, source_target_pairs={{24,0},{25,1},{26,2},{27,3},{28,4},{29,5},{30,6},{31,7},{16,8},{17... | collective-permute-start | bytes 196616 | tf_op jit(solution)/shard_map/ppermute | solution.py:22
  14.2 2.5 %shard_map.258 = (f32[32,4,64,128]{3,2,1,0:T(8,128)S(1)}, bf16[16,256,256]{2,1,0:T(8,128)(2,1)S(1)}, bf16[256,2048]{1,0:T(8,128)(2,1)S(1)}) custom-call(f32[32,4,64,128]{3,2,1,0:T(8,128)} %state_hbm.1, bf16[256,2048]{1,0:T(8,128)(2,1)} %proj_hbm.1), custom_call_target="tpu_custom_call" | custom-call | tf_op jit(solution)/shard_map/pallas_call | solution.py:60
  16.7 2.0 %copy-done.3 = f32[32,4,64,128]{3,2,1,0:T(8,128)} copy-done((f32[32,4,64,128]{3,2,1,0:T(8,128)}, f32[32,4,64,128]{3,2,1,0:T(8,128)S(1)}, u32[]{:S(2)}) %copy-start.3) | copy-done | bytes 4194328
  18.8 0.9 %shard_map.259 = (bf16[32,1024]{1,0:T(8,128)(2,1)S(1)}, f32[32,256]{1,0:T(8,128)S(1)}, f32[32,256]{1,0:T(8,128)S(1)}, bf16[32,256]{1,0:T(8,128)(2,1)S(1)}, bf16[32,1024]{1,0:T(8,128)(2,1)S(1)}) custom-call(f32[32,1024]{1,0:T(8,128)S(1)} %get-tuple-element.49.refs_0_, bf16[32,1024]{1,0:T(8,128)(2,1)S(1)} %collective-permute-done.3.refs_1_, ...), custom_call_target="tpu_custom_call" | custom-call | flops 33554432 | tf_op jit(solution)/shard_map/pallas_call | solution.py:60
  20.0 1.0 %collective-permute-done.6 = bf16[32,1024]{1,0:T(8,128)(2,1)S(1)} collective-permute-done((bf16[32,1024]{1,0:T(8,128)(2,1)S(1)}, bf16[32,1024]{1,0:T(8,128)(2,1)S(1)}, u32[]{:S(2)}, u32[]{:S(2)}) %collective-permute-start.6) | collective-permute-done | bytes 65568 | tf_op jit(solution)/shard_map/ppermute | solution.py:46
  21.1 3.7 %collective-permute-start.9 = (bf16[32,1024]{1,0:T(8,128)(2,1)S(1)}, bf16[32,1024]{1,0:T(8,128)(2,1)S(1)}, u32[]{:S(2)}, u32[]{:S(2)}) collective-permute-start(bf16[32,1024]{1,0:T(8,128)(2,1)S(1)} %fusion), channel_id=1, source_target_pairs={{0,6},{1,7},{2,4},{3,5},{4,2},{5,3},{6,0},{7,1},{8,14},{9,15},{10,... | collective-permute-start | bytes 196616 | tf_op jit(solution)/shard_map/ppermute | solution.py:22
  25.5 1.8 %collective-permute-done.9 = bf16[32,1024]{1,0:T(8,128)(2,1)S(1)} collective-permute-done((bf16[32,1024]{1,0:T(8,128)(2,1)S(1)}, bf16[32,1024]{1,0:T(8,128)(2,1)S(1)}, u32[]{:S(2)}, u32[]{:S(2)}) %collective-permute-start.9) | collective-permute-done | bytes 65568 | tf_op jit(solution)/shard_map/ppermute | solution.py:22
  27.3 3.3 %collective-permute-done.8 = bf16[32,1024]{1,0:T(8,128)(2,1)S(1)} collective-permute-done((bf16[32,1024]{1,0:T(8,128)(2,1)S(1)}, bf16[32,1024]{1,0:T(8,128)(2,1)S(1)}, u32[]{:S(2)}, u32[]{:S(2)}) %collective-permute-start.8) | collective-permute-done | bytes 65568 | tf_op jit(solution)/shard_map/ppermute | solution.py:22
  31.9 2.4 %collective-permute-start.12 = (bf16[32,1152]{1,0:T(8,128)(2,1)S(1)}, bf16[32,1152]{1,0:T(8,128)(2,1)S(1)}, u32[]{:S(2)}, u32[]{:S(2)}) collective-permute-start(bf16[32,1152]{1,0:T(8,128)(2,1)S(1)} %pad_maximum_fusion.refs_0_.mine_ref), channel_id=1, source_target_pairs={{0,24},{1,25},{2,26},{3,27},{4,28},{5,29},{6,30},{7,31},{8,16},{9,... | collective-permute-start | bytes 221192 | tf_op jit(solution)/shard_map/ppermute | solution.py:22
  34.3 1.6 %collective-permute-done.10.refs_1_ = bf16[32,1152]{1,0:T(8,128)(2,1)S(1)} collective-permute-done((bf16[32,1152]{1,0:T(8,128)(2,1)S(1)}, bf16[32,1152]{1,0:T(8,128)(2,1)S(1)}, u32[]{:S(2)}, u32[]{:S(2)}) %collective-permute-start.10) | collective-permute-done | bytes 73760 | tf_op jit(solution)/shard_map/ppermute | solution.py:22
  37.2 0.8 %shard_map.262 = (f32[32,1024]{1,0:T(8,128)S(1)}, f32[32,1024]{1,0:T(8,128)S(1)}) custom-call(bf16[32,1152]{1,0:T(8,128)(2,1)S(1)} %pad_maximum_fusion.refs_0_.mine_ref, bf16[32,1152]{1,0:T(8,128)(2,1)S(1)} %collective-permute-done.13.other_ref.refs_4_, f32[1,2048]{1,0:T(1,128)S(1)} %bitcast.12, bf16[2048,256]{1,0:T(8,128)(2,1)S(1)} %copy-done.5, ...), custom_call_target="tpu_custom_call" | custom-call | flops 100663296 | tf_op jit(solution)/shard_map/pallas_call | solution.py:60
  38.6 0.8 %shard_map.263 = (bf16[128,512]{1,0:T(8,128)(2,1)S(1)}, f32[32,1024]{1,0:T(8,128)S(1)}, bf16[96,1024]{1,0:T(8,128)(2,1)S(1)}) custom-call(f32[128,1024]{1,0:T(8,128)S(1)} %get-tuple-element.65.partial_ref, f32[128,128]{1,0:T(8,128)S(1)} %get-tuple-element.66.square_ref, bf16[32,1152]{1,0:T(8,128)(2,1)S(1)} %pad_maximum_fusion.refs_0_.mine_ref, ...), custom_call_target="tpu_custom_call" | custom-call | flops 402653184 | tf_op jit(solution)/shard_map/pallas_call | solution.py:60
  41.1 2.4 %collective-permute-start.21 = (bf16[32,1024]{1,0:T(8,128)(2,1)S(1)}, bf16[32,1024]{1,0:T(8,128)(2,1)S(1)}, u32[]{:S(2)}, u32[]{:S(2)}) collective-permute-start(bf16[32,1024]{1,0:T(8,128)(2,1)S(1)} %get-tuple-element.84), channel_id=1, source_target_pairs={{25,0},{24,1},{27,2},{26,3},{29,4},{28,5},{31,6},{30,7},{17,8},{16... | collective-permute-start | bytes 196616 | tf_op jit(solution)/shard_map/ppermute | solution.py:22
  44.4 1.6 %collective-permute-done.21 = bf16[32,1024]{1,0:T(8,128)(2,1)S(1)} collective-permute-done((bf16[32,1024]{1,0:T(8,128)(2,1)S(1)}, bf16[32,1024]{1,0:T(8,128)(2,1)S(1)}, u32[]{:S(2)}, u32[]{:S(2)}) %collective-permute-start.21) | collective-permute-done | bytes 65568 | tf_op jit(solution)/shard_map/ppermute | solution.py:22
  46.0 1.6 %collective-permute-done.20 = bf16[32,1024]{1,0:T(8,128)(2,1)S(1)} collective-permute-done((bf16[32,1024]{1,0:T(8,128)(2,1)S(1)}, bf16[32,1024]{1,0:T(8,128)(2,1)S(1)}, u32[]{:S(2)}, u32[]{:S(2)}) %collective-permute-start.20) | collective-permute-done | bytes 65568 | tf_op jit(solution)/shard_map/ppermute | solution.py:22
  47.6 2.5 %collective-permute-start.24 = (bf16[32,256]{1,0:T(8,128)(2,1)S(1)}, bf16[32,256]{1,0:T(8,128)(2,1)S(1)}, u32[]{:S(2)}, u32[]{:S(2)}) collective-permute-start(bf16[32,256]{1,0:T(8,128)(2,1)S(1)} %get-tuple-element.90), channel_id=1, source_target_pairs={{0,7},{1,6},{2,5},{3,4},{4,3},{5,2},{6,1},{7,0},{8,15},{9,14},{10,... | collective-permute-start | bytes 49160 | tf_op jit(solution)/shard_map/ppermute | solution.py:22
  50.1 1.6 %collective-permute-start.22 = (bf16[32,256]{1,0:T(8,128)(2,1)S(1)}, bf16[32,256]{1,0:T(8,128)(2,1)S(1)}, u32[]{:S(2)}, u32[]{:S(2)}) collective-permute-start(bf16[32,256]{1,0:T(8,128)(2,1)S(1)} %get-tuple-element.89), channel_id=1, source_target_pairs={{0,3},{1,2},{2,1},{3,0},{4,7},{5,6},{6,5},{7,4},{8,11},{9,10},{10,... | collective-permute-start | bytes 49160 | tf_op jit(solution)/shard_map/ppermute | solution.py:22
  51.8 2.2 %copy-done.4 = f32[32,4,64,128]{3,2,1,0:T(8,128)S(1)} copy-done((f32[32,4,64,128]{3,2,1,0:T(8,128)S(1)}, f32[32,4,64,128]{3,2,1,0:T(8,128)}, u32[]{:S(2)}) %copy-start.4) | copy-done | bytes 4194328
  53.9 2.5 %shard_map.265 = (f32[32,4,64,128]{3,2,1,0:T(8,128)}, bf16[3,3,32,256]{3,2,1,0:T(8,128)(2,1)}) custom-call(f32[32,4,64,128]{3,2,1,0:T(8,128)S(1)} %copy-done.4, f32[32,512]{1,0:T(8,128)S(1)} %get-tuple-element.55.refs_6_.decay_ref, f32[32,256]{1,0:T(8,128)S(1)} %get-tuple-element.75.fed_ref, f32[32,256]{1,0:T(8,128)S(1)} %get-tuple-element.76.write_ref, ...), custom_call_target="tpu_custom_call" | custom-call | flops 8388608 | tf_op jit(solution)/shard_map/pallas_call | solution.py:60
  (69 shorter events, 8.3 us)
Async XLA Ops:
  1.5 6.2 %collective-permute-start = (bf16[32,512]{1,0:T(8,128)(2,1)S(1)}, bf16[32,512]{1,0:T(8,128)(2,1)S(1)}, u32[]{:S(2)}, u32[]{:S(2)}) collective-permute-start(bf16[32,512]{1,0:T(8,128)(2,1)S(1)} %get-tuple-element.87), channel_id=1, source_target_pairs={{0,9},{1,8},{2,11},{3,10},{4,13},{5,12},{6,15},{7,14},{8,1},{9,0},... | collective-permute-start | bytes 98312 | tf_op jit(solution)/shard_map/ppermute | solution.py:22
  3.9 3.7 %collective-permute-start.1 = (bf16[32,512]{1,0:T(8,128)(2,1)S(1)}, bf16[32,512]{1,0:T(8,128)(2,1)S(1)}, u32[]{:S(2)}, u32[]{:S(2)}) collective-permute-start(bf16[32,512]{1,0:T(8,128)(2,1)S(1)} %get-tuple-element.88), channel_id=1, source_target_pairs={{0,17},{1,16},{2,19},{3,18},{4,21},{5,20},{6,23},{7,22},{8,25},{9,... | collective-permute-start | bytes 98312 | tf_op jit(solution)/shard_map/ppermute | solution.py:22
  5.7 4.6 %collective-permute-start.2 = (bf16[32,512]{1,0:T(8,128)(2,1)S(1)}, bf16[32,512]{1,0:T(8,128)(2,1)S(1)}, u32[]{:S(2)}, u32[]{:S(2)}) collective-permute-start(bf16[32,512]{1,0:T(8,128)(2,1)S(1)} %get-tuple-element.86), channel_id=1, source_target_pairs={{0,25},{1,24},{2,27},{3,26},{4,29},{5,28},{6,31},{7,30},{8,17},{9,... | collective-permute-start | bytes 98312 | tf_op jit(solution)/shard_map/ppermute | solution.py:22
  10.6 8.1 %collective-permute-start.3 = (bf16[32,1024]{1,0:T(8,128)(2,1)S(1)}, bf16[32,1024]{1,0:T(8,128)(2,1)S(1)}, u32[]{:S(2)}, u32[]{:S(2)}) collective-permute-start(bf16[32,1024]{1,0:T(8,128)(2,1)S(1)} %get-tuple-element.50), channel_id=1, source_target_pairs={{8,0},{9,1},{10,2},{11,3},{12,4},{13,5},{14,6},{15,7},{0,8},{1,9},... | collective-permute-start | bytes 196616 | tf_op jit(solution)/shard_map/ppermute | solution.py:22
  11.1 7.6 %collective-permute-start.4 = (bf16[32,1024]{1,0:T(8,128)(2,1)S(1)}, bf16[32,1024]{1,0:T(8,128)(2,1)S(1)}, u32[]{:S(2)}, u32[]{:S(2)}) collective-permute-start(bf16[32,1024]{1,0:T(8,128)(2,1)S(1)} %get-tuple-element.51), channel_id=1, source_target_pairs={{16,0},{17,1},{18,2},{19,3},{20,4},{21,5},{22,6},{23,7},{24,8},{25... | collective-permute-start | bytes 196616 | tf_op jit(solution)/shard_map/ppermute | solution.py:22
  11.2 7.5 %collective-permute-start.5 = (bf16[32,1024]{1,0:T(8,128)(2,1)S(1)}, bf16[32,1024]{1,0:T(8,128)(2,1)S(1)}, u32[]{:S(2)}, u32[]{:S(2)}) collective-permute-start(bf16[32,1024]{1,0:T(8,128)(2,1)S(1)} %get-tuple-element.52), channel_id=1, source_target_pairs={{24,0},{25,1},{26,2},{27,3},{28,4},{29,5},{30,6},{31,7},{16,8},{17... | collective-permute-start | bytes 196616 | tf_op jit(solution)/shard_map/ppermute | solution.py:22
  21.1 6.3 %collective-permute-start.9 = (bf16[32,1024]{1,0:T(8,128)(2,1)S(1)}, bf16[32,1024]{1,0:T(8,128)(2,1)S(1)}, u32[]{:S(2)}, u32[]{:S(2)}) collective-permute-start(bf16[32,1024]{1,0:T(8,128)(2,1)S(1)} %fusion), channel_id=1, source_target_pairs={{0,6},{1,7},{2,4},{3,5},{4,2},{5,3},{6,0},{7,1},{8,14},{9,15},{10,... | collective-permute-start | bytes 196616 | tf_op jit(solution)/shard_map/ppermute | solution.py:22
  24.7 5.9 %collective-permute-start.8 = (bf16[32,1024]{1,0:T(8,128)(2,1)S(1)}, bf16[32,1024]{1,0:T(8,128)(2,1)S(1)}, u32[]{:S(2)}, u32[]{:S(2)}) collective-permute-start(bf16[32,1024]{1,0:T(8,128)(2,1)S(1)} %fusion), channel_id=1, source_target_pairs={{0,4},{1,5},{2,6},{3,7},{4,0},{5,1},{6,2},{7,3},{8,12},{9,13},{10,... | collective-permute-start | bytes 196616 | tf_op jit(solution)/shard_map/ppermute | solution.py:22
  24.7 5.9 %collective-permute-start.7 = (bf16[32,1024]{1,0:T(8,128)(2,1)S(1)}, bf16[32,1024]{1,0:T(8,128)(2,1)S(1)}, u32[]{:S(2)}, u32[]{:S(2)}) collective-permute-start(bf16[32,1024]{1,0:T(8,128)(2,1)S(1)} %fusion), channel_id=1, source_target_pairs={{0,2},{1,3},{2,0},{3,1},{4,6},{5,7},{6,4},{7,5},{8,10},{9,11},{10,... | collective-permute-start | bytes 196616 | tf_op jit(solution)/shard_map/ppermute | solution.py:22
  30.7 5.1 %collective-permute-start.10 = (bf16[32,1152]{1,0:T(8,128)(2,1)S(1)}, bf16[32,1152]{1,0:T(8,128)(2,1)S(1)}, u32[]{:S(2)}, u32[]{:S(2)}) collective-permute-start(bf16[32,1152]{1,0:T(8,128)(2,1)S(1)} %pad_maximum_fusion.refs_0_.mine_ref), channel_id=1, source_target_pairs={{0,8},{1,9},{2,10},{3,11},{4,12},{5,13},{6,14},{7,15},{8,0},{9,1},... | collective-permute-start | bytes 221192 | tf_op jit(solution)/shard_map/ppermute | solution.py:22
  31.2 5.0 %collective-permute-start.11 = (bf16[32,1152]{1,0:T(8,128)(2,1)S(1)}, bf16[32,1152]{1,0:T(8,128)(2,1)S(1)}, u32[]{:S(2)}, u32[]{:S(2)}) collective-permute-start(bf16[32,1152]{1,0:T(8,128)(2,1)S(1)} %pad_maximum_fusion.refs_0_.mine_ref), channel_id=1, source_target_pairs={{0,16},{1,17},{2,18},{3,19},{4,20},{5,21},{6,22},{7,23},{8,24},{9,... | collective-permute-start | bytes 221192 | tf_op jit(solution)/shard_map/ppermute | solution.py:22
  31.9 5.3 %collective-permute-start.12 = (bf16[32,1152]{1,0:T(8,128)(2,1)S(1)}, bf16[32,1152]{1,0:T(8,128)(2,1)S(1)}, u32[]{:S(2)}, u32[]{:S(2)}) collective-permute-start(bf16[32,1152]{1,0:T(8,128)(2,1)S(1)} %pad_maximum_fusion.refs_0_.mine_ref), channel_id=1, source_target_pairs={{0,24},{1,25},{2,26},{3,27},{4,28},{5,29},{6,30},{7,31},{8,16},{9,... | collective-permute-start | bytes 221192 | tf_op jit(solution)/shard_map/ppermute | solution.py:22
  34.3 2.9 %collective-permute-start.13 = (bf16[32,1152]{1,0:T(8,128)(2,1)S(1)}, bf16[32,1152]{1,0:T(8,128)(2,1)S(1)}, u32[]{:S(2)}, u32[]{:S(2)}) collective-permute-start(bf16[32,1152]{1,0:T(8,128)(2,1)S(1)} %pad_maximum_fusion.refs_0_.mine_ref), channel_id=1, source_target_pairs={{0,1},{1,0},{2,3},{3,2},{4,5},{5,4},{6,7},{7,6},{8,9},{9,8},{10,11... | collective-permute-start | bytes 221192 | tf_op jit(solution)/shard_map/ppermute | solution.py:46
  35.9 2.7 %collective-permute-start.14 = (bf16[32,1024]{1,0:T(8,128)(2,1)S(1)}, bf16[32,1024]{1,0:T(8,128)(2,1)S(1)}, u32[]{:S(2)}, u32[]{:S(2)}) collective-permute-start(bf16[32,1024]{1,0:T(8,128)(2,1)S(1)} %slice.40), channel_id=1, source_target_pairs={{0,1},{1,0},{2,3},{3,2},{4,5},{5,4},{6,7},{7,6},{8,9},{9,8},{10,11... | collective-permute-start | bytes 196616 | tf_op jit(solution)/shard_map/ppermute | solution.py:46
  36.2 2.4 %collective-permute-start.15 = (bf16[32,1024]{1,0:T(8,128)(2,1)S(1)}, bf16[32,1024]{1,0:T(8,128)(2,1)S(1)}, u32[]{:S(2)}, u32[]{:S(2)}) collective-permute-start(bf16[32,1024]{1,0:T(8,128)(2,1)S(1)} %slice.41), channel_id=1, source_target_pairs={{0,1},{1,0},{2,3},{3,2},{4,5},{5,4},{6,7},{7,6},{8,9},{9,8},{10,11... | collective-permute-start | bytes 196616 | tf_op jit(solution)/shard_map/ppermute | solution.py:46
  37.2 1.4 %collective-permute-start.16 = (bf16[32,1024]{1,0:T(8,128)(2,1)S(1)}, bf16[32,1024]{1,0:T(8,128)(2,1)S(1)}, u32[]{:S(2)}, u32[]{:S(2)}) collective-permute-start(bf16[32,1024]{1,0:T(8,128)(2,1)S(1)} %slice.42), channel_id=1, source_target_pairs={{0,1},{1,0},{2,3},{3,2},{4,5},{5,4},{6,7},{7,6},{8,9},{9,8},{10,11... | collective-permute-start | bytes 196616 | tf_op jit(solution)/shard_map/ppermute | solution.py:46
  39.4 1.6 %collective-permute-start.18 = (bf16[96,1024]{1,0:T(8,128)(2,1)S(1)}, bf16[96,1024]{1,0:T(8,128)(2,1)S(1)}, u32[]{:S(2)}, u32[]{:S(2)}) collective-permute-start(bf16[96,1024]{1,0:T(8,128)(2,1)S(1)} %get-tuple-element.73), channel_id=1, source_target_pairs={{0,1},{1,0},{2,3},{3,2},{4,5},{5,4},{6,7},{7,6},{8,9},{9,8},{10,11... | collective-permute-start | bytes 589832 | tf_op jit(solution)/shard_map/ppermute | solution.py:46
  40.3 4.1 %collective-permute-start.17 = (bf16[32,1024]{1,0:T(8,128)(2,1)S(1)}, bf16[32,1024]{1,0:T(8,128)(2,1)S(1)}, u32[]{:S(2)}, u32[]{:S(2)}) collective-permute-start(bf16[32,1024]{1,0:T(8,128)(2,1)S(1)} %get-tuple-element.71), channel_id=1, source_target_pairs={{0,1},{1,0},{2,3},{3,2},{4,5},{5,4},{6,7},{7,6},{8,9},{9,8},{10,11... | collective-permute-start | bytes 196616 | tf_op jit(solution)/shard_map/ppermute | solution.py:46
  41.1 4.9 %collective-permute-start.21 = (bf16[32,1024]{1,0:T(8,128)(2,1)S(1)}, bf16[32,1024]{1,0:T(8,128)(2,1)S(1)}, u32[]{:S(2)}, u32[]{:S(2)}) collective-permute-start(bf16[32,1024]{1,0:T(8,128)(2,1)S(1)} %get-tuple-element.84), channel_id=1, source_target_pairs={{25,0},{24,1},{27,2},{26,3},{29,4},{28,5},{31,6},{30,7},{17,8},{16... | collective-permute-start | bytes 196616 | tf_op jit(solution)/shard_map/ppermute | solution.py:22
  43.5 4.1 %collective-permute-start.20 = (bf16[32,1024]{1,0:T(8,128)(2,1)S(1)}, bf16[32,1024]{1,0:T(8,128)(2,1)S(1)}, u32[]{:S(2)}, u32[]{:S(2)}) collective-permute-start(bf16[32,1024]{1,0:T(8,128)(2,1)S(1)} %get-tuple-element.85), channel_id=1, source_target_pairs={{17,0},{16,1},{19,2},{18,3},{21,4},{20,5},{23,6},{22,7},{25,8},{24... | collective-permute-start | bytes 196616 | tf_op jit(solution)/shard_map/ppermute | solution.py:22
  43.7 3.9 %collective-permute-start.19 = (bf16[32,1024]{1,0:T(8,128)(2,1)S(1)}, bf16[32,1024]{1,0:T(8,128)(2,1)S(1)}, u32[]{:S(2)}, u32[]{:S(2)}) collective-permute-start(bf16[32,1024]{1,0:T(8,128)(2,1)S(1)} %get-tuple-element.83), channel_id=1, source_target_pairs={{9,0},{8,1},{11,2},{10,3},{13,4},{12,5},{15,6},{14,7},{1,8},{0,9},... | collective-permute-start | bytes 196616 | tf_op jit(solution)/shard_map/ppermute | solution.py:22
  47.6 8.8 %collective-permute-start.24 = (bf16[32,256]{1,0:T(8,128)(2,1)S(1)}, bf16[32,256]{1,0:T(8,128)(2,1)S(1)}, u32[]{:S(2)}, u32[]{:S(2)}) collective-permute-start(bf16[32,256]{1,0:T(8,128)(2,1)S(1)} %get-tuple-element.90), channel_id=1, source_target_pairs={{0,7},{1,6},{2,5},{3,4},{4,3},{5,2},{6,1},{7,0},{8,15},{9,14},{10,... | collective-permute-start | bytes 49160 | tf_op jit(solution)/shard_map/ppermute | solution.py:22
  50.1 6.3 %collective-permute-start.23 = (bf16[32,256]{1,0:T(8,128)(2,1)S(1)}, bf16[32,256]{1,0:T(8,128)(2,1)S(1)}, u32[]{:S(2)}, u32[]{:S(2)}) collective-permute-start(bf16[32,256]{1,0:T(8,128)(2,1)S(1)} %get-tuple-element.91), channel_id=1, source_target_pairs={{0,5},{1,4},{2,7},{3,6},{4,1},{5,0},{6,3},{7,2},{8,13},{9,12},{10,... | collective-permute-start | bytes 49160 | tf_op jit(solution)/shard_map/ppermute | solution.py:22
  50.1 6.3 %collective-permute-start.22 = (bf16[32,256]{1,0:T(8,128)(2,1)S(1)}, bf16[32,256]{1,0:T(8,128)(2,1)S(1)}, u32[]{:S(2)}, u32[]{:S(2)}) collective-permute-start(bf16[32,256]{1,0:T(8,128)(2,1)S(1)} %get-tuple-element.89), channel_id=1, source_target_pairs={{0,3},{1,2},{2,1},{3,0},{4,7},{5,6},{6,5},{7,4},{8,11},{9,10},{10,... | collective-permute-start | bytes 49160 | tf_op jit(solution)/shard_map/ppermute | solution.py:22
  (11 other events, 129.2 us)
